TPU v7x, 128 devices: a whole 4x4x4 slice. The times are simulated.
128 devices in a mesh: sp: 32 (over z, y, core), tp: 4 (over x).
Axes of the slice: x: 4, y: 4, z: 4, core: 2. Of those that a mesh axis runs over, the one named last changes fastest.
Arguments:
- stream: bfloat16 [8192, 2048], P('sp'), may hold values from -6 to 6
- narrow_query_weight: bfloat16 [8192, 1024], P('sp', 'tp'), may hold values from -6 to 6
- wide_query_weight: bfloat16 [8192, 2048], P('sp', 'tp'), may hold values from -6 to 6
- value_rows_heads: bfloat16 [8192, 2, 1024], P('sp', None, 'tp'), may hold values from -6 to 6
- output_gate_logits: bfloat16 [8192, 2, 1024], P('sp', None, 'tp'), may hold values from -6 to 6
- narrow_forget_logits: bfloat16 [2, 8192, 1024], P(None, 'sp', 'tp'), may hold values from -6 to 6
- wide_forget_logits: bfloat16 [2, 8192, 2048], P(None, 'sp', 'tp'), may hold values from -6 to 6
- narrow_forget_headroom: float32 [2, 1024], P(None, 'tp'), may hold values from 0 to 0.08, as said below
- wide_forget_headroom: float32 [2, 2048], P(None, 'tp'), may hold values from 0 to 0.08, as said below
- extra_log_decay: float32 [8192, 2, 16], P('sp', None, 'tp'), may hold values from -1.4 to 0
- per_head_norm_gain: float32 [64], replicated, may hold values from 0.1 to 1.9
- mixer_output_weight: bfloat16 [2, 1024, 2048], replicated, may hold values from -0.125 to 0.125
- feedforward_norm_gain: float32 [2048], replicated, may hold values from 0.1 to 1.9
- expert_gate_matrix: bfloat16 [32, 2048, 4096], P('sp', None, 'tp'), may hold values from -0.125 to 0.125
- expert_up_matrix: bfloat16 [32, 2048, 4096], P('sp', None, 'tp'), may hold values from -0.125 to 0.125
- expert_down_matrix: bfloat16 [32, 4096, 2048], P('sp', 'tp'), may hold values from -0.09375 to 0.09375
- routes: int32 [8192, 2], P('sp'), may hold values from 0 to 31, all different within a row; in each aligned block of 64 rows (0 to 63, 64 to 127, ...) at most 8 rows name the same one
- router_scores_chosen: float32 [8192, 2], P('sp'), may hold values from -8 to 8
Outputs:
- result: bfloat16 [8192, 2048], P(('sp', 'tp'))
Inputs may be any that keep to these rules, and one draw needn't show every extreme that they name: `routes`: each row names 2 different experts; in each aligned block of 64 rows no expert is named by more than 8 rows. `narrow_forget_headroom`: positive. `wide_forget_headroom`: positive.
All inputs are finite; a program needn't handle non-finite values.
Results may differ from a plain program's by a relative error of at most 0.011.
Values may be sent and summed in bfloat16 or wider, within the bound.
No kernel may reach another device: no remote copies, remote signals or barrier semaphores. Data moves between devices by JAX's collectives and lax.ppermute only.
A program may use at most 128 MiB of HBM per device.

v0:
```python
from functools import partial

import jax
import jax.numpy as jnp
from jax import lax
from jax.sharding import Mesh
from jax.sharding import PartitionSpec as P

BLOCK = 64
SP = ("sp_0", "sp_1", "sp_2")
SP_TP = ("sp_0", "sp_1", "sp_2", "tp")


EPS = 1e-06
TOP_PRECISION = lax.Precision.HIGHEST


def neutral_like(x, identity):
    return jax.tree.map(
        lambda part, zero: jnp.zeros_like(part) + jnp.asarray(zero, part.dtype), x, identity
    )


def entering_2(x, axes, combine, identity, reverse):
    before = start = neutral_like(x, identity)
    so_far = x
    for axis in reversed(axes):
        count, here = (lax.axis_size(axis), lax.axis_index(axis))
        pieces = jax.tree.map(
            lambda part, kind: lax.all_gather(part.astype(kind), axis),
            so_far,
            jax.tree.map(lambda a: jnp.bfloat16 if a.dtype == jnp.float32 else a.dtype, x),
        )
        inside, so_far = (start, start)
        for k in reversed(range(count)) if reverse else range(count):
            passed = k > here if reverse else k < here
            so_far = combine(
                so_far, jax.tree.map(lambda part, own: part[k].astype(own.dtype), pieces, x)
            )
            inside = jax.tree.map(lambda new, old: jnp.where(passed, new, old), so_far, inside)
        before = combine(inside, before)
    return before


def copy_for_each(x, axis):
    count = lax.axis_size(axis)
    return lax.all_to_all(jnp.broadcast_to(x[None], (count, *x.shape)), axis, 0, 0, tiled=True)


def laid_out(tiles, dim):
    tiles = jnp.moveaxis(tiles, 0, dim)
    dims = tiles.shape
    return tiles.reshape(*dims[:dim], dims[dim] * dims[dim + 1], *dims[dim + 2 :])


def gathered_copies(x, axis, dim):
    tiles = copy_for_each(x, axis)
    return laid_out(tiles, dim)


def split_up(x, dim, count):
    dims = x.shape
    tiles = x.reshape(*dims[:dim], count, dims[dim] // count, *dims[dim + 1 :])
    return jnp.moveaxis(tiles, dim, 0)


def sent_and_summed(x, axis, dim):
    tiles = split_up(x, dim, lax.axis_size(axis))
    arrived = lax.all_to_all(tiles, axis, split_axis=0, concat_axis=0, tiled=True)
    return arrived.astype(jnp.float32).sum(axis=0)


def to_blocks(source, length):
    token_rows, total_head_count, breadth = source.shape
    return source.reshape(token_rows // length, length, total_head_count, breadth).transpose(
        0, 2, 1, 3
    )


def from_blocks(source):
    blocks, total_head_count, length, breadth = source.shape
    return source.transpose(0, 2, 1, 3).reshape(blocks * length, total_head_count, breadth)


def block_sweep(query_rows, block_openings, values, inside, initial):
    ending = inside[:, :, -1:, :]
    query_within_block = query_rows * jnp.exp(inside)
    k_inside = block_openings * jnp.exp(-inside)
    key_block_ending = block_openings * jnp.exp(ending - inside)
    length = query_rows.shape[2]
    triangle = jnp.tril(jnp.ones((length, length), jnp.float32))
    scores = (
        jnp.einsum("nhtk,nhsk->nhts", query_within_block, k_inside, precision=TOP_PRECISION)
        * triangle
    )
    within = jnp.einsum("nhts,nhsv->nhtv", scores, values, precision=TOP_PRECISION)

    def advance(present_state, inputs):
        block_of_queries, block_opening_state, block_of_values, ending_block = inputs
        state_readout = jnp.einsum(
            "ifm,imo->ifo", block_of_queries, present_state, precision=TOP_PRECISION
        )
        expanded_state = jnp.einsum(
            "lbi,lbp->lip", block_opening_state, block_of_values, precision=TOP_PRECISION
        )
        return (
            present_state * jnp.exp(ending_block[:, 0, :])[:, :, None] + expanded_state,
            state_readout,
        )

    closing, carried = lax.scan(
        advance, initial, (query_within_block, key_block_ending, values, ending)
    )
    return (within + carried, closing)


def prepare_inputs(query_rows, forget_gate, forget_headroom, surge_amount, head_slice):
    token_rows, total_head_count = surge_amount.shape
    query_heads = jax.nn.silu(query_rows.astype(jnp.float32)).reshape(
        token_rows, total_head_count, -1
    )
    value_heads = head_slice.astype(jnp.float32).reshape(token_rows, total_head_count, -1)
    pre_forget = forget_gate.astype(jnp.float32).reshape(2, token_rows, total_head_count, -1)
    block_openings = jax.nn.sigmoid(-pre_forget) * forget_headroom.reshape(
        2, 1, total_head_count, -1
    )
    decay_logarithm = jnp.log1p(-block_openings) + surge_amount[None, :, :, None]
    return (query_heads, block_openings, value_heads, decay_logarithm)


def combine_states(earlier, later):
    return tuple(
        (
            (
                earlier_one[0] * later_one[0],
                earlier_one[1] * later_one[0][:, :, None] + later_one[1],
            )
            for earlier_one, later_one in zip(earlier, later)
        )
    )


def entering_states(parts, backward):
    identity = tuple(((jnp.ones_like(member[0]), jnp.zeros_like(member[1])) for member in parts))
    if backward:
        return entering_2(parts, SP, combine_states, identity, True)
    return entering_2(parts, SP, combine_states, identity, False)


def one_direction(groups, backward):
    blocked = []
    insides = []
    running_state = []
    totals = []
    for group in groups:
        group_members = tuple((to_blocks(member, BLOCK) for member in group))
        inside = jnp.cumsum(group_members[3], axis=2)
        endings = inside[:, :, -1:, :]
        blocked.append(group_members)
        insides.append(inside)
        running_state.append(jnp.cumsum(endings, axis=0) - endings + inside)
        totals.append(jnp.sum(endings[:, :, 0, :], axis=0))
    swept = []
    closing = []
    for token_position in range(len(blocked)):
        group_members = blocked[token_position]
        zero_state = jnp.zeros(
            (group_members[0].shape[1], group_members[0].shape[3], group_members[2].shape[3]),
            jnp.float32,
        )
        result_pair = block_sweep(
            group_members[0],
            group_members[1],
            group_members[2],
            insides[token_position],
            zero_state,
        )
        swept.append(result_pair[0])
        closing.append(result_pair[1])
    parts = tuple(((jnp.exp(sum_log), state_end) for sum_log, state_end in zip(totals, closing)))
    entering = entering_states(parts, backward)
    outputs = []
    for token_position in range(len(blocked)):
        group_members = blocked[token_position]
        incoming_state = entering[token_position][1]
        state_readout = jnp.einsum(
            "qrxa,rai->qrxi",
            group_members[0] * jnp.exp(running_state[token_position]),
            incoming_state,
            precision=TOP_PRECISION,
        )
        outputs.append(from_blocks(swept[token_position] + state_readout))
    return outputs


def slot_table(block_routes, experts, capacity):
    flattened = block_routes.reshape(-1)
    matches = (flattened[:, None] == jnp.arange(experts, dtype=jnp.int32)[None, :]).astype(
        jnp.int32
    )
    earlier = jnp.cumsum(matches, axis=0) - matches
    token_position = jnp.sum(earlier * matches, axis=1)
    return (flattened * capacity + token_position).reshape(block_routes.shape)


def dispatch(block_slots, block_rows, slot_count):
    picks = jnp.sum(
        (block_slots[:, :, None] == jnp.arange(slot_count, dtype=jnp.int32)).astype(jnp.bfloat16),
        axis=1,
    )
    return jnp.einsum("rs,rd->sd", picks, block_rows, preferred_element_type=jnp.float32).astype(
        jnp.bfloat16
    )


def local(
    stream,
    narrow_query_weight,
    wide_query_weight,
    value_rows_heads,
    output_gate_logits,
    narrow_forget_logits,
    wide_forget_logits,
    narrow_forget_headroom,
    wide_forget_headroom,
    extra_log_decay,
    per_head_norm_gain,
    mixer_output_weight,
    feedforward_norm_gain,
    expert_gate_matrix,
    expert_up_matrix,
    expert_down_matrix,
    routes,
    router_scores_chosen,
):
    token_rows = stream.shape[0]
    prepared = [
        prepare_inputs(
            narrow_query_weight,
            narrow_forget_logits,
            narrow_forget_headroom,
            extra_log_decay[:, 0],
            value_rows_heads[:, 0],
        ),
        prepare_inputs(
            wide_query_weight,
            wide_forget_logits,
            wide_forget_headroom,
            extra_log_decay[:, 1],
            value_rows_heads[:, 1],
        ),
    ]
    ahead = one_direction(
        [(group[0], group[1][0], group[2], group[3][0]) for group in prepared], False
    )
    behind = one_direction(
        [
            (
                jnp.flip(group[0], 0),
                jnp.flip(group[1][1], 0),
                jnp.flip(group[2], 0),
                jnp.flip(group[3][1], 0),
            )
            for group in prepared
        ],
        True,
    )
    mixed_groups = []
    for head_group_index in range(2):
        summed = ahead[head_group_index] + jnp.flip(behind[head_group_index], 0)
        scale = lax.rsqrt(jnp.mean(summed * summed, axis=-1, keepdims=True) + EPS)
        gate_heads = jax.nn.silu(
            output_gate_logits[:, head_group_index].astype(jnp.float32)
        ).reshape(summed.shape)
        mixed_groups.append(
            (summed * scale * per_head_norm_gain * gate_heads).reshape(token_rows, -1)
        )
    mixed = jnp.stack(mixed_groups, axis=1).astype(jnp.bfloat16)
    model_width = mixer_output_weight.shape[2]
    projected = jnp.einsum(
        "tgc,gcd->td",
        gathered_copies(mixed, "tp", 2),
        mixer_output_weight,
        preferred_element_type=jnp.float32,
    )
    residual = stream.astype(jnp.float32) + projected
    norm_rows = (
        residual
        * lax.rsqrt(jnp.mean(residual * residual, axis=-1, keepdims=True) + EPS)
        * feedforward_norm_gain
    ).astype(jnp.bfloat16)
    group_count = lax.axis_size("tp")
    experts = lax.axis_size(SP)
    row_count = token_rows // group_count
    top_count = routes.shape[1]
    capacity = max(2, 2 * top_count * row_count // experts)
    slot_count = experts * capacity
    own_index = lax.axis_index("tp")
    slot_ids = jax.vmap(partial(slot_table, experts=experts, capacity=capacity))(
        routes.reshape(group_count, row_count, top_count)
    )
    grouped_rows = norm_rows.reshape(group_count, row_count, model_width)
    gate_weights = expert_gate_matrix[0]
    up_weights = expert_up_matrix[0]
    down_weights = expert_down_matrix[0]
    own_slots = lax.dynamic_index_in_dim(slot_ids, own_index, 0, keepdims=False)
    buffers = jax.vmap(partial(dispatch, slot_count=slot_count))(slot_ids, grouped_rows)
    buffers = buffers.reshape(group_count, experts, capacity, model_width)
    arrived = lax.all_to_all(buffers, SP, split_axis=1, concat_axis=1, tiled=True)
    gate_part = jnp.einsum(
        "...d,df->...f", arrived, gate_weights, preferred_element_type=jnp.float32
    )
    up_part = jnp.einsum("...d,df->...f", arrived, up_weights, preferred_element_type=jnp.float32)
    hidden = (jax.nn.silu(gate_part) * up_part).astype(jnp.bfloat16)
    sources = hidden.shape[1]
    count = hidden.shape[2]
    flattened = hidden.reshape(-1, hidden.shape[3])
    summed_rows = sent_and_summed(
        jnp.dot(flattened, down_weights, preferred_element_type=jnp.float32).astype(jnp.bfloat16),
        "tp",
        0,
    )
    returning = summed_rows.astype(jnp.bfloat16).reshape(sources, count, -1)
    returned = lax.all_to_all(returning, SP, split_axis=0, concat_axis=0, tiled=True)
    picked = returned.reshape(slot_count, model_width)[own_slots]
    own_logits = lax.dynamic_slice_in_dim(router_scores_chosen, own_index * row_count, row_count, 0)
    weights = jax.nn.sigmoid(own_logits - own_logits[:, ::-1])
    own_residual = lax.dynamic_slice_in_dim(residual, own_index * row_count, row_count, 0)
    mixed_out = jnp.sum(weights[:, :, None] * picked.astype(jnp.float32), axis=1)
    return (own_residual + mixed_out).astype(jnp.bfloat16)


def solution(mesh):
    torus = Mesh(mesh.devices.reshape(4, 4, 2, mesh.shape["tp"]), ("sp_0", "sp_1", "sp_2", "tp"))
    return jax.shard_map(
        local,
        mesh=torus,
        in_specs=(
            P(SP, None),
            P(SP, "tp"),
            P(SP, "tp"),
            P(SP, None, "tp"),
            P(SP, None, "tp"),
            P(None, SP, "tp"),
            P(None, SP, "tp"),
            P(None, "tp"),
            P(None, "tp"),
            P(SP, None, "tp"),
            P(),
            P(),
            P(),
            P(SP, None, "tp"),
            P(SP, None, "tp"),
            P(SP, "tp", None),
            P(SP, None),
            P(SP, None),
        ),
        out_specs=P(SP_TP, None),
        check_vma=False,
    )
```

profile of v0, /device:TPU:1, one launch (start us, length us, event | category | flops | bytes accessed | tf_op | source)
XLA Modules:
  0.0 487.3 jit_solution(6591007310275203923)
XLA Ops:
  8.9 8.1 %all_gather.126 = bf16[4,4,128]{2,1,0:T(4,128)(2,1)S(1)} all-gather(bf16[1,4,128]{2,1,0:T(4,128)(2,1)S(1)} %fusion.440), channel_id=1, replica_groups=mesh['sp_0'=4,'sp_1'=4,'sp_2'=2,'tp'=4] {'sp_1'}, dimensions={0}, use_global_device_ids=true | all-gather | bytes 5120 | tf_op jit(solution)/shard_map/all_gather | solution.py:30
  17.0 9.0 %all_gather.127 = bf16[4,4,128]{2,1,0:T(4,128)(2,1)S(1)} all-gather(bf16[1,4,128]{2,1,0:T(4,128)(2,1)S(1)} %fusion.431), channel_id=1, replica_groups=mesh['sp_0'=4,'sp_1'=4,'sp_2'=2,'tp'=4] {'sp_0'}, dimensions={0}, use_global_device_ids=true | all-gather | bytes 5120 | tf_op jit(solution)/shard_map/all_gather | solution.py:30
  27.4 5.8 %all-gather.10 = bf16[2,4,128]{2,1,0:T(4,128)(2,1)S(1)} all-gather(bf16[1,4,128]{2,1,0:T(4,128)(2,1)S(1)} %fusion.446), channel_id=6, replica_groups=mesh['sp_0'=4,'sp_1'=4,'sp_2'=2,'tp'=4] {'sp_2'}, dimensions={0}, use_global_device_ids=true | all-gather | bytes 3072 | tf_op jit(solution)/shard_map/all_gather | solution.py:30
  55.4 7.0 %all_gather.112 = bf16[4,4,64]{2,1,0:T(4,128)(2,1)S(1)} all-gather(bf16[1,4,64]{2,1,0:T(4,128)(2,1)S(1)} %fusion.442), channel_id=1, replica_groups=mesh['sp_0'=4,'sp_1'=4,'sp_2'=2,'tp'=4] {'sp_1'}, dimensions={0}, use_global_device_ids=true | all-gather | bytes 2560 | tf_op jit(solution)/shard_map/all_gather | solution.py:30
  63.6 7.0 %all_gather.113 = bf16[4,4,64]{2,1,0:T(4,128)(2,1)S(1)} all-gather(bf16[1,4,64]{2,1,0:T(4,128)(2,1)S(1)} %fusion.421), channel_id=1, replica_groups=mesh['sp_0'=4,'sp_1'=4,'sp_2'=2,'tp'=4] {'sp_0'}, dimensions={0}, use_global_device_ids=true | all-gather | bytes 2560 | tf_op jit(solution)/shard_map/all_gather | solution.py:30
  73.3 5.8 %all-gather.8 = bf16[2,4,64]{2,1,0:T(4,128)(2,1)S(1)} all-gather(bf16[1,4,64]{2,1,0:T(4,128)(2,1)S(1)} %fusion.444), channel_id=2, replica_groups=mesh['sp_0'=4,'sp_1'=4,'sp_2'=2,'tp'=4] {'sp_2'}, dimensions={0}, use_global_device_ids=true | all-gather | bytes 1536 | tf_op jit(solution)/shard_map/all_gather | solution.py:30
  113.5 13.0 %while.55 = (s32[]{:T(128)}, f32[4,128,64]{1,2,0:T(8,128)S(1)}, f32[4,4,64,64]{3,2,1,0:T(8,128)}, f32[4,4,1,128]{3,1,2,0:T(4,128)S(1)}, f32[4,4,64,128]{3,2,1,0:...) while((s32[]{:T(128)}, f32[4,128,64]{1,2,0:T(8,128)S(1)}, ...), condition=%wide.region_18.19_spmd.clone, body=%wide.region_17.18_spmd.clone.sunk | while | flops 50462720 | bytes 990832 | solution.py:111
  132.0 9.4 %all_gather.130 = bf16[4,4,128,64]{2,3,1,0:T(8,128)(2,1)S(1)} all-gather(bf16[1,4,128,64]{2,3,1,0:T(8,128)(2,1)S(1)} %fusion.234), channel_id=1, replica_groups=mesh['sp_0'=4,'sp_1'=4,'sp_2'=2,'tp'=4] {'sp_1'}, dimensions={0}, use_global_device_ids=true | all-gather | bytes 327680 | tf_op jit(solution)/shard_map/all_gather | solution.py:30
  141.5 9.5 %all_gather.131 = bf16[4,4,128,64]{2,3,1,0:T(8,128)(2,1)S(1)} all-gather(bf16[1,4,128,64]{2,3,1,0:T(8,128)(2,1)S(1)} %fusion.216), channel_id=1, replica_groups=mesh['sp_0'=4,'sp_1'=4,'sp_2'=2,'tp'=4] {'sp_0'}, dimensions={0}, use_global_device_ids=true | all-gather | bytes 327680 | tf_op jit(solution)/shard_map/all_gather | solution.py:30
  166.5 12.0 %while.54 = (s32[]{:T(128)}, f32[4,128,64]{1,2,0:T(8,128)S(1)}, f32[4,4,64,64]{3,2,1,0:T(8,128)}, f32[4,4,1,128]{3,1,2,0:T(4,128)}, f32[4,4,64,128]{3,2,1,0:T(8,...) while((s32[]{:T(128)}, f32[4,128,64]{1,2,0:T(8,128)S(1)}, ...), condition=%wide.region_13.14_spmd.clone, body=%wide.region_12.13_spmd.clone.sunk | while | flops 50462720 | bytes 925804 | solution.py:111
  178.5 7.7 %all-gather.5 = bf16[8,128,64]{1,2,0:T(8,128)(2,1)S(1)} all-gather(bf16[4,128,64]{1,2,0:T(8,128)(2,1)S(1)} %convert_element_type.1218), channel_id=7, replica_groups=mesh['sp_0'=4,'sp_1'=4,'sp_2'=2,'tp'=4] {'sp_2'}, dimensions={0}, use_global_device_ids=true | all-gather | bytes 196608 | tf_op jit(solution)/shard_map/all_gather | solution.py:30
  187.0 9.5 %all_gather.123 = bf16[4,4,128,64]{2,3,1,0:T(8,128)(2,1)S(1)} all-gather(bf16[1,4,128,64]{2,3,1,0:T(8,128)(2,1)S(1)} %fusion.230), channel_id=1, replica_groups=mesh['sp_0'=4,'sp_1'=4,'sp_2'=2,'tp'=4] {'sp_1'}, dimensions={0}, use_global_device_ids=true | all-gather | bytes 327680 | tf_op jit(solution)/shard_map/all_gather | solution.py:30
  197.3 9.4 %all_gather.124 = bf16[4,4,128,64]{2,3,1,0:T(8,128)(2,1)S(1)} all-gather(bf16[1,4,128,64]{2,3,1,0:T(8,128)(2,1)S(1)} %fusion.198), channel_id=1, replica_groups=mesh['sp_0'=4,'sp_1'=4,'sp_2'=2,'tp'=4] {'sp_0'}, dimensions={0}, use_global_device_ids=true | all-gather | bytes 327680 | tf_op jit(solution)/shard_map/all_gather | solution.py:30
  228.3 7.6 %all-gather.3 = bf16[8,64,64]{2,1,0:T(8,128)(2,1)S(1)} all-gather(bf16[4,64,64]{2,1,0:T(8,128)(2,1)S(1)} %convert_element_type.1156), channel_id=5, replica_groups=mesh['sp_0'=4,'sp_1'=4,'sp_2'=2,'tp'=4] {'sp_2'}, dimensions={0}, use_global_device_ids=true | all-gather | bytes 98304 | tf_op jit(solution)/shard_map/all_gather | solution.py:30
  236.8 9.7 %all_gather.116 = bf16[4,4,64,64]{3,2,1,0:T(8,128)(2,1)S(1)} all-gather(bf16[1,4,64,64]{3,2,1,0:T(8,128)(2,1)S(1)} %fusion.226), channel_id=1, replica_groups=mesh['sp_0'=4,'sp_1'=4,'sp_2'=2,'tp'=4] {'sp_1'}, dimensions={0}, use_global_device_ids=true | all-gather | bytes 163840 | tf_op jit(solution)/shard_map/all_gather | solution.py:30
  247.4 9.6 %all_gather.117 = bf16[4,4,64,64]{3,2,1,0:T(8,128)(2,1)S(1)} all-gather(bf16[1,4,64,64]{3,2,1,0:T(8,128)(2,1)S(1)} %fusion.180), channel_id=1, replica_groups=mesh['sp_0'=4,'sp_1'=4,'sp_2'=2,'tp'=4] {'sp_0'}, dimensions={0}, use_global_device_ids=true | all-gather | bytes 163840 | tf_op jit(solution)/shard_map/all_gather | solution.py:30
  267.4 7.4 %all-gather.1 = bf16[8,64,64]{2,1,0:T(8,128)(2,1)S(1)} all-gather(bf16[4,64,64]{2,1,0:T(8,128)(2,1)S(1)} %convert_element_type.1096), channel_id=3, replica_groups=mesh['sp_0'=4,'sp_1'=4,'sp_2'=2,'tp'=4] {'sp_2'}, dimensions={0}, use_global_device_ids=true | all-gather | bytes 98304 | tf_op jit(solution)/shard_map/all_gather | solution.py:30
  275.6 9.9 %all_gather.109 = bf16[4,4,64,64]{3,2,1,0:T(8,128)(2,1)S(1)} all-gather(bf16[1,4,64,64]{3,2,1,0:T(8,128)(2,1)S(1)} %fusion.222), channel_id=1, replica_groups=mesh['sp_0'=4,'sp_1'=4,'sp_2'=2,'tp'=4] {'sp_1'}, dimensions={0}, use_global_device_ids=true | all-gather | bytes 163840 | tf_op jit(solution)/shard_map/all_gather | solution.py:30
  286.4 9.4 %all_gather.110 = bf16[4,4,64,64]{3,2,1,0:T(8,128)(2,1)S(1)} all-gather(bf16[1,4,64,64]{3,2,1,0:T(8,128)(2,1)S(1)} %fusion.162), channel_id=1, replica_groups=mesh['sp_0'=4,'sp_1'=4,'sp_2'=2,'tp'=4] {'sp_0'}, dimensions={0}, use_global_device_ids=true | all-gather | bytes 163840 | tf_op jit(solution)/shard_map/all_gather | solution.py:30
  307.7 8.3 %all-to-all-done = bf16[4,256,2,256]{3,1,2,0:T(8,128)(2,1)S(1)} async-done(((bf16[4,256,2,256]{3,1,2,0:T(8,128)(2,1)}), bf16[4,256,2,256]{3,1,2,0:T(8,128)(2,1)S(1)}, u32[]{:S(2)}, u32[]{:S(2)}) %all-to-all-start) | async-done | bytes 1048608 | tf_op jit(solution)/shard_map/all_to_all | solution.py:47
  316.2 6.1 %multiply_reduce_fusion = (f32[256]{0:T(256)S(1)}, f32[256,2048]{1,0:T(8,128)S(1)}) fusion(bf16[256,2,1024]{2,0,1:T(8,128)(2,1)S(1)} %bitcast.1018, bf16[2,1024,2048]{2,1,0:T(8,128)(2,1)} %param.37, bf16[256,2048]{1,0:T(8,128)(2,1)} %param.26), kind=kOutput, calls=%fused_computation.78 | convolution fusion | flops 2149580544 | bytes 12583936 | tf_op jit(solution)/shard_map/tgc,gcd->td/dot_general | solution.py:280
  324.5 63.8 %all_to_all.20 = bf16[4,32,8,2048]{3,2,0,1:T(8,128)(2,1)S(1)} all-to-all(bf16[4,32,8,2048]{3,2,0,1:T(8,128)(2,1)S(1)} %copy.277), channel_id=1, replica_groups=mesh['sp_0'=4,'sp_1'=4,'sp_2'=2,'tp'=4] {'sp_0','sp_1','sp_2'}, dimensions={1} | all-to-all | bytes 8388608 | tf_op jit(solution)/shard_map/all_to_all | solution.py:309
  403.0 51.9 %all_to_all.21 = bf16[4,256,2048]{2,1,0:T(8,128)(2,1)} all-to-all(bf16[4,256,2048]{2,1,0:T(8,128)(2,1)S(1)} %bitcast.1006), channel_id=1, replica_groups=mesh['sp_0'=4,'sp_1'=4,'sp_2'=2,'tp'=4] {'tp'}, dimensions={0} | all-to-all | bytes 8388608 | tf_op jit(solution)/shard_map/all_to_all | solution.py:69
  464.9 16.5 %all-to-all-done.3 = bf16[32,8,2048]{2,1,0:T(8,128)(2,1)S(1)} async-done(((bf16[32,8,2048]{2,1,0:T(8,128)(2,1)}), bf16[32,8,2048]{2,1,0:T(8,128)(2,1)S(1)}, u32[]{:S(2)}, u32[]{:S(2)}) %all-to-all-start.3) | async-done | bytes 1048608 | tf_op jit(solution)/shard_map/all_to_all | solution.py:324
  (309 shorter events, 205.0 us)
Async XLA Ops:
  4.6 42.3 %copy-start.15 = (bf16[2,256,256]{2,1,0:T(8,128)(2,1)S(1)}, bf16[2,256,256]{2,1,0:T(8,128)(2,1)}, u32[]{:S(2)}) copy-start(bf16[2,256,256]{2,1,0:T(8,128)(2,1)} %param.31) | copy-start | bytes 786436
  4.6 42.6 %copy-start.21 = (f32[2,256]{1,0:T(2,128)S(1)}, f32[2,256]{1,0:T(2,128)}, u32[]{:S(2)}) copy-start(f32[2,256]{1,0:T(2,128)} %param.33) | copy-start | bytes 6148
  26.1 133.3 %copy-start.12 = (f32[64,64]{1,0:T(8,128)}, f32[64,64]{1,0:T(8,128)S(1)}, u32[]{:S(2)}) copy-start(f32[64,64]{1,0:T(8,128)S(1)} %fusion.399) | copy-start | bytes 49156
  126.5 26.7 %copy-start = (f32[256,4,128]{2,0,1:T(8,128)S(1)}, f32[256,4,128]{2,0,1:T(8,128)}, u32[]{:S(2)}) copy-start(f32[256,4,128]{2,0,1:T(8,128)} %copy.258) | copy-start | bytes 1572868
  126.5 27.5 %copy-start.1 = (f32[4,4,64,64]{3,2,1,0:T(8,128)S(1)}, f32[4,4,64,64]{3,2,1,0:T(8,128)}, u32[]{:S(2)}) copy-start(f32[4,4,64,64]{3,2,1,0:T(8,128)} %get-tuple-element.163) | copy-start | bytes 786436
  178.5 32.0 %copy-start.6 = (f32[256,4,64]{0,2,1:T(8,128)S(1)}, f32[256,4,64]{0,2,1:T(8,128)}, u32[]{:S(2)}) copy-start(f32[256,4,64]{0,2,1:T(8,128)} %rev.44) | copy-start | bytes 786436
  178.5 33.4 %copy-start.11 = (f32[256,4,64]{0,2,1:T(8,128)S(1)}, f32[256,4,64]{0,2,1:T(8,128)}, u32[]{:S(2)}) copy-start(f32[256,4,64]{0,2,1:T(8,128)} %get-tuple-element.479) | copy-start | bytes 786436
  210.2 5.3 %copy-start.13 = (f32[64,64]{1,0:T(8,128)S(1)}, f32[64,64]{1,0:T(8,128)}, u32[]{:S(2)}) copy-start(f32[64,64]{1,0:T(8,128)} %copy-done.12) | copy-start | bytes 49156
  228.2 30.9 %copy-start.2 = (f32[4,4,64,64]{3,2,1,0:T(8,128)S(1)}, f32[4,4,64,64]{3,2,1,0:T(8,128)}, u32[]{:S(2)}) copy-start(f32[4,4,64,64]{3,2,1,0:T(8,128)} %get-tuple-element.159) | copy-start | bytes 786436
  228.3 30.9 %copy-start.4 = (f32[4,4,64,64]{3,2,1,0:T(8,128)S(1)}, f32[4,4,64,64]{3,2,1,0:T(8,128)}, u32[]{:S(2)}) copy-start(f32[4,4,64,64]{3,2,1,0:T(8,128)} %convolution_multiply_fusion.2) | copy-start | bytes 786436
  235.9 25.4 %copy-start.10 = (f32[1,256,4,64]{1,3,2,0:T(8,128)S(1)}, f32[1,256,4,64]{1,3,2,0:T(8,128)}, u32[]{:S(2)}) copy-start(f32[1,256,4,64]{1,3,2,0:T(8,128)} %get-tuple-element.480) | copy-start | bytes 786436
  263.9 10.9 %copy-start.19 = (f32[4,64]{1,0:T(4,128)S(1)}, f32[4,64]{1,0:T(4,128)}, u32[]{:S(2)}) copy-start(f32[4,64]{1,0:T(4,128)} %get-tuple-element.532) | copy-start | bytes 3076
  264.1 21.4 %copy-start.18 = (f32[4,64]{1,0:T(4,128)S(1)}, f32[4,64]{1,0:T(4,128)}, u32[]{:S(2)}) copy-start(f32[4,64]{1,0:T(4,128)} %get-tuple-element.513) | copy-start | bytes 3076
  267.3 32.7 %copy-start.5 = (f32[256,4,64]{0,2,1:T(8,128)S(1)}, f32[256,4,64]{0,2,1:T(8,128)}, u32[]{:S(2)}) copy-start(f32[256,4,64]{0,2,1:T(8,128)} %rev.39) | copy-start | bytes 786436
  267.3 32.8 %copy-start.7 = (bf16[256,2,256]{2,1,0:T(2,128)(2,1)S(1)}, bf16[256,2,256]{2,1,0:T(2,128)(2,1)}, u32[]{:S(2)}) copy-start(bf16[256,2,256]{2,1,0:T(2,128)(2,1)} %param.30) | copy-start | bytes 786436
  295.8 5.0 %copy-start.16 = (f32[256,4]{0,1:T(4,128)S(1)}, f32[256,4]{0,1:T(4,128)}, u32[]{:S(2)}) copy-start(f32[256,4]{0,1:T(4,128)} %add_rsqrt_fusion) | copy-start | bytes 12292
  295.8 5.0 %copy-start.23 = (f32[64]{0:T(128)S(1)}, f32[64]{0:T(128)}, u32[]{:S(2)}) copy-start(f32[64]{0:T(128)} %param.36) | copy-start | bytes 772
  300.1 6.3 %copy-start.20 = (s32[256,2]{0,1:T(2,128)S(1)}, s32[256,2]{0,1:T(2,128)}, u32[]{:S(2)}) copy-start(s32[256,2]{0,1:T(2,128)} %param.42) | copy-start | bytes 6148
  302.3 13.8 %all-to-all-start = ((bf16[4,256,2,256]{3,1,2,0:T(8,128)(2,1)}), bf16[4,256,2,256]{3,1,2,0:T(8,128)(2,1)S(1)}, u32[]{:S(2)}, u32[]{:S(2)}) async-start(bf16[4,256,2,256]{3,1,2,0:T(8,128)(2,1)} %broadcast_in_dim.25), calls=%async_computation | async-start | bytes 2097152 | tf_op jit(solution)/shard_map/all_to_all | solution.py:47
  316.2 6.2 %copy-start.17 = (f32[2048]{0:T(1024)S(1)}, f32[2048]{0:T(1024)}, u32[]{:S(2)}) copy-start(f32[2048]{0:T(1024)} %param.38) | copy-start | bytes 24580
  324.5 63.8 %copy-start.24 = (bf16[1,2048,1024]{2,1,0:T(8,128)(2,1)S(1)}, bf16[1,2048,1024]{2,1,0:T(8,128)(2,1)}, u32[]{:S(2)}) copy-start(bf16[1,2048,1024]{2,1,0:T(8,128)(2,1)} %param.40) | copy-start | bytes 12582916
  392.8 5.4 %copy-start.26 = (bf16[1,1024,2048]{2,1,0:T(8,128)(2,1)S(1)}, bf16[1,1024,2048]{2,1,0:T(8,128)(2,1)}, u32[]{:S(2)}) copy-start(bf16[1,1024,2048]{2,1,0:T(8,128)(2,1)} %param.41) | copy-start | bytes 12582916
  454.9 9.6 %copy-start.22 = (f32[256,2]{0,1:T(2,128)S(1)}, f32[256,2]{0,1:T(2,128)}, u32[]{:S(2)}) copy-start(f32[256,2]{0,1:T(2,128)} %param.43) | copy-start | bytes 6148
  459.2 22.2 %all-to-all-start.3 = ((bf16[32,8,2048]{2,1,0:T(8,128)(2,1)}), bf16[32,8,2048]{2,1,0:T(8,128)(2,1)S(1)}, u32[]{:S(2)}, u32[]{:S(2)}) async-start(bf16[32,8,2048]{2,1,0:T(8,128)(2,1)} %bitcast.173), calls=%async_computation.3 | async-start | bytes 2097152 | tf_op jit(solution)/shard_map/all_to_all | solution.py:324
  (5 other events, 20.0 us)
where the time goes:
time: 496 us; the launch traced here: 487 us
  blocking collectives  292 us (59%)
  matrix products  70.7 us (14%)
  local copies, waits for them, and re-layouts  53.8 us (11%)
  other arithmetic  34.8 us (7%)
  waiting for transfers between devices  24.8 us (5%)
  starting transfers between devices  9.12 us (2%)
    all_gather x24, blocking collectives, entering_2(): lax.all_gather(part.astype(kind), axis)  177 us
    all_to_all x1, blocking collectives, local(): lax.all_to_all(buffers, SP, split_axis=1, concat_axis=1, tiled=True)  63.8 us
    all_to_all x1, blocking collectives, sent_and_summed(): lax.all_to_all(tiles, axis, split_axis=0, concat_axis=0, tiled=True)  51.9 us
    dot_general x16, matrix products, advance(): jnp.einsum('ifm,imo->ifo', block_of_queries, present_state, precision=TOP...  19.9 us
    all_to_all x1, waiting for transfers between devices, local(): lax.all_to_all(returning, SP, split_axis=0, concat_axis=0, tiled=True)  16.5 us
  transfers between devices with their start and end apart: 2, of which 2 were waited for; matrix products, arithmetic and copies ran while one was open for 0% of the time, Pallas kernels for 0%

commit v1 on v0

v1 whole, which is shorter than its diff:
```python
from functools import partial

import jax
import jax.numpy as jnp
from jax import lax
from jax.experimental import pallas as pl
from jax.experimental.pallas import tpu as pltpu
from jax.sharding import Mesh
from jax.sharding import PartitionSpec as P

SP = ("sp_0", "sp_1", "sp_2")
SP_TP = ("sp_0", "sp_1", "sp_2", "tp")

EPS = 1e-06
F32 = jnp.float32
BF16 = jnp.bfloat16

TOK = 256
BLK = 64
NB = TOK // BLK
LANES = 128
TILES = 6
STATE_ROWS = 2 * TILES * 64
PAY_ROWS = STATE_ROWS + 32


def dot(a, b):
    return lax.dot_general(a, b, (((1,), (0,)), ((), ())), preferred_element_type=F32)


def dot_t(a, b):
    return lax.dot_general(a, b, (((1,), (1,)), ((), ())), preferred_element_type=F32)


def silu(x):
    return x / (1.0 + jnp.exp(-x))


def local_kernel(
    nq_ref, wq_ref, nf_ref, wf_ref, nh_ref, wh_ref, ex_ref, v0_ref, v1_ref, pay_ref, out_ref, qr_ref
):
    ri = lax.broadcasted_iota(jnp.int32, (TOK, TOK), 0)
    ci = lax.broadcasted_iota(jnp.int32, (TOK, TOK), 1)
    same = (ri // BLK) == (ci // BLK)
    tri = (same & (ci <= ri), same & (ci >= ri))
    ones = tuple(jnp.where(t, 1.0, 0.0).astype(BF16) for t in tri)
    lane = lax.broadcasted_iota(jnp.int32, (1, LANES), 1)
    low = lane < 64
    low2 = (lax.broadcasted_iota(jnp.int32, (1, 2 * LANES), 1) % LANES) < 64
    decays = [None] * (2 * TILES)

    def prepare(tile, q_raw, f_raw, rooms, extra):
        q = silu(q_raw.astype(F32)).reshape(NB, BLK, LANES)
        qi, ki, ke, qr, ends = [], [], [], [], []
        for d in range(2):
            opening = rooms[d] / (1.0 + jnp.exp(f_raw[d].astype(F32)))
            ld = jnp.log(1.0 - opening) + extra
            hi = ld.astype(BF16)
            lo = (ld - hi.astype(F32)).astype(BF16)
            both = dot(ones[d], jnp.concatenate([hi, lo], axis=1))
            inside = (both[:, :LANES] + both[:, LANES:]).reshape(NB, BLK, LANES)
            opening = opening.reshape(NB, BLK, LANES)
            edge = BLK - 1 if d == 0 else 0
            end = [inside[b, edge : edge + 1, :] for b in range(NB)]
            start = [None] * NB
            run = jnp.zeros((1, LANES), F32)
            for b in range(NB) if d == 0 else reversed(range(NB)):
                start[b] = run
                run = run + end[b]
            decays[d * TILES + tile] = jnp.exp(run)
            start4 = jnp.stack(start, axis=0)
            end4 = jnp.stack(end, axis=0)
            qi.append((q * jnp.exp(inside)).reshape(TOK, LANES))
            qr.append((q * jnp.exp(inside + start4)).reshape(TOK, LANES).astype(BF16))
            ki.append((opening * jnp.exp(-inside)).reshape(TOK, LANES))
            ke.append((opening * jnp.exp(end4 - inside)).reshape(TOK, LANES).astype(BF16))
            ends.append([jnp.exp(e) for e in end])
        qr_ref[tile] = jnp.concatenate(qr, axis=1)
        return qi, ki, jnp.concatenate(ke, axis=1), ends

    def block_states(tile, kv, ends):
        states = [[None, None] for _ in range(NB)]
        for d in range(2):
            run = jnp.zeros((64, LANES), F32)
            for b in range(NB) if d == 0 else reversed(range(NB)):
                states[b][d] = run
                run = run * ends[d][b] + kv[b * 64 : b * 64 + 64, d * LANES : (d + 1) * LANES]
            row = (d * TILES + tile) * 64
            pay_ref[row : row + 64, :] = run.astype(BF16)
        return [jnp.concatenate(s, axis=1) for s in states]

    def transposed(v):
        return jnp.transpose(v.astype(F32))

    def spread(vt):
        return jnp.where(same, jnp.concatenate([vt] * NB, axis=0), 0.0).astype(BF16)

    def scores(qi, ki):
        total = jnp.where(tri[0], dot_t(qi[0].astype(BF16), ki[0].astype(BF16)), 0.0)
        total = total + jnp.where(tri[1], dot_t(qi[1].astype(BF16), ki[1].astype(BF16)), 0.0)
        return total.astype(BF16)

    for p in range(2):
        cols = slice(p * LANES, (p + 1) * LANES)
        v = v0_ref[:, cols]
        extra = jnp.where(low, ex_ref[:, 2 * p : 2 * p + 1], ex_ref[:, 2 * p + 1 : 2 * p + 2])
        qi, ki, ke, ends = prepare(
            p, nq_ref[:, cols], (nf_ref[0, :, cols], nf_ref[1, :, cols]),
            (nh_ref[0:1, cols], nh_ref[1:2, cols]), extra,
        )
        vt = transposed(v)
        kv = jnp.where(low2, dot(spread(vt[:64]), ke), dot(spread(vt[64:]), ke))
        states = block_states(p, kv, ends)
        q_cat = jnp.concatenate([x.astype(BF16) for x in qi], axis=1)
        parts = []
        for b in range(NB):
            s = jnp.concatenate(
                [jnp.where(low2, states[b], 0.0), jnp.where(low2, 0.0, states[b])], axis=0
            )
            parts.append(dot_t(q_cat[b * BLK : (b + 1) * BLK], s.astype(BF16)))
        first = dot(scores(qi, [jnp.where(low, k, 0.0) for k in ki]), v)
        second = dot(scores(qi, [jnp.where(low, 0.0, k) for k in ki]), v)
        out_ref[p] = jnp.where(low, first, second) + jnp.concatenate(parts, axis=0)

    for p in range(2):
        v = v1_ref[:, p * LANES : (p + 1) * LANES]
        vt = transposed(v)
        inner, q_cats, head_states = [], [], []
        for i in range(2):
            h = 2 * p + i
            cols = slice(h * LANES, (h + 1) * LANES)
            qi, ki, ke, ends = prepare(
                2 + h, wq_ref[:, cols], (wf_ref[0, :, cols], wf_ref[1, :, cols]),
                (wh_ref[0:1, cols], wh_ref[1:2, cols]), ex_ref[:, 4 + h : 5 + h],
            )
            kv = dot(spread(vt[i * 64 : i * 64 + 64]), ke)
            head_states.append(block_states(2 + h, kv, ends))
            q_cats.append(jnp.concatenate([x.astype(BF16) for x in qi], axis=1))
            inner.append(dot(scores(qi, ki), v))
        parts = []
        for b in range(NB):
            s = jnp.concatenate([head_states[0][b], head_states[1][b]], axis=0).astype(BF16)
            rows = slice(b * BLK, (b + 1) * BLK)
            parts.append(
                jnp.where(low, dot_t(q_cats[0][rows], s), dot_t(q_cats[1][rows], s))
            )
        out_ref[2 + p] = jnp.where(low, inner[0], inner[1]) + jnp.concatenate(parts, axis=0)

    pad = jnp.zeros((16 - 2 * TILES, LANES), F32)
    dec = jnp.concatenate(decays + [pad], axis=0)
    high = dec.astype(BF16)
    pay_ref[STATE_ROWS : STATE_ROWS + 16, :] = high
    pay_ref[STATE_ROWS + 16 : STATE_ROWS + 32, :] = (dec - high.astype(F32)).astype(BF16)


def level_kernel(count, has_carry, last, here_ref, pieces_ref, *refs):
    here = here_ref[0]
    refs = list(refs)
    carry_s, carry_d = (refs.pop(0), refs.pop(0)) if has_carry else (None, None)
    if last:
        (in_ref,) = refs
    else:
        s_ref, d_ref, pay_ref = refs
    dec = [
        pieces_ref[k, STATE_ROWS : STATE_ROWS + 16, :].astype(F32)
        + pieces_ref[k, STATE_ROWS + 16 : STATE_ROWS + 32, :].astype(F32)
        for k in range(count)
    ]
    totals, inner = [], []
    for t in range(2 * TILES):
        rows = slice(t * 64, t * 64 + 64)
        order = list(range(count)) if t < TILES else list(reversed(range(count)))
        run = jnp.zeros((64, LANES), F32)
        run_d = jnp.ones((1, LANES), F32)
        mine, mine_d = run, run_d
        for k in order:
            mine = jnp.where(here == k, run, mine)
            mine_d = jnp.where(here == k, run_d, mine_d)
            if last and k == order[-1]:
                break
            d = dec[k][t : t + 1]
            run = run * d + pieces_ref[k, rows, :].astype(F32)
            run_d = run_d * d
        if has_carry:
            cd = carry_d[t : t + 1, :]
            mine = mine * cd + carry_s[rows, :]
            mine_d = mine_d * cd
        if last:
            in_ref[rows, :] = mine.astype(BF16)
        else:
            s_ref[rows, :] = mine
            pay_ref[rows, :] = run.astype(BF16)
            totals.append(run_d)
            inner.append(mine_d)
    if not last:
        pad = jnp.zeros((16 - 2 * TILES, LANES), F32)
        d_ref[...] = jnp.concatenate(inner + [pad], axis=0)
        total = jnp.concatenate(totals + [pad], axis=0)
        high = total.astype(BF16)
        pay_ref[STATE_ROWS : STATE_ROWS + 16, :] = high
        pay_ref[STATE_ROWS + 16 : STATE_ROWS + 32, :] = (total - high.astype(F32)).astype(BF16)


VMEM = pl.BlockSpec(memory_space=pltpu.VMEM)
SMEM = pl.BlockSpec(memory_space=pltpu.SMEM)


def level(axis, payload, carry, last):
    count = lax.axis_size(axis)
    pieces = lax.all_gather(payload, axis)
    here = lax.axis_index(axis).astype(jnp.int32).reshape(1)
    if last:
        shapes = jax.ShapeDtypeStruct((STATE_ROWS, LANES), BF16)
    else:
        shapes = (
            jax.ShapeDtypeStruct((STATE_ROWS, LANES), F32),
            jax.ShapeDtypeStruct((16, LANES), F32),
            jax.ShapeDtypeStruct((PAY_ROWS, LANES), BF16),
        )
    return pl.pallas_call(
        partial(level_kernel, count, carry is not None, last),
        out_shape=shapes,
        in_specs=[SMEM] + [VMEM] * (1 + (0 if carry is None else 2)),
        out_specs=VMEM if last else (VMEM,) * 3,
        name="level_" + axis,
    )(here, pieces, *(carry or ()))


def mix_kernel(out_ref, qr_ref, in_ref, g0_ref, g1_ref, gain_ref, mixed_ref):
    low = lax.broadcasted_iota(jnp.int32, (1, LANES), 1) < 64
    low2 = (lax.broadcasted_iota(jnp.int32, (1, 2 * LANES), 1) % LANES) < 64

    def entering(tile):
        a = in_ref[tile * 64 : tile * 64 + 64, :]
        b = in_ref[(TILES + tile) * 64 : (TILES + tile) * 64 + 64, :]
        return jnp.concatenate([a, b], axis=1)

    zero = jnp.zeros((64, 2 * LANES), BF16)
    for u in range(4):
        if u < 2:
            s = entering(u).astype(F32)
            s = jnp.concatenate([jnp.where(low2, s, 0.0), jnp.where(low2, 0.0, s)], axis=0)
            o = dot_t(qr_ref[u], s.astype(BF16))
        else:
            t = 2 + 2 * (u - 2)
            o = dot_t(qr_ref[t], jnp.concatenate([entering(t), zero], axis=0))
            o = o + dot_t(qr_ref[t + 1], jnp.concatenate([zero, entering(t + 1)], axis=0))
        o = o + out_ref[u]
        square = o * o
        first = jnp.sum(jnp.where(low, square, 0.0), axis=-1, keepdims=True)
        second = jnp.sum(jnp.where(low, 0.0, square), axis=-1, keepdims=True)
        scale = lax.rsqrt(jnp.where(low, first, second) * (1.0 / 64) + EPS)
        g_ref = g0_ref if u < 2 else g1_ref
        c = (u % 2) * LANES
        gate = silu(g_ref[:, c : c + LANES].astype(F32))
        mixed = o * scale * gain_ref[...] * gate
        mixed_ref[:, u * LANES : (u + 1) * LANES] = mixed.astype(BF16)


def route_kernel(
    experts, capacity, copies, own_ref, x_ref, w_ref, stream_ref, gain_ref, routes_ref, routes_t_ref,
    score_ref, res_ref, buf_ref, pick_ref, acc_ref,
):
    step = pl.program_id(0)
    part = dot(x_ref[0], w_ref[0])

    @pl.when(step == 0)
    def _():
        acc_ref[...] = stream_ref[...].astype(F32) + part

    @pl.when(step > 0)
    def _():
        acc_ref[...] += part

    @pl.when(step == pl.num_programs(0) - 1)
    def _():
        residual = acc_ref[...]
        res_ref[...] = residual
        mean = jnp.mean(residual * residual, axis=-1, keepdims=True)
        norm = (residual * lax.rsqrt(mean + EPS) * gain_ref[...]).astype(BF16)
        rows = residual.shape[0]
        col = [routes_ref[:, k : k + 1] for k in range(2)]
        row = [routes_t_ref[0, k : k + 1, :] for k in range(2)]
        ri = lax.broadcasted_iota(jnp.int32, (rows, rows), 0)
        ci = lax.broadcasted_iota(jnp.int32, (rows, rows), 1)
        earlier = ci < ri

        def count(hit):
            return jnp.sum(jnp.where(hit, 1.0, 0.0), axis=-1, keepdims=True).astype(jnp.int32)

        rank0 = count((col[0] == row[0]) & earlier)
        rank1 = count((col[1] == row[1]) & earlier) + count(col[1] == row[0])
        slot0 = col[0] * capacity + rank0
        slot1 = col[1] * capacity + rank1
        width = experts * copies * capacity
        j = lax.broadcasted_iota(jnp.int32, (rows, width), 1)
        code = (j // (copies * capacity)) * capacity + j % capacity
        hit0 = code == slot0
        hit1 = code == slot1
        s0, s1 = score_ref[:, 0:1], score_ref[:, 1:2]
        weight0 = 1.0 / (1.0 + jnp.exp(s1 - s0))
        weight1 = 1.0 / (1.0 + jnp.exp(s0 - s1))
        pick = jnp.where(hit0, weight0, 0.0) + jnp.where(hit1, weight1, 0.0)
        high = pick.astype(BF16)
        pick_ref[:rows, :] = high
        pick_ref[rows:, :] = (pick - high.astype(F32)).astype(BF16)
        chosen = jnp.where(hit0 | hit1, 1.0, 0.0)
        chosen = jnp.transpose(chosen).astype(BF16)
        buf_ref[...] = dot(chosen, norm).astype(BF16)


def final_kernel(pick_ref, back_ref, res_ref, o_ref):
    rows = res_ref.shape[0]
    both = dot(pick_ref[...], back_ref[...])
    o_ref[...] = (res_ref[...] + both[:rows] + both[rows:]).astype(BF16)


def local(
    stream,
    narrow_query_weight,
    wide_query_weight,
    value_rows_heads,
    output_gate_logits,
    narrow_forget_logits,
    wide_forget_logits,
    narrow_forget_headroom,
    wide_forget_headroom,
    extra_log_decay,
    per_head_norm_gain,
    mixer_output_weight,
    feedforward_norm_gain,
    expert_gate_matrix,
    expert_up_matrix,
    expert_down_matrix,
    routes,
    router_scores_chosen,
):
    extra = extra_log_decay.reshape(TOK, 8)
    payload, inner, q_run = pl.pallas_call(
        local_kernel,
        out_shape=(
            jax.ShapeDtypeStruct((PAY_ROWS, LANES), BF16),
            jax.ShapeDtypeStruct((4, TOK, LANES), F32),
            jax.ShapeDtypeStruct((TILES, TOK, 2 * LANES), BF16),
        ),
        in_specs=[VMEM] * 9,
        out_specs=(VMEM,) * 3,
        name="local_mixer",
    )(
        narrow_query_weight, wide_query_weight, narrow_forget_logits, wide_forget_logits,
        narrow_forget_headroom, wide_forget_headroom, extra,
        value_rows_heads[:, 0], value_rows_heads[:, 1],
    )
    s, d, payload = level("sp_2", payload, None, False)
    s, d, payload = level("sp_1", payload, (s, d), False)
    entering = level("sp_0", payload, (s, d), True)
    gain2 = jnp.concatenate([per_head_norm_gain, per_head_norm_gain]).reshape(1, LANES)
    mixed = pl.pallas_call(
        mix_kernel,
        out_shape=jax.ShapeDtypeStruct((TOK, 4 * LANES), BF16),
        in_specs=[VMEM] * 6,
        out_specs=VMEM,
        name="mix",
    )(inner, q_run, entering, output_gate_logits[:, 0], output_gate_logits[:, 1], gain2)

    tp = lax.axis_size("tp")
    rows = TOK // tp
    width = stream.shape[1]
    experts = lax.axis_size(SP)
    capacity = max(2, 2 * routes.shape[1] * rows // experts)
    slots = experts * tp * capacity
    own = lax.axis_index("tp").astype(jnp.int32).reshape(1)
    arrived = lax.all_to_all(mixed.reshape(tp, rows, 4 * LANES), "tp", 0, 0, tiled=True)
    routes_t = routes.reshape(tp, rows, 2).transpose(0, 2, 1)
    residual, buffers, pick = pl.pallas_call(
        partial(route_kernel, experts, capacity, tp),
        grid_spec=pltpu.PrefetchScalarGridSpec(
            num_scalar_prefetch=1,
            grid=(2 * tp,),
            in_specs=[
                pl.BlockSpec((1, rows, 2 * LANES), lambda i, o: (i // 2, 0, i % 2)),
                pl.BlockSpec((1, 2 * LANES, width), lambda i, o: (i % 2, i // 2, 0)),
                pl.BlockSpec((rows, width), lambda i, o: (o[0], 0)),
                pl.BlockSpec((1, width), lambda i, o: (0, 0)),
                pl.BlockSpec((rows, 2), lambda i, o: (o[0], 0)),
                pl.BlockSpec((1, 2, rows), lambda i, o: (o[0], 0, 0)),
                pl.BlockSpec((rows, 2), lambda i, o: (o[0], 0)),
            ],
            out_specs=[
                pl.BlockSpec((rows, width), lambda i, o: (0, 0)),
                pl.BlockSpec((slots, width), lambda i, o: (0, 0)),
                pl.BlockSpec((2 * rows, slots), lambda i, o: (0, 0)),
            ],
            scratch_shapes=[pltpu.VMEM((rows, width), F32)],
        ),
        out_shape=(
            jax.ShapeDtypeStruct((rows, width), F32),
            jax.ShapeDtypeStruct((slots, width), BF16),
            jax.ShapeDtypeStruct((2 * rows, slots), BF16),
        ),
        name="project_and_route",
    )(
        own, arrived, mixer_output_weight, stream, feedforward_norm_gain.reshape(1, width), routes,
        routes_t, router_scores_chosen,
    )
    tokens = lax.all_to_all(buffers, SP_TP, 0, 0, tiled=True)
    gate = jnp.dot(tokens, expert_gate_matrix[0], preferred_element_type=F32)
    up = jnp.dot(tokens, expert_up_matrix[0], preferred_element_type=F32)
    hidden = (jax.nn.silu(gate) * up).astype(BF16)
    part = jnp.dot(hidden, expert_down_matrix[0], preferred_element_type=F32).astype(BF16)
    back = lax.all_to_all(part, SP_TP, 0, 0, tiled=True)
    col = width // 4
    return pl.pallas_call(
        final_kernel,
        grid=(4,),
        in_specs=[
            pl.BlockSpec((2 * rows, slots), lambda i: (0, 0)),
            pl.BlockSpec((slots, col), lambda i: (0, i)),
            pl.BlockSpec((rows, col), lambda i: (0, i)),
        ],
        out_specs=pl.BlockSpec((rows, col), lambda i: (0, i)),
        out_shape=jax.ShapeDtypeStruct((rows, width), BF16),
        name="combine",
    )(pick, back, residual)


def solution(mesh):
    torus = Mesh(mesh.devices.reshape(4, 4, 2, mesh.shape["tp"]), ("sp_0", "sp_1", "sp_2", "tp"))
    return jax.shard_map(
        local,
        mesh=torus,
        in_specs=(
            P(SP, None),
            P(SP, "tp"),
            P(SP, "tp"),
            P(SP, None, "tp"),
            P(SP, None, "tp"),
            P(None, SP, "tp"),
            P(None, SP, "tp"),
            P(None, "tp"),
            P(None, "tp"),
            P(SP, None, "tp"),
            P(),
            P(),
            P(),
            P(SP, None, "tp"),
            P(SP, None, "tp"),
            P(SP, "tp", None),
            P(SP, None),
            P(SP, None),
        ),
        out_specs=P(SP_TP, None),
        check_vma=False,
    )
```

time: 496 us -> 221 us (0.45); the launches traced: 487 us -> 220 us
  blocking collectives: 292 us -> 157 us
  matrix products: 70.7 us -> 14.6 us
  local copies, waits for them, and re-layouts: 53.8 us -> 8.93 us
  other arithmetic: 34.8 us -> 1.31 us
  Pallas kernels: 0 us -> 31.6 us
  waiting for transfers between devices: 24.8 us -> 3.27 us
  starting transfers between devices: 9.12 us -> 4.02 us
    all_gather x24 -> x3, blocking collectives: 177 us -> 35.6 us  [level(): pieces = lax.all_gather(payload, axis)]
    dot_general x49 -> x3, matrix products: 70.7 us -> 14.6 us  [the longest x1 5.36 us: local(): gate = jnp.dot(tokens, expert_gate_matrix[0], preferred_element_type=F32)]
    pallas_call x0 -> x7, Pallas kernels: none -> 31.6 us  [the longest x1 11.1 us: local(): pl.pallas_call(partial(route_kernel, experts, capacity, tp), grid_spec=pl...]
    all_to_all x2 -> x1, waiting for transfers between devices: 24.8 us -> 3.27 us  [local(): lax.all_to_all(mixed.reshape(tp, rows, 4 * LANES), 'tp', 0, 0, tiled=True)]
    rev x14 -> x0, local copies, waits for them, and re-layouts: 13.8 us -> none  [the longest x3 5.26 us: local(): jnp.flip(group[0], 0)]
    convert_element_type x35 -> x0, other arithmetic: 11.6 us -> none  [the longest x12 5.35 us: entering_2(): part[k].astype(own.dtype)]
    another operation x16 -> x0, local copies, waits for them, and re-layouts: 11.5 us -> none  [the longest x11 8.71 us: to_blocks(): source.reshape(token_rows // length, length, total_head_count, breadth)]
    reduce_sum x8 -> x0, other arithmetic: 7.6 us -> none  [the longest x1 4.25 us: sent_and_summed(): return arrived.astype(jnp.float32).sum(axis=0)]
  transfers between devices with their start and end apart: 2 -> 1, of which waited for: 2 -> 1; matrix products, arithmetic and copies ran while one was open for 0% -> 1% of each run, Pallas kernels for 0% -> 0%
where the time goes in v1:
time: 221 us; the launch traced here: 220 us
  blocking collectives  157 us (71%)
  Pallas kernels  31.6 us (14%)
  matrix products  14.6 us (7%)
  local copies, waits for them, and re-layouts  8.93 us (4%)
  starting transfers between devices  4.02 us (2%)
  waiting for transfers between devices  3.27 us (1%)
    all_to_all x1, blocking collectives, local(): tokens = lax.all_to_all(buffers, SP_TP, 0, 0, tiled=True)  63.5 us
    all_to_all x1, blocking collectives, local(): back = lax.all_to_all(part, SP_TP, 0, 0, tiled=True)  57.5 us
    all_gather x3, blocking collectives, level(): pieces = lax.all_gather(payload, axis)  35.6 us
    pallas_call x1, Pallas kernels, local(): pl.pallas_call(partial(route_kernel, experts, capacity, tp), grid_spec=pl...  11.1 us
    pallas_call x1, Pallas kernels, local(): pl.pallas_call(local_kernel, out_shape=(jax.ShapeDtypeStruct((PAY_ROWS, L...  7.04 us
    pallas_call x3, Pallas kernels, level(): pl.pallas_call(partial(level_kernel, count, carry is not None, last), out...  6.36 us
    dot_general x1, matrix products, local(): gate = jnp.dot(tokens, expert_gate_matrix[0], preferred_element_type=F32)  5.36 us
    dot_general x1, matrix products, local(): jnp.dot(hidden, expert_down_matrix[0], preferred_element_type=F32)  4.73 us
  transfers between devices with their start and end apart: 1, of which 1 were waited for; matrix products, arithmetic and copies ran while one was open for 1% of the time, Pallas kernels for 0%

profile of v1, /device:TPU:1, one launch (start us, length us, event | category | flops | bytes accessed | tf_op | source)
XLA Modules:
  0.0 220.4 jit_solution(3509395555587068508)
XLA Ops:
  0.0 1.3 maximum_bitcast_fusion.gain_ref
  2.0 0.8 copy.28.ex_ref
  2.8 1.5 fusion.15
  4.3 1.5 fusion.14
  6.5 7.0 %local_mixer.1 = (bf16[800,128]{1,0:T(8,128)(2,1)}, f32[4,256,128]{2,1,0:T(8,128)}, bf16[6,256,256]{2,1,0:T(8,128)(2,1)}) custom-call(bf16[256,256]{1,0:T(8,128)(2,1)} %nq_ref.1, bf16[256,512]{1,0:T(8,128)(2,1)} %wq_ref.1, bf16[2,256,256]{2,1,0:T(8,128)(2,1)} %nf_ref.1, bf16[2,256,512]{2,1,0:T(8,128)(2,1)} %wf_ref.1, f32[2,256]{1,0:T(2,128)} %nh_ref.1, ...), custom_call_target="tpu_custom_call" | custom-call | tf_op jit(solution)/shard_map/local_mixer/pallas_call | solution.py:339
  13.6 4.9 %all-gather = bf16[1600,128]{1,0:T(8,128)(2,1)} all-gather(bf16[800,128]{1,0:T(8,128)(2,1)} %get-tuple-element.19), channel_id=2, replica_groups=mesh['sp_0'=4,'sp_1'=4,'sp_2'=2,'tp'=4] {'sp_2'}, dimensions={0}, use_global_device_ids=true | all-gather | bytes 614400 | tf_op jit(solution)/shard_map/all_gather | solution.py:210
  18.5 1.9 level_sp_2.1
  20.4 15.3 %all-gather.1 = bf16[3200,128]{1,0:T(8,128)(2,1)} all-gather(bf16[800,128]{1,0:T(8,128)(2,1)} %get-tuple-element.20), channel_id=3, replica_groups=mesh['sp_0'=4,'sp_1'=4,'sp_2'=2,'tp'=4] {'sp_1'}, dimensions={0}, use_global_device_ids=true | all-gather | bytes 1024000 | tf_op jit(solution)/shard_map/all_gather | solution.py:210
  35.7 2.3 %level_sp_1.1 = (f32[768,128]{1,0:T(8,128)}, f32[16,128]{1,0:T(8,128)}, bf16[800,128]{1,0:T(8,128)(2,1)}) custom-call(s32[1]{0:T(128)} %bitcast.4.here_ref, bf16[4,800,128]{2,1,0:T(8,128)(2,1)} %bitcast.54, f32[768,128]{1,0:T(8,128)} %get-tuple-element.21.refs_0_, f32[16,128]{1,0:T(8,128)} %get-tuple-element.22.refs_1_), custom_call_target="tpu_custom_call" | custom-call | tf_op jit(solution)/shard_map/level_sp_1/pallas_call | solution.py:220
  38.0 15.4 %all-gather.2 = bf16[3200,128]{1,0:T(8,128)(2,1)} all-gather(bf16[800,128]{1,0:T(8,128)(2,1)} %get-tuple-element.23), channel_id=4, replica_groups=mesh['sp_0'=4,'sp_1'=4,'sp_2'=2,'tp'=4] {'sp_0'}, dimensions={0}, use_global_device_ids=true | all-gather | bytes 1024000 | tf_op jit(solution)/shard_map/all_gather | solution.py:210
  53.4 0.7 copy_bitcast_fusion
  54.2 2.1 level_sp_0.1.in_ref
  56.3 2.6 %mix.1 = bf16[256,512]{1,0:T(8,128)(2,1)} custom-call(f32[4,256,128]{2,1,0:T(8,128)} %get-tuple-element.17.out_ref, bf16[6,256,256]{2,1,0:T(8,128)(2,1)} %get-tuple-element.18.qr_ref, bf16[768,128]{1,0:T(8,128)(2,1)} %level_sp_0.1.in_ref, bf16[256,256]{1,0:T(8,128)(2,1)} %get-tuple-element.36.g0_ref, bf16[256,256]{1,0:T(8,128)(2,1)} %get-tuple-element.35.g1_ref, ...), custom_call_target="tpu_custom_call" | custom-call | tf_op jit(solution)/shard_map/mix/pallas_call | solution.py:358
  59.0 4.0 %all-to-all-start = ((bf16[4,64,512]{2,1,0:T(8,128)(2,1)}), bf16[4,64,512]{2,1,0:T(8,128)(2,1)S(1)}, u32[]{:S(2)}, u32[]{:S(2)}) async-start(bf16[4,64,512]{2,1,0:T(8,128)(2,1)} %bitcast.56), calls=%async_computation | async-start | bytes 524288 | tf_op jit(solution)/shard_map/all_to_all | solution.py:373
  63.1 0.8 copy.32.routes_ref
  64.5 0.8 copy.33.score_ref
  65.2 3.3 %all-to-all-done.x_ref = bf16[4,64,512]{2,1,0:T(8,128)(2,1)S(1)} async-done(((bf16[4,64,512]{2,1,0:T(8,128)(2,1)}), bf16[4,64,512]{2,1,0:T(8,128)(2,1)S(1)}, u32[]{:S(2)}, u32[]{:S(2)}) %all-to-all-start) | async-done | bytes 262176 | tf_op jit(solution)/shard_map/all_to_all | solution.py:373
  69.2 11.1 %project_and_route.1 = (f32[64,2048]{1,0:T(8,128)}, bf16[1024,2048]{1,0:T(8,128)(2,1)}, bf16[128,1024]{1,0:T(8,128)(2,1)}) custom-call(s32[1]{0:T(128)} %bitcast.own_ref, bf16[4,64,512]{2,1,0:T(8,128)(2,1)} %copy-done, bf16[2,1024,2048]{2,1,0:T(8,128)(2,1)} %w_ref.1, bf16[256,2048]{1,0:T(8,128)(2,1)} %stream_ref.1, f32[1,2048]{1,0:T(1,128)} %bitcast.58, ...), custom_call_target="tpu_custom_call" | custom-call | tf_op jit(solution)/shard_map/project_and_route/pallas_call | solution.py:375
  80.3 63.5 %all_to_all.28 = bf16[128,8,2048]{2,1,0:T(8,128)(2,1)S(1)} all-to-all(bf16[128,8,2048]{2,1,0:T(8,128)(2,1)} %bitcast.52), channel_id=1, replica_groups=mesh['sp_0'=4,'sp_1'=4,'sp_2'=2,'tp'=4] {'sp_0','sp_1','sp_2','tp'}, dimensions={0} | all-to-all | bytes 8388608 | tf_op jit(solution)/shard_map/all_to_all | solution.py:406
  143.8 4.5 %fusion.2 = f32[1024,1024]{1,0:T(8,128)S(1)} fusion(bf16[1,2048,1024]{2,1,0:T(8,128)(2,1)S(1)} %copy-done.3, bf16[128,8,2048]{2,1,0:T(8,128)(2,1)S(1)} %all_to_all.28), kind=kOutput, calls=%fused_computation.2 | convolution fusion | flops 4294967296 | bytes 12582912 | tf_op jit(solution)/shard_map/dot_general | solution.py:408
  148.4 5.4 %multiply_convert_fusion = bf16[1024,1024]{1,0:T(8,128)(2,1)S(1)} fusion(f32[1024,1024]{1,0:T(8,128)S(1)} %fusion.2, bf16[1,2048,1024]{2,1,0:T(8,128)(2,1)S(1)} %copy-done.4, bf16[128,8,2048]{2,1,0:T(8,128)(2,1)S(1)} %all_to_all.28), kind=kOutput, calls=%fused_computation.9 | convolution fusion | flops 4301258752 | bytes 14680064 | tf_op jit(solution)/shard_map/dot_general | solution.py:407
  153.7 4.7 %convert_bitcast_fusion = bf16[128,8,2048]{2,1,0:T(8,128)(2,1)S(1)} fusion(bf16[1024,1024]{1,0:T(8,128)(2,1)S(1)} %multiply_convert_fusion, bf16[1,1024,2048]{2,1,0:T(8,128)(2,1)S(1)} %copy-done.5), kind=kOutput, calls=%fused_computation.8 | convolution fusion | flops 4297064448 | bytes 10485760 | tf_op jit(solution)/shard_map/dot_general | solution.py:410
  158.5 57.5 %all_to_all.29 = bf16[128,8,2048]{2,1,0:T(8,128)(2,1)} all-to-all(bf16[128,8,2048]{2,1,0:T(8,128)(2,1)S(1)} %convert_bitcast_fusion), channel_id=1, replica_groups=mesh['sp_0'=4,'sp_1'=4,'sp_2'=2,'tp'=4] {'sp_0','sp_1','sp_2','tp'}, dimensions={0} | all-to-all | bytes 8388608 | tf_op jit(solution)/shard_map/all_to_all | solution.py:411
  215.9 4.5 %combine.1 = bf16[64,2048]{1,0:T(8,128)(2,1)} custom-call(bf16[128,1024]{1,0:T(8,128)(2,1)} %get-tuple-element.26.pick_ref, bf16[1024,2048]{1,0:T(8,128)(2,1)} %bitcast.51, f32[64,2048]{1,0:T(8,128)} %get-tuple-element.28.res_ref), custom_call_target="tpu_custom_call" | custom-call | tf_op jit(solution)/shard_map/combine/pallas_call | solution.py:413
  (16 shorter events, 2.8 us)
Async XLA Ops:
  18.5 44.5 %copy-start.1 = (s32[256,2]{0,1:T(2,128)S(1)}, s32[256,2]{0,1:T(2,128)}, u32[]{:S(2)}) copy-start(s32[256,2]{0,1:T(2,128)} %param.34) | copy-start | bytes 6148
  20.4 44.0 %copy-start.2 = (f32[256,2]{0,1:T(2,128)S(1)}, f32[256,2]{0,1:T(2,128)}, u32[]{:S(2)}) copy-start(f32[256,2]{0,1:T(2,128)} %param.35) | copy-start | bytes 6148
  59.0 9.5 %all-to-all-start = ((bf16[4,64,512]{2,1,0:T(8,128)(2,1)}), bf16[4,64,512]{2,1,0:T(8,128)(2,1)S(1)}, u32[]{:S(2)}, u32[]{:S(2)}) async-start(bf16[4,64,512]{2,1,0:T(8,128)(2,1)} %bitcast.56), calls=%async_computation | async-start | bytes 524288 | tf_op jit(solution)/shard_map/all_to_all | solution.py:373
  68.5 0.7 copy-start
  80.3 63.5 %copy-start.3 = (bf16[1,2048,1024]{2,1,0:T(8,128)(2,1)S(1)}, bf16[1,2048,1024]{2,1,0:T(8,128)(2,1)}, u32[]{:S(2)}) copy-start(bf16[1,2048,1024]{2,1,0:T(8,128)(2,1)} %param.32) | copy-start | bytes 12582916
  143.8 4.5 %copy-start.4 = (bf16[1,2048,1024]{2,1,0:T(8,128)(2,1)S(1)}, bf16[1,2048,1024]{2,1,0:T(8,128)(2,1)}, u32[]{:S(2)}) copy-start(bf16[1,2048,1024]{2,1,0:T(8,128)(2,1)} %param.31) | copy-start | bytes 12582916
  148.3 5.4 %copy-start.5 = (bf16[1,1024,2048]{2,1,0:T(8,128)(2,1)S(1)}, bf16[1,1024,2048]{2,1,0:T(8,128)(2,1)}, u32[]{:S(2)}) copy-start(bf16[1,1024,2048]{2,1,0:T(8,128)(2,1)} %param.33) | copy-start | bytes 12582916

commit v2 on v1

v2 whole, which is shorter than its diff:
```python
from functools import partial

import jax
import jax.numpy as jnp
from jax import lax
from jax.experimental import pallas as pl
from jax.experimental.pallas import tpu as pltpu
from jax.sharding import Mesh
from jax.sharding import PartitionSpec as P

SP = ("sp_0", "sp_1", "sp_2")
SP_TP = ("sp_0", "sp_1", "sp_2", "tp")

EPS = 1e-06
F32 = jnp.float32
BF16 = jnp.bfloat16

TOK = 256
BLK = 64
NB = TOK // BLK
LANES = 128
TILES = 6
STATE_ROWS = TILES * 64
PAY_ROWS = STATE_ROWS + 16


def dot(a, b):
    return lax.dot_general(a, b, (((1,), (0,)), ((), ())), preferred_element_type=F32)


def dot_t(a, b):
    return lax.dot_general(a, b, (((1,), (1,)), ((), ())), preferred_element_type=F32)


def silu(x):
    return x / (1.0 + jnp.exp(-x))


def local_kernel(
    nf_hbm, nh_hbm, ex_hbm, nq_hbm, v_hbm, wf_hbm, wh_hbm, wq_hbm, w_hbm, pay_ref, out_ref, qr_ref,
    w_ref, nf_ref, nh_ref, ex_ref, nq_ref, v_ref, wf_ref, wh_ref, wq_ref, sems,
):
    sources = (nf_hbm, nh_hbm, ex_hbm, nq_hbm, v_hbm, wf_hbm, wh_hbm, wq_hbm, w_hbm)
    targets = (nf_ref, nh_ref, ex_ref, nq_ref, v_ref, wf_ref, wh_ref, wq_ref, w_ref)
    copies = [
        pltpu.make_async_copy(a, b, sems.at[i]) for i, (a, b) in enumerate(zip(sources, targets))
    ]
    for copy in copies:
        copy.start()
    for copy in copies[:-1]:
        copy.wait()
    ex = jnp.transpose(jnp.concatenate([ex_ref[0], ex_ref[1]], axis=0))
    ri = lax.broadcasted_iota(jnp.int32, (TOK, TOK), 0)
    ci = lax.broadcasted_iota(jnp.int32, (TOK, TOK), 1)
    same = (ri // BLK) == (ci // BLK)
    tri = (same & (ci <= ri), same & (ci >= ri))
    ones = tuple(jnp.where(t, 1.0, 0.0).astype(BF16) for t in tri)
    lane = lax.broadcasted_iota(jnp.int32, (1, LANES), 1)
    low = lane < 64
    low2 = (lax.broadcasted_iota(jnp.int32, (1, 2 * LANES), 1) % LANES) < 64
    decays = [None] * (2 * TILES)

    def prepare(tile, q_raw, f_raw, rooms, extra):
        q = silu(q_raw.astype(F32)).reshape(NB, BLK, LANES)
        qi, ki, ke, qr, ends = [], [], [], [], []
        for d in range(2):
            opening = rooms[d] / (1.0 + jnp.exp(f_raw[d].astype(F32)))
            ld = jnp.log(1.0 - opening) + extra
            hi = ld.astype(BF16)
            lo = (ld - hi.astype(F32)).astype(BF16)
            both = dot(ones[d], jnp.concatenate([hi, lo], axis=1))
            inside = (both[:, :LANES] + both[:, LANES:]).reshape(NB, BLK, LANES)
            opening = opening.reshape(NB, BLK, LANES)
            edge = BLK - 1 if d == 0 else 0
            end = [inside[b, edge : edge + 1, :] for b in range(NB)]
            start = [None] * NB
            run = jnp.zeros((1, LANES), F32)
            for b in range(NB) if d == 0 else reversed(range(NB)):
                start[b] = run
                run = run + end[b]
            decays[d * TILES + tile] = jnp.exp(run)
            start4 = jnp.stack(start, axis=0)
            end4 = jnp.stack(end, axis=0)
            qi.append((q * jnp.exp(inside)).reshape(TOK, LANES))
            qr.append((q * jnp.exp(inside + start4)).reshape(TOK, LANES).astype(BF16))
            ki.append((opening * jnp.exp(-inside)).reshape(TOK, LANES))
            ke.append((opening * jnp.exp(end4 - inside)).reshape(TOK, LANES).astype(BF16))
            ends.append([jnp.exp(e) for e in end])
        qr_ref[tile] = jnp.concatenate(qr, axis=1)
        return qi, ki, jnp.concatenate(ke, axis=1), ends

    def block_states(tile, kv, ends):
        states = [[None, None] for _ in range(NB)]
        for d in range(2):
            run = jnp.zeros((64, LANES), F32)
            for b in range(NB) if d == 0 else reversed(range(NB)):
                states[b][d] = run
                run = run * ends[d][b] + kv[b * 64 : b * 64 + 64, d * LANES : (d + 1) * LANES]
            pay_ref[d, tile * 64 : tile * 64 + 64, :] = run.astype(BF16)
        return [jnp.concatenate(s, axis=1) for s in states]

    def transposed(v):
        return jnp.transpose(v.astype(F32))

    def spread(vt):
        return jnp.where(same, jnp.concatenate([vt] * NB, axis=0), 0.0).astype(BF16)

    def scores(qi, ki):
        total = jnp.where(tri[0], dot_t(qi[0].astype(BF16), ki[0].astype(BF16)), 0.0)
        total = total + jnp.where(tri[1], dot_t(qi[1].astype(BF16), ki[1].astype(BF16)), 0.0)
        return total.astype(BF16)

    for p in range(2):
        cols = slice(p * LANES, (p + 1) * LANES)
        v = v_ref[:, 0, cols]
        extra = jnp.where(low, ex[:, 2 * p : 2 * p + 1], ex[:, 2 * p + 1 : 2 * p + 2])
        qi, ki, ke, ends = prepare(
            p, nq_ref[:, cols], (nf_ref[0, :, cols], nf_ref[1, :, cols]),
            (nh_ref[0:1, cols], nh_ref[1:2, cols]), extra,
        )
        vt = transposed(v)
        kv = jnp.where(low2, dot(spread(vt[:64]), ke), dot(spread(vt[64:]), ke))
        states = block_states(p, kv, ends)
        q_cat = jnp.concatenate([x.astype(BF16) for x in qi], axis=1)
        parts = []
        for b in range(NB):
            s = jnp.concatenate(
                [jnp.where(low2, states[b], 0.0), jnp.where(low2, 0.0, states[b])], axis=0
            )
            parts.append(dot_t(q_cat[b * BLK : (b + 1) * BLK], s.astype(BF16)))
        first = dot(scores(qi, [jnp.where(low, k, 0.0) for k in ki]), v)
        second = dot(scores(qi, [jnp.where(low, 0.0, k) for k in ki]), v)
        out_ref[p] = jnp.where(low, first, second) + jnp.concatenate(parts, axis=0)

    for p in range(2):
        v = v_ref[:, 1, p * LANES : (p + 1) * LANES]
        vt = transposed(v)
        inner, q_cats, head_states = [], [], []
        for i in range(2):
            h = 2 * p + i
            cols = slice(h * LANES, (h + 1) * LANES)
            qi, ki, ke, ends = prepare(
                2 + h, wq_ref[:, cols], (wf_ref[0, :, cols], wf_ref[1, :, cols]),
                (wh_ref[0:1, cols], wh_ref[1:2, cols]), ex[:, 4 + h : 5 + h],
            )
            kv = dot(spread(vt[i * 64 : i * 64 + 64]), ke)
            head_states.append(block_states(2 + h, kv, ends))
            q_cats.append(jnp.concatenate([x.astype(BF16) for x in qi], axis=1))
            inner.append(dot(scores(qi, ki), v))
        parts = []
        for b in range(NB):
            s = jnp.concatenate([head_states[0][b], head_states[1][b]], axis=0).astype(BF16)
            rows = slice(b * BLK, (b + 1) * BLK)
            parts.append(
                jnp.where(low, dot_t(q_cats[0][rows], s), dot_t(q_cats[1][rows], s))
            )
        out_ref[2 + p] = jnp.where(low, inner[0], inner[1]) + jnp.concatenate(parts, axis=0)

    for d in range(2):
        pay_ref[d, STATE_ROWS:, :] = packed(decays[d * TILES : (d + 1) * TILES])
    copies[-1].wait()


def packed(rows):
    dec = jnp.concatenate(rows + [jnp.zeros((8 - TILES, LANES), F32)], axis=0)
    high = dec.astype(BF16).astype(F32)
    return jnp.concatenate([high, dec - high], axis=0).astype(BF16)


def unpacked(rows):
    rows = rows.astype(F32)
    return rows[:8] + rows[8:]


def pair_kernel(pieces_ref, pay_ref):
    core = lax.axis_index("sp_2")
    first, second = pieces_ref[core, core], pieces_ref[1 - core, core]
    d0, d1 = unpacked(first[STATE_ROWS:]), unpacked(second[STATE_ROWS:])
    for t in range(TILES):
        rows = slice(t * 64, t * 64 + 64)
        total = first[rows].astype(F32) * d1[t : t + 1] + second[rows].astype(F32)
        pay_ref[rows, :] = total.astype(BF16)
    both = d0 * d1
    pay_ref[STATE_ROWS:, :] = packed([both[:TILES]])


def level_kernel(count, axis, last, *refs):
    pieces, refs = refs[:count], refs[count:]
    backward = lax.axis_index("sp_2") == 1
    here = lax.axis_index(axis)
    if last:
        carry_s, carry_d, in_ref = refs
    else:
        s_ref, d_ref, pay_ref = refs
    far = jnp.where(backward, count - 1 - here, here)
    dec = [unpacked(p[STATE_ROWS:, :]) for p in pieces]

    def chosen(values, k):
        return jnp.where(backward, values[(count - k) % count], values[k])

    steps = [chosen(dec, k) for k in range(count)]
    mine_d = jnp.ones((8, LANES), F32)
    for k in range(1, count):
        mine_d = mine_d * jnp.where(far >= k, steps[k], 1.0)
    total_d = steps[0]
    for k in range(1, count):
        total_d = total_d * steps[k]
    for t in range(TILES):
        rows = slice(t * 64, t * 64 + 64)
        states = [p[rows, :].astype(F32) for p in pieces]
        ordered = [chosen(states, k) for k in range(count)]
        row = slice(t, t + 1)
        mine = jnp.zeros((64, LANES), F32)
        for k in range(count - 1, 0, -1):
            mine = jnp.where(far >= k, mine * steps[k][row] + ordered[k], mine)
        if last:
            in_ref[rows, :] = (mine * carry_d[row, :] + carry_s[rows, :]).astype(BF16)
            continue
        run = mine * steps[0][row] + ordered[0]
        for k in range(count - 1, 0, -1):
            run = jnp.where(far < k, run * steps[k][row] + ordered[k], run)
        s_ref[rows, :] = mine
        pay_ref[rows, :] = run.astype(BF16)
    if not last:
        d_ref[...] = mine_d
        pay_ref[STATE_ROWS:, :] = packed([total_d[:TILES]])


def from_each(x, axis, tiles=None):
    count = lax.axis_size(axis)
    return [
        lax.ppermute(x if tiles is None else tiles[j], axis, [(i, (i + j) % count) for i in range(count)])
        for j in range(1, count)
    ]


VMEM = pl.BlockSpec(memory_space=pltpu.VMEM)
HBM = pl.BlockSpec(memory_space=pltpu.HBM)


def in_hbm(x):
    return pltpu.with_memory_space_constraint(x, pltpu.HBM)


def small_call(kernel, name, shapes, *arrays, scratch=()):
    return pl.pallas_call(
        kernel,
        out_shape=shapes,
        in_specs=[VMEM] * len(arrays),
        out_specs=jax.tree.map(lambda _: VMEM, shapes),
        scratch_shapes=scratch,
        compiler_params=pltpu.CompilerParams(vmem_limit_bytes=8 * 2**20),
        name=name,
    )(*arrays)


def entering_states(payload):
    states = jax.ShapeDtypeStruct((STATE_ROWS, LANES), F32)
    decays = jax.ShapeDtypeStruct((8, LANES), F32)
    half = jax.ShapeDtypeStruct((PAY_ROWS, LANES), BF16)
    pieces = lax.all_gather(payload, "sp_2")
    chip = small_call(pair_kernel, "pair", half, pieces)
    s, d, row = small_call(
        partial(level_kernel, lax.axis_size("sp_1"), "sp_1", False), "level_1", (states, decays, half),
        chip, *from_each(chip, "sp_1"),
    )
    entering = small_call(
        partial(level_kernel, lax.axis_size("sp_0"), "sp_0", True), "level_0",
        jax.ShapeDtypeStruct((STATE_ROWS, LANES), BF16), row, *from_each(row, "sp_0"), s, d,
    )
    return lax.all_gather(entering, "sp_2"), pieces


def mix_kernel(out_ref, qr_ref, in_ref, pieces_ref, gate_ref, gain_ref, *refs):
    *tile_refs, mixed_ref = refs
    low = lax.broadcasted_iota(jnp.int32, (1, LANES), 1) < 64
    low2 = (lax.broadcasted_iota(jnp.int32, (1, 2 * LANES), 1) % LANES) < 64

    core = lax.axis_index("sp_2")
    gain = jnp.concatenate([gain_ref[...], gain_ref[...]], axis=1)
    dec = [unpacked(pieces_ref[d, d, STATE_ROWS:, :]) for d in range(2)]

    def entering(tile):
        rows = slice(tile * 64, tile * 64 + 64)
        parts = []
        for d in range(2):
            chip = in_ref[d, rows, :].astype(F32)
            past = chip * dec[d][tile : tile + 1] + pieces_ref[d, d, rows, :].astype(F32)
            parts.append(jnp.where(core == d, chip, past))
        return jnp.concatenate(parts, axis=1)

    zero = jnp.zeros((64, 2 * LANES), F32)
    for u in range(4):
        if u < 2:
            s = entering(u)
            s = jnp.concatenate([jnp.where(low2, s, 0.0), jnp.where(low2, 0.0, s)], axis=0)
            o = dot_t(qr_ref[u], s.astype(BF16))
        else:
            t = 2 + 2 * (u - 2)
            o = dot_t(qr_ref[t], jnp.concatenate([entering(t), zero], axis=0).astype(BF16))
            o = o + dot_t(qr_ref[t + 1], jnp.concatenate([zero, entering(t + 1)], axis=0).astype(BF16))
        o = o + out_ref[u]
        square = o * o
        first = jnp.sum(jnp.where(low, square, 0.0), axis=-1, keepdims=True)
        second = jnp.sum(jnp.where(low, 0.0, square), axis=-1, keepdims=True)
        scale = lax.rsqrt(jnp.where(low, first, second) * (1.0 / 64) + EPS)
        c = (u % 2) * LANES
        gate = silu(gate_ref[:, u // 2, c : c + LANES].astype(F32))
        mixed = o * scale * gain * gate
        mixed_ref[:, u * LANES : (u + 1) * LANES] = mixed.astype(BF16)
    count, rows = len(tile_refs), tile_refs[0].shape[0]
    for j, tile_ref in enumerate(tile_refs):
        place = lax.rem(lax.axis_index("tp") + j, count)
        tile_ref[...] = mixed_ref[pl.ds(place * rows, rows), :]


def earlier_in_block(size, rows, axis):
    ri = lax.broadcasted_iota(jnp.int32, (size, size), 0)
    ci = lax.broadcasted_iota(jnp.int32, (size, size), 1)
    first, second = (ri, ci) if axis == 0 else (ci, ri)
    same = (ri // rows) == (ci // rows)
    return same, same & (first < second)


def slots_of(col, row, capacity, rows, axis):
    same, earlier = earlier_in_block(col[0].shape[0], rows, axis)
    own = row if axis == 0 else col
    other = col if axis == 0 else row

    def count(hit):
        return jnp.sum(jnp.where(hit, 1.0, 0.0), axis=axis, keepdims=True).astype(jnp.int32)

    rank0 = count((own[0] == other[0]) & earlier)
    rank1 = count((own[1] == other[1]) & earlier) + count((own[1] == other[0]) & same)
    return own[0] * capacity + rank0, own[1] * capacity + rank1


def route_kernel(
    experts, capacity, copies, x0_ref, x1_ref, x2_ref, x3_ref, w_ref, stream_ref, gain_ref,
    routes_ref, score_ref, res_ref, buf_ref, pick_ref, table_ref,
):
    rows, width = res_ref.shape
    here = lax.axis_index("tp")
    own = pl.ds(here * rows, rows)
    residual = stream_ref[own, :].astype(F32)
    span = 2 * LANES
    for j, x_ref in enumerate((x0_ref, x1_ref, x2_ref, x3_ref)):
        source = lax.rem(here + copies - j, copies)
        for g in range(2):
            part = x_ref[:, g * span : (g + 1) * span]
            residual = residual + dot(part, w_ref[g, pl.ds(source * span, span), :])
    res_ref[...] = residual
    mean = jnp.mean(residual * residual, axis=-1, keepdims=True)
    norm = (residual * lax.rsqrt(mean + EPS) * gain_ref[...]).astype(BF16)
    table = jnp.concatenate(
        [routes_ref[...].astype(F32), score_ref[...], jnp.zeros((4, routes_ref.shape[1]), F32)], axis=0
    )
    table_ref[...] = jnp.transpose(table)
    table = table_ref[own, :]
    table_t = jnp.transpose(table)
    col = [table[:, k : k + 1].astype(jnp.int32) for k in range(2)]
    row = [table_t[k : k + 1, :].astype(jnp.int32) for k in range(2)]
    slots = slots_of(col, row, capacity, rows, 1)
    s0, s1 = table[:, 2:3], table[:, 3:4]
    weights = (1.0 / (1.0 + jnp.exp(s1 - s0)), 1.0 / (1.0 + jnp.exp(s0 - s1)))
    j = lax.broadcasted_iota(jnp.int32, (rows, experts * copies * capacity), 1)
    code = (j // (copies * capacity)) * capacity + j % capacity
    hits = [code == slot for slot in slots]
    pick = jnp.where(hits[0], weights[0], 0.0) + jnp.where(hits[1], weights[1], 0.0)
    high = pick.astype(BF16)
    pick_ref[:rows, :] = high
    pick_ref[rows:, :] = (pick - high.astype(F32)).astype(BF16)
    chosen = jnp.transpose(jnp.where(hits[0] | hits[1], 1.0, 0.0)).astype(BF16)
    buf_ref[...] = dot(chosen, norm).astype(BF16)


def final_kernel(pick_ref, back_ref, res_ref, o_ref):
    rows = res_ref.shape[0]
    both = dot(pick_ref[...], back_ref[...])
    o_ref[...] = (res_ref[...] + both[:rows] + both[rows:]).astype(BF16)


def local(
    stream,
    narrow_query_weight,
    wide_query_weight,
    value_rows_heads,
    output_gate_logits,
    narrow_forget_logits,
    wide_forget_logits,
    narrow_forget_headroom,
    wide_forget_headroom,
    extra_log_decay,
    per_head_norm_gain,
    mixer_output_weight,
    feedforward_norm_gain,
    expert_gate_matrix,
    expert_up_matrix,
    expert_down_matrix,
    routes,
    router_scores_chosen,
):
    local_inputs = (
        narrow_forget_logits, narrow_forget_headroom, extra_log_decay.transpose(1, 2, 0),
        narrow_query_weight, value_rows_heads, wide_forget_logits, wide_forget_headroom,
        wide_query_weight,
    )
    payload, inner, q_run, mixer_weight = pl.pallas_call(
        local_kernel,
        out_shape=(
            jax.ShapeDtypeStruct((2, PAY_ROWS, LANES), BF16),
            jax.ShapeDtypeStruct((4, TOK, LANES), F32),
            jax.ShapeDtypeStruct((TILES, TOK, 2 * LANES), BF16),
            pltpu.VMEM(mixer_output_weight.shape, BF16),
        ),
        in_specs=[HBM] * 9,
        out_specs=(VMEM,) * 4,
        scratch_shapes=[pltpu.VMEM(x.shape, x.dtype) for x in local_inputs]
        + [pltpu.SemaphoreType.DMA((9,))],
        compiler_params=pltpu.CompilerParams(vmem_limit_bytes=16 * 2**20),
        name="local_mixer",
    )(*map(in_hbm, local_inputs), in_hbm(mixer_output_weight))
    entering, pieces = entering_states(payload)
    tp = lax.axis_size("tp")
    rows = TOK // tp
    tiles = small_call(
        mix_kernel, "mix", (jax.ShapeDtypeStruct((rows, 4 * LANES), BF16),) * tp, inner, q_run,
        entering, pieces, output_gate_logits, per_head_norm_gain.reshape(1, 64),
        scratch=[pltpu.VMEM((TOK, 4 * LANES), BF16)],
    )
    width = stream.shape[1]
    experts = lax.axis_size(SP)
    capacity = max(2, 2 * routes.shape[1] * rows // experts)
    slots = experts * tp * capacity
    arrived = [tiles[0]] + from_each(None, "tp", tiles)
    residual, buffers, pick = pl.pallas_call(
        partial(route_kernel, experts, capacity, tp),
        out_shape=(
            jax.ShapeDtypeStruct((rows, width), F32),
            jax.ShapeDtypeStruct((slots, width), BF16),
            jax.ShapeDtypeStruct((2 * rows, slots), BF16),
        ),
        in_specs=[VMEM] * 9,
        out_specs=(VMEM,) * 3,
        scratch_shapes=[pltpu.VMEM((TOK, 8), F32)],
        compiler_params=pltpu.CompilerParams(vmem_limit_bytes=24 * 2**20),
        name="project_and_route",
    )(
        *arrived, mixer_weight, stream, feedforward_norm_gain.reshape(1, width),
        routes.T, router_scores_chosen.T,
    )
    tokens = lax.all_to_all(buffers, SP_TP, 0, 0, tiled=True)
    gate = jnp.dot(tokens, expert_gate_matrix[0], preferred_element_type=F32)
    up = jnp.dot(tokens, expert_up_matrix[0], preferred_element_type=F32)
    hidden = (jax.nn.silu(gate) * up).astype(BF16)
    part = jnp.dot(hidden, expert_down_matrix[0], preferred_element_type=F32).astype(BF16)
    back = lax.all_to_all(part, SP_TP, 0, 0, tiled=True)
    col = width // 4
    return pl.pallas_call(
        final_kernel,
        grid=(4,),
        in_specs=[
            pl.BlockSpec((2 * rows, slots), lambda i: (0, 0)),
            pl.BlockSpec((slots, col), lambda i: (0, i)),
            pl.BlockSpec((rows, col), lambda i: (0, i)),
        ],
        out_specs=pl.BlockSpec((rows, col), lambda i: (0, i)),
        out_shape=jax.ShapeDtypeStruct((rows, width), BF16),
        compiler_params=pltpu.CompilerParams(vmem_limit_bytes=12 * 2**20),
        name="combine",
    )(pick, back, residual)


def solution(mesh):
    torus = Mesh(mesh.devices.reshape(4, 4, 2, mesh.shape["tp"]), ("sp_0", "sp_1", "sp_2", "tp"))
    return jax.shard_map(
        local,
        mesh=torus,
        in_specs=(
            P(SP, None),
            P(SP, "tp"),
            P(SP, "tp"),
            P(SP, None, "tp"),
            P(SP, None, "tp"),
            P(None, SP, "tp"),
            P(None, SP, "tp"),
            P(None, "tp"),
            P(None, "tp"),
            P(SP, None, "tp"),
            P(),
            P(),
            P(),
            P(SP, None, "tp"),
            P(SP, None, "tp"),
            P(SP, "tp", None),
            P(SP, None),
            P(SP, None),
        ),
        out_specs=P(SP_TP, None),
        check_vma=False,
    )
```

time: 221 us -> 181 us (0.82)
  blocking collectives: 157 us -> 121 us
  Pallas kernels: 31.6 us -> 15.1 us
  waiting for transfers between devices: 3.27 us -> 16.9 us
  starting transfers between devices: 4.02 us -> 13.4 us
  local copies, waits for them, and re-layouts: 8.93 us -> 0.05 us
    all_gather x3 -> x2, blocking collectives: 35.6 us -> 5.61 us  [the longest x1 3.24 us: entering_states(): pieces = lax.all_gather(payload, 'sp_2')]
    ppermute x0 -> x9, waiting for transfers between devices: none -> 16.9 us  [from_each(): lax.ppermute(x if tiles is None else tiles[j], axis, [(i, (i + j) % count...]
    pallas_call x6, Pallas kernels: 27.1 us -> 12.6 us  [the longest x1 7.33 us: local(): pl.pallas_call(local_kernel, out_shape=(jax.ShapeDtypeStruct((2, PAY_ROWS...]
    ppermute x0 -> x9, starting transfers between devices: none -> 13.4 us  [from_each(): lax.ppermute(x if tiles is None else tiles[j], axis, [(i, (i + j) % count...]
    all_to_all x1, blocking collectives: 63.5 us -> 58.8 us  [local(): tokens = lax.all_to_all(buffers, SP_TP, 0, 0, tiled=True)]
    all_to_all x1 -> x0, starting transfers between devices: 4.02 us -> none  [local(): lax.all_to_all(mixed.reshape(tp, rows, 4 * LANES), 'tp', 0, 0, tiled=True)]
    all_to_all x1 -> x0, waiting for transfers between devices: 3.27 us -> none  [local(): lax.all_to_all(mixed.reshape(tp, rows, 4 * LANES), 'tp', 0, 0, tiled=True)]
    slice x2 -> x0, local copies, waits for them, and re-layouts: 2.96 us -> none  [the longest x1 1.48 us: local(): output_gate_logits[:, 1]]
  transfers between devices with their start and end apart: 1 -> 9, of which waited for: 1 -> 8; matrix products, arithmetic and copies ran while one was open for 1% -> 0% of each run, Pallas kernels for 0% -> 0%
where the time goes in v2:
time: 181 us
  blocking collectives  121 us (67%)
  waiting for transfers between devices  16.9 us (9%)
  Pallas kernels  15.1 us (8%)
  matrix products  14.4 us (8%)
  starting transfers between devices  13.4 us (7%)
    all_to_all x1, blocking collectives, local(): tokens = lax.all_to_all(buffers, SP_TP, 0, 0, tiled=True)  58.8 us
    all_to_all x1, blocking collectives, local(): back = lax.all_to_all(part, SP_TP, 0, 0, tiled=True)  56.8 us
    ppermute x9, waiting for transfers between devices, from_each(): lax.ppermute(x if tiles is None else tiles[j], axis, [(i, (i + j) % count...  16.9 us
    ppermute x9, starting transfers between devices, from_each(): lax.ppermute(x if tiles is None else tiles[j], axis, [(i, (i + j) % count...  13.4 us
    pallas_call x1, Pallas kernels, local(): pl.pallas_call(local_kernel, out_shape=(jax.ShapeDtypeStruct((2, PAY_ROWS...  7.33 us
    dot_general x1, matrix products, local(): up = jnp.dot(tokens, expert_up_matrix[0], preferred_element_type=F32)  5.14 us
    dot_general x1, matrix products, local(): jnp.dot(hidden, expert_down_matrix[0], preferred_element_type=F32)  4.76 us
    dot_general x1, matrix products, local(): gate = jnp.dot(tokens, expert_gate_matrix[0], preferred_element_type=F32)  4.54 us
  transfers between devices with their start and end apart: 9, of which 8 were waited for; matrix products, arithmetic and copies ran while one was open for 0% of the time, Pallas kernels for 0%

profile of v2, /device:TPU:1, one launch (start us, length us, event | category | flops | bytes accessed | tf_op | source)
XLA Modules:
  0.0 181.1 jit_solution(1020504477823488214)
XLA Ops:
  0.0 7.3 %local_mixer.1 = (bf16[2,400,128]{2,1,0:T(8,128)(2,1)S(1)}, f32[4,256,128]{2,1,0:T(8,128)S(1)}, bf16[6,256,256]{2,1,0:T(8,128)(2,1)S(1)}, bf16[2,1024,2048]{2,1,0:T(8,128)(2,1)S(1)}) custom-call(bf16[2,256,256]{2,1,0:T(8,128)(2,1)} %nf_hbm.1, f32[2,256]{1,0:T(2,128)} %nh_hbm.1, f32[2,4,256]{2,1,0:T(4,128)} %bitcast.41, bf16[256,256]{1,0:T(8,128)(2,1)} %nq_hbm.1, ...), custom_call_target="tpu_custom_call" | custom-call | tf_op jit(solution)/shard_map/local_mixer/pallas_call | solution.py:408
  7.4 3.2 %all-gather = bf16[4,400,128]{2,1,0:T(8,128)(2,1)S(1)} all-gather(bf16[2,400,128]{2,1,0:T(8,128)(2,1)S(1)} %get-tuple-element.21), channel_id=2, replica_groups=mesh['sp_0'=4,'sp_1'=4,'sp_2'=2,'tp'=4] {'sp_2'}, dimensions={0}, use_global_device_ids=true | all-gather | bytes 614400 | tf_op jit(solution)/shard_map/all_gather | solution.py:261
  10.7 2.9 %collective-permute-start.2 = (bf16[400,128]{1,0:T(8,128)(2,1)S(1)}, bf16[400,128]{1,0:T(8,128)(2,1)S(1)}, u32[]{:S(2)}, u32[]{:S(2)}) collective-permute-start(bf16[400,128]{1,0:T(8,128)(2,1)S(1)} %pair.1.refs_0_), channel_id=1, source_target_pairs={{0,24},{8,0},{16,8},{24,16},{1,25},{9,1},{17,9},{25,17},{2,26},{10... | collective-permute-start | bytes 307208 | tf_op jit(solution)/shard_map/ppermute | solution.py:232
  14.6 2.9 %collective-permute-done.2.refs_3_ = bf16[400,128]{1,0:T(8,128)(2,1)S(1)} collective-permute-done((bf16[400,128]{1,0:T(8,128)(2,1)S(1)}, bf16[400,128]{1,0:T(8,128)(2,1)S(1)}, u32[]{:S(2)}, u32[]{:S(2)}) %collective-permute-start.2) | collective-permute-done | bytes 102432 | tf_op jit(solution)/shard_map/ppermute | solution.py:232
  17.5 1.2 collective-permute-done.1.refs_2_
  18.7 3.3 %collective-permute-done.refs_1_ = bf16[400,128]{1,0:T(8,128)(2,1)S(1)} collective-permute-done((bf16[400,128]{1,0:T(8,128)(2,1)S(1)}, bf16[400,128]{1,0:T(8,128)(2,1)S(1)}, u32[]{:S(2)}, u32[]{:S(2)}) %collective-permute-start) | collective-permute-done | bytes 102432 | tf_op jit(solution)/shard_map/ppermute | solution.py:232
  22.2 3.8 %collective-permute-start.5 = (bf16[400,128]{1,0:T(8,128)(2,1)S(1)}, bf16[400,128]{1,0:T(8,128)(2,1)S(1)}, u32[]{:S(2)}, u32[]{:S(2)}) collective-permute-start(bf16[400,128]{1,0:T(8,128)(2,1)S(1)} %get-tuple-element.22.refs_0_), channel_id=1, source_target_pairs={{0,96},{32,0},{64,32},{96,64},{1,97},{33,1},{65,33},{97,65},{2,98}... | collective-permute-start | bytes 307208 | tf_op jit(solution)/shard_map/ppermute | solution.py:232
  26.0 0.7 collective-permute-start.3
  26.7 3.5 %collective-permute-done.5.refs_3_ = bf16[400,128]{1,0:T(8,128)(2,1)S(1)} collective-permute-done((bf16[400,128]{1,0:T(8,128)(2,1)S(1)}, bf16[400,128]{1,0:T(8,128)(2,1)S(1)}, u32[]{:S(2)}, u32[]{:S(2)}) %collective-permute-start.5) | collective-permute-done | bytes 102432 | tf_op jit(solution)/shard_map/ppermute | solution.py:232
  30.3 0.9 collective-permute-done.4.refs_2_
  31.1 2.8 %collective-permute-done.3.refs_1_ = bf16[400,128]{1,0:T(8,128)(2,1)S(1)} collective-permute-done((bf16[400,128]{1,0:T(8,128)(2,1)S(1)}, bf16[400,128]{1,0:T(8,128)(2,1)S(1)}, u32[]{:S(2)}, u32[]{:S(2)}) %collective-permute-start.3) | collective-permute-done | bytes 102432 | tf_op jit(solution)/shard_map/ppermute | solution.py:232
  34.1 2.4 %all-gather.1 = bf16[768,128]{1,0:T(8,128)(2,1)S(1)} all-gather(bf16[384,128]{1,0:T(8,128)(2,1)S(1)} %level_0.1), channel_id=3, replica_groups=mesh['sp_0'=4,'sp_1'=4,'sp_2'=2,'tp'=4] {'sp_2'}, dimensions={0}, use_global_device_ids=true | all-gather | bytes 294912 | tf_op jit(solution)/shard_map/all_gather | solution.py:271
  36.5 1.9 %mix.1 = (bf16[64,512]{1,0:T(8,128)(2,1)S(1)}, bf16[64,512]{1,0:T(8,128)(2,1)S(1)}, bf16[64,512]{1,0:T(8,128)(2,1)S(1)}, bf16[64,512]{1,0:T(8,128)(2,1)S(1)}) custom-call(f32[4,256,128]{2,1,0:T(8,128)S(1)} %get-tuple-element.19.out_ref, bf16[6,256,256]{2,1,0:T(8,128)(2,1)S(1)} %get-tuple-element.20.qr_ref, bf16[2,384,128]{2,1,0:T(8,128)(2,1)S(1)} %bitcast.36, ...), custom_call_target="tpu_custom_call" | custom-call | tf_op jit(solution)/shard_map/mix/pallas_call | solution.py:246
  38.4 1.3 collective-permute-start.6
  39.7 2.5 %collective-permute-start.7 = (bf16[64,512]{1,0:T(8,128)(2,1)S(1)}, bf16[64,512]{1,0:T(8,128)(2,1)S(1)}, u32[]{:S(2)}, u32[]{:S(2)}) collective-permute-start(bf16[64,512]{1,0:T(8,128)(2,1)S(1)} %get-tuple-element.27), channel_id=1, source_target_pairs={{0,2},{1,3},{2,0},{3,1},{4,6},{5,7},{6,4},{7,5},{8,10},{9,11},{10,... | collective-permute-start | bytes 196616 | tf_op jit(solution)/shard_map/ppermute | solution.py:232
  42.1 1.2 collective-permute-start.8
  43.3 1.8 collective-permute-done.7.x2_ref
  45.6 2.9 %project_and_route.1 = (f32[64,2048]{1,0:T(8,128)S(1)}, bf16[1024,2048]{1,0:T(8,128)(2,1)S(1)}, bf16[128,1024]{1,0:T(8,128)(2,1)S(1)}) custom-call(bf16[64,512]{1,0:T(8,128)(2,1)S(1)} %get-tuple-element.25.x0_ref, bf16[64,512]{1,0:T(8,128)(2,1)S(1)} %collective-permute-done.6.x1_ref, bf16[64,512]{1,0:T(8,128)(2,1)S(1)} %collective-permute-done.7.x2_ref, ...), custom_call_target="tpu_custom_call" | custom-call | tf_op jit(solution)/shard_map/project_and_route/pallas_call | solution.py:436
  48.5 58.8 %all_to_all.23 = bf16[128,8,2048]{2,1,0:T(8,128)(2,1)S(1)} all-to-all(bf16[128,8,2048]{2,1,0:T(8,128)(2,1)S(1)} %bitcast.33), channel_id=1, replica_groups=mesh['sp_0'=4,'sp_1'=4,'sp_2'=2,'tp'=4] {'sp_0','sp_1','sp_2','tp'}, dimensions={0} | all-to-all | bytes 8388608 | tf_op jit(solution)/shard_map/all_to_all | solution.py:452
  107.3 4.5 %fusion.4 = f32[1024,1024]{1,0:T(8,128)S(1)} fusion(bf16[1,2048,1024]{2,1,0:T(8,128)(2,1)S(1)} %copy-done.6, bf16[128,8,2048]{2,1,0:T(8,128)(2,1)S(1)} %all_to_all.23), kind=kOutput, calls=%fused_computation.4 | convolution fusion | flops 4294967296 | bytes 12582912 | tf_op jit(solution)/shard_map/dot_general | solution.py:453
  111.9 5.1 %multiply_convert_fusion = bf16[1024,1024]{1,0:T(8,128)(2,1)S(1)} fusion(f32[1024,1024]{1,0:T(8,128)S(1)} %fusion.4, bf16[1,2048,1024]{2,1,0:T(8,128)(2,1)S(1)} %copy-done.7, bf16[128,8,2048]{2,1,0:T(8,128)(2,1)S(1)} %all_to_all.23), kind=kOutput, calls=%fused_computation.9 | convolution fusion | flops 4301258752 | bytes 14680064 | tf_op jit(solution)/shard_map/dot_general | solution.py:454
  117.0 4.8 %convert_bitcast_fusion = bf16[128,8,2048]{2,1,0:T(8,128)(2,1)S(1)} fusion(bf16[1024,1024]{1,0:T(8,128)(2,1)S(1)} %multiply_convert_fusion, bf16[1,1024,2048]{2,1,0:T(8,128)(2,1)S(1)} %copy-done.8), kind=kOutput, calls=%fused_computation.8 | convolution fusion | flops 4297064448 | bytes 10485760 | tf_op jit(solution)/shard_map/dot_general | solution.py:456
  121.8 56.8 %all_to_all.24 = bf16[128,8,2048]{2,1,0:T(8,128)(2,1)S(1)} all-to-all(bf16[128,8,2048]{2,1,0:T(8,128)(2,1)S(1)} %convert_bitcast_fusion), channel_id=1, replica_groups=mesh['sp_0'=4,'sp_1'=4,'sp_2'=2,'tp'=4] {'sp_0','sp_1','sp_2','tp'}, dimensions={0} | all-to-all | bytes 8388608 | tf_op jit(solution)/shard_map/all_to_all | solution.py:457
  178.6 2.5 %combine.1 = bf16[64,2048]{1,0:T(8,128)(2,1)} custom-call(bf16[128,1024]{1,0:T(8,128)(2,1)S(1)} %get-tuple-element.30.pick_ref, bf16[1024,2048]{1,0:T(8,128)(2,1)S(1)} %bitcast.32, f32[64,2048]{1,0:T(8,128)S(1)} %get-tuple-element.32.res_ref), custom_call_target="tpu_custom_call" | custom-call | tf_op jit(solution)/shard_map/combine/pallas_call | solution.py:459
  (26 shorter events, 1.9 us)
Async XLA Ops:
  0.0 36.5 %copy-start.1 = (bf16[256,2,256]{2,1,0:T(2,128)(2,1)S(1)}, bf16[256,2,256]{2,1,0:T(2,128)(2,1)}, u32[]{:S(2)}) copy-start(bf16[256,2,256]{2,1,0:T(2,128)(2,1)} %gate_ref.1) | copy-start | bytes 786436
  0.0 36.5 %copy-start.5 = (f32[64]{0:T(128)S(1)}, f32[64]{0:T(128)}, u32[]{:S(2)}) copy-start(f32[64]{0:T(128)} %param.28) | copy-start | bytes 772
  7.3 38.2 %copy-start = (bf16[256,2048]{1,0:T(8,128)(2,1)S(1)}, bf16[256,2048]{1,0:T(8,128)(2,1)}, u32[]{:S(2)}) copy-start(bf16[256,2048]{1,0:T(8,128)(2,1)} %stream_ref.1) | copy-start | bytes 3145732
  7.4 38.2 %copy-start.2 = (f32[2048]{0:T(1024)S(1)}, f32[2048]{0:T(1024)}, u32[]{:S(2)}) copy-start(f32[2048]{0:T(1024)} %param.30) | copy-start | bytes 24580
  7.4 38.2 %copy-start.3 = (s32[256,2]{0,1:T(2,128)S(1)}, s32[256,2]{0,1:T(2,128)}, u32[]{:S(2)}) copy-start(s32[256,2]{0,1:T(2,128)} %param.34) | copy-start | bytes 6148
  7.4 38.2 %copy-start.4 = (f32[256,2]{0,1:T(2,128)S(1)}, f32[256,2]{0,1:T(2,128)}, u32[]{:S(2)}) copy-start(f32[256,2]{0,1:T(2,128)} %param.35) | copy-start | bytes 6148
  10.7 6.8 %collective-permute-start.2 = (bf16[400,128]{1,0:T(8,128)(2,1)S(1)}, bf16[400,128]{1,0:T(8,128)(2,1)S(1)}, u32[]{:S(2)}, u32[]{:S(2)}) collective-permute-start(bf16[400,128]{1,0:T(8,128)(2,1)S(1)} %pair.1.refs_0_), channel_id=1, source_target_pairs={{0,24},{8,0},{16,8},{24,16},{1,25},{9,1},{17,9},{25,17},{2,26},{10... | collective-permute-start | bytes 307208 | tf_op jit(solution)/shard_map/ppermute | solution.py:232
  13.6 5.1 %collective-permute-start.1 = (bf16[400,128]{1,0:T(8,128)(2,1)S(1)}, bf16[400,128]{1,0:T(8,128)(2,1)S(1)}, u32[]{:S(2)}, u32[]{:S(2)}) collective-permute-start(bf16[400,128]{1,0:T(8,128)(2,1)S(1)} %pair.1.refs_0_), channel_id=1, source_target_pairs={{0,16},{8,24},{16,0},{24,8},{1,17},{9,25},{17,1},{25,9},{2,18},{10... | collective-permute-start | bytes 307208 | tf_op jit(solution)/shard_map/ppermute | solution.py:232
  13.9 8.1 %collective-permute-start = (bf16[400,128]{1,0:T(8,128)(2,1)S(1)}, bf16[400,128]{1,0:T(8,128)(2,1)S(1)}, u32[]{:S(2)}, u32[]{:S(2)}) collective-permute-start(bf16[400,128]{1,0:T(8,128)(2,1)S(1)} %pair.1.refs_0_), channel_id=1, source_target_pairs={{0,8},{8,16},{16,24},{24,0},{1,9},{9,17},{17,25},{25,1},{2,10},{10... | collective-permute-start | bytes 307208 | tf_op jit(solution)/shard_map/ppermute | solution.py:232
  22.2 8.1 %collective-permute-start.5 = (bf16[400,128]{1,0:T(8,128)(2,1)S(1)}, bf16[400,128]{1,0:T(8,128)(2,1)S(1)}, u32[]{:S(2)}, u32[]{:S(2)}) collective-permute-start(bf16[400,128]{1,0:T(8,128)(2,1)S(1)} %get-tuple-element.22.refs_0_), channel_id=1, source_target_pairs={{0,96},{32,0},{64,32},{96,64},{1,97},{33,1},{65,33},{97,65},{2,98}... | collective-permute-start | bytes 307208 | tf_op jit(solution)/shard_map/ppermute | solution.py:232
  26.0 5.1 %collective-permute-start.4 = (bf16[400,128]{1,0:T(8,128)(2,1)S(1)}, bf16[400,128]{1,0:T(8,128)(2,1)S(1)}, u32[]{:S(2)}, u32[]{:S(2)}) collective-permute-start(bf16[400,128]{1,0:T(8,128)(2,1)S(1)} %get-tuple-element.22.refs_0_), channel_id=1, source_target_pairs={{0,64},{32,96},{64,0},{96,32},{1,65},{33,97},{65,1},{97,33},{2,66}... | collective-permute-start | bytes 307208 | tf_op jit(solution)/shard_map/ppermute | solution.py:232
  26.0 7.9 %collective-permute-start.3 = (bf16[400,128]{1,0:T(8,128)(2,1)S(1)}, bf16[400,128]{1,0:T(8,128)(2,1)S(1)}, u32[]{:S(2)}, u32[]{:S(2)}) collective-permute-start(bf16[400,128]{1,0:T(8,128)(2,1)S(1)} %get-tuple-element.22.refs_0_), channel_id=1, source_target_pairs={{0,32},{32,64},{64,96},{96,0},{1,33},{33,65},{65,97},{97,1},{2,34}... | collective-permute-start | bytes 307208 | tf_op jit(solution)/shard_map/ppermute | solution.py:232
  38.4 4.9 %collective-permute-start.6 = (bf16[64,512]{1,0:T(8,128)(2,1)S(1)}, bf16[64,512]{1,0:T(8,128)(2,1)S(1)}, u32[]{:S(2)}, u32[]{:S(2)}) collective-permute-start(bf16[64,512]{1,0:T(8,128)(2,1)S(1)} %get-tuple-element.26), channel_id=1, source_target_pairs={{0,1},{1,2},{2,3},{3,0},{4,5},{5,6},{6,7},{7,4},{8,9},{9,10},{10,1... | collective-permute-start | bytes 196616 | tf_op jit(solution)/shard_map/ppermute | solution.py:232
  39.7 5.4 %collective-permute-start.7 = (bf16[64,512]{1,0:T(8,128)(2,1)S(1)}, bf16[64,512]{1,0:T(8,128)(2,1)S(1)}, u32[]{:S(2)}, u32[]{:S(2)}) collective-permute-start(bf16[64,512]{1,0:T(8,128)(2,1)S(1)} %get-tuple-element.27), channel_id=1, source_target_pairs={{0,2},{1,3},{2,0},{3,1},{4,6},{5,7},{6,4},{7,5},{8,10},{9,11},{10,... | collective-permute-start | bytes 196616 | tf_op jit(solution)/shard_map/ppermute | solution.py:232
  42.1 3.4 %collective-permute-start.8 = (bf16[64,512]{1,0:T(8,128)(2,1)S(1)}, bf16[64,512]{1,0:T(8,128)(2,1)S(1)}, u32[]{:S(2)}, u32[]{:S(2)}) collective-permute-start(bf16[64,512]{1,0:T(8,128)(2,1)S(1)} %get-tuple-element.28), channel_id=1, source_target_pairs={{0,3},{1,0},{2,1},{3,2},{4,7},{5,4},{6,5},{7,6},{8,11},{9,8},{10,9... | collective-permute-start | bytes 196616 | tf_op jit(solution)/shard_map/ppermute | solution.py:232
  48.5 58.8 %copy-start.6 = (bf16[1,2048,1024]{2,1,0:T(8,128)(2,1)S(1)}, bf16[1,2048,1024]{2,1,0:T(8,128)(2,1)}, u32[]{:S(2)}) copy-start(bf16[1,2048,1024]{2,1,0:T(8,128)(2,1)} %param.31) | copy-start | bytes 12582916
  107.3 4.6 %copy-start.7 = (bf16[1,2048,1024]{2,1,0:T(8,128)(2,1)S(1)}, bf16[1,2048,1024]{2,1,0:T(8,128)(2,1)}, u32[]{:S(2)}) copy-start(bf16[1,2048,1024]{2,1,0:T(8,128)(2,1)} %param.32) | copy-start | bytes 12582916
  111.9 5.2 %copy-start.8 = (bf16[1,1024,2048]{2,1,0:T(8,128)(2,1)S(1)}, bf16[1,1024,2048]{2,1,0:T(8,128)(2,1)}, u32[]{:S(2)}) copy-start(bf16[1,1024,2048]{2,1,0:T(8,128)(2,1)} %param.33) | copy-start | bytes 12582916

commit v3 on v2

--- a/solution.py
+++ b/solution.py
@@ -36,92 +36,174 @@
     return x / (1.0 + jnp.exp(-x))
 
 
-def local_kernel(
-    nf_hbm, nh_hbm, ex_hbm, nq_hbm, v_hbm, wf_hbm, wh_hbm, wq_hbm, w_hbm, pay_ref, out_ref, qr_ref,
-    w_ref, nf_ref, nh_ref, ex_ref, nq_ref, v_ref, wf_ref, wh_ref, wq_ref, sems,
-):
-    sources = (nf_hbm, nh_hbm, ex_hbm, nq_hbm, v_hbm, wf_hbm, wh_hbm, wq_hbm, w_hbm)
-    targets = (nf_ref, nh_ref, ex_ref, nq_ref, v_ref, wf_ref, wh_ref, wq_ref, w_ref)
+def copied(sources, targets, sems):
     copies = [
         pltpu.make_async_copy(a, b, sems.at[i]) for i, (a, b) in enumerate(zip(sources, targets))
     ]
     for copy in copies:
         copy.start()
-    for copy in copies[:-1]:
-        copy.wait()
-    ex = jnp.transpose(jnp.concatenate([ex_ref[0], ex_ref[1]], axis=0))
-    ri = lax.broadcasted_iota(jnp.int32, (TOK, TOK), 0)
-    ci = lax.broadcasted_iota(jnp.int32, (TOK, TOK), 1)
-    same = (ri // BLK) == (ci // BLK)
-    tri = (same & (ci <= ri), same & (ci >= ri))
-    ones = tuple(jnp.where(t, 1.0, 0.0).astype(BF16) for t in tri)
-    lane = lax.broadcasted_iota(jnp.int32, (1, LANES), 1)
-    low = lane < 64
-    low2 = (lax.broadcasted_iota(jnp.int32, (1, 2 * LANES), 1) % LANES) < 64
-    decays = [None] * (2 * TILES)
-
-    def prepare(tile, q_raw, f_raw, rooms, extra):
-        q = silu(q_raw.astype(F32)).reshape(NB, BLK, LANES)
-        qi, ki, ke, qr, ends = [], [], [], [], []
-        for d in range(2):
-            opening = rooms[d] / (1.0 + jnp.exp(f_raw[d].astype(F32)))
-            ld = jnp.log(1.0 - opening) + extra
-            hi = ld.astype(BF16)
-            lo = (ld - hi.astype(F32)).astype(BF16)
-            both = dot(ones[d], jnp.concatenate([hi, lo], axis=1))
-            inside = (both[:, :LANES] + both[:, LANES:]).reshape(NB, BLK, LANES)
-            opening = opening.reshape(NB, BLK, LANES)
-            edge = BLK - 1 if d == 0 else 0
-            end = [inside[b, edge : edge + 1, :] for b in range(NB)]
-            start = [None] * NB
-            run = jnp.zeros((1, LANES), F32)
-            for b in range(NB) if d == 0 else reversed(range(NB)):
-                start[b] = run
-                run = run + end[b]
-            decays[d * TILES + tile] = jnp.exp(run)
-            start4 = jnp.stack(start, axis=0)
-            end4 = jnp.stack(end, axis=0)
-            qi.append((q * jnp.exp(inside)).reshape(TOK, LANES))
-            qr.append((q * jnp.exp(inside + start4)).reshape(TOK, LANES).astype(BF16))
-            ki.append((opening * jnp.exp(-inside)).reshape(TOK, LANES))
-            ke.append((opening * jnp.exp(end4 - inside)).reshape(TOK, LANES).astype(BF16))
-            ends.append([jnp.exp(e) for e in end])
-        qr_ref[tile] = jnp.concatenate(qr, axis=1)
-        return qi, ki, jnp.concatenate(ke, axis=1), ends
-
-    def block_states(tile, kv, ends):
+    return copies
+
+
+class Tiles:
+    def __init__(self, ex_ref):
+        ri = lax.broadcasted_iota(jnp.int32, (TOK, TOK), 0)
+        ci = lax.broadcasted_iota(jnp.int32, (TOK, TOK), 1)
+        self.same = (ri // BLK) == (ci // BLK)
+        self.tri = (self.same & (ci <= ri), self.same & (ci >= ri))
+        self.ones = tuple(jnp.where(t, 1.0, 0.0).astype(BF16) for t in self.tri)
+        self.low = lax.broadcasted_iota(jnp.int32, (1, LANES), 1) < 64
+        self.low2 = (lax.broadcasted_iota(jnp.int32, (1, 2 * LANES), 1) % LANES) < 64
+        self.ex = jnp.transpose(jnp.concatenate([ex_ref[0], ex_ref[1]], axis=0))
+
+    def extra(self, tile):
+        if tile >= 2:
+            return self.ex[:, tile + 2 : tile + 3]
+        return jnp.where(
+            self.low, self.ex[:, 2 * tile : 2 * tile + 1], self.ex[:, 2 * tile + 1 : 2 * tile + 2]
+        )
+
+    def decayed(self, tile, d, f_raw, room):
+        opening = room / (1.0 + jnp.exp(f_raw.astype(F32)))
+        ld = jnp.log(1.0 - opening) + self.extra(tile)
+        hi = ld.astype(BF16)
+        lo = (ld - hi.astype(F32)).astype(BF16)
+        both = dot(self.ones[d], jnp.concatenate([hi, lo], axis=1))
+        inside = (both[:, :LANES] + both[:, LANES:]).reshape(NB, BLK, LANES)
+        edge = BLK - 1 if d == 0 else 0
+        end = [inside[b, edge : edge + 1, :] for b in range(NB)]
+        start = [None] * NB
+        run = jnp.zeros((1, LANES), F32)
+        for b in range(NB) if d == 0 else reversed(range(NB)):
+            start[b] = run
+            run = run + end[b]
+        opening = opening.reshape(NB, BLK, LANES)
+        ke = (opening * jnp.exp(jnp.stack(end, axis=0) - inside)).reshape(TOK, LANES).astype(BF16)
+        return opening, inside, [jnp.exp(e) for e in end], jnp.stack(start, axis=0), run, ke
+
+    def block_values(self, tile, v, ke):
+        vt = jnp.transpose(v.astype(F32))
+
+        def spread(part):
+            return jnp.where(self.same, jnp.concatenate([part] * NB, axis=0), 0.0).astype(BF16)
+
+        if tile >= 2:
+            half = (tile % 2) * 64
+            return dot(spread(vt[half : half + 64]), ke)
+        return jnp.where(self.low2, dot(spread(vt[:64]), ke), dot(spread(vt[64:]), ke))
+
+    def swept(self, kv, ends):
         states = [[None, None] for _ in range(NB)]
+        closing = []
         for d in range(2):
             run = jnp.zeros((64, LANES), F32)
             for b in range(NB) if d == 0 else reversed(range(NB)):
                 states[b][d] = run
                 run = run * ends[d][b] + kv[b * 64 : b * 64 + 64, d * LANES : (d + 1) * LANES]
-            pay_ref[d, tile * 64 : tile * 64 + 64, :] = run.astype(BF16)
-        return [jnp.concatenate(s, axis=1) for s in states]
-
-    def transposed(v):
-        return jnp.transpose(v.astype(F32))
-
-    def spread(vt):
-        return jnp.where(same, jnp.concatenate([vt] * NB, axis=0), 0.0).astype(BF16)
+            closing.append(run)
+        return [jnp.concatenate(s, axis=1) for s in states], closing
+
+
+def place_of(tile):
+    if tile < 2:
+        return slice(tile * LANES, (tile + 1) * LANES), slice(tile * LANES, (tile + 1) * LANES)
+    h = tile - 2
+    return slice(h * LANES, (h + 1) * LANES), slice(h // 2 * LANES, (h // 2 + 1) * LANES)
+
+
+def states_kernel(
+    nf_hbm, nh_hbm, ex_hbm, v_hbm, wf_hbm, wh_hbm, pay_ref, nf_ref, nh_ref, ex_ref, v_ref, wf_ref,
+    wh_ref, sems,
+):
+    copies = copied(
+        (nf_hbm, nh_hbm, ex_hbm, v_hbm, wf_hbm, wh_hbm),
+        (nf_ref, nh_ref, ex_ref, v_ref, wf_ref, wh_ref),
+        sems,
+    )
+    for copy in copies[:4]:
+        copy.wait()
+    tiles = Tiles(ex_ref)
+    decays = [[], []]
+    for tile in range(TILES):
+        if tile == 2:
+            for copy in copies[4:]:
+                copy.wait()
+        cols, v_cols = place_of(tile)
+        f_ref, h_ref = (nf_ref, nh_ref) if tile < 2 else (wf_ref, wh_ref)
+        ke, ends = [], []
+        for d in range(2):
+            _, _, end, _, total, k = tiles.decayed(tile, d, f_ref[d, :, cols], h_ref[d : d + 1, cols])
+            ke.append(k)
+            ends.append(end)
+            decays[d].append(jnp.exp(total))
+        kv = tiles.block_values(tile, v_ref[:, 0 if tile < 2 else 1, v_cols], jnp.concatenate(ke, axis=1))
+        _, closing = tiles.swept(kv, ends)
+        for d in range(2):
+            pay_ref[d, tile * 64 : tile * 64 + 64, :] = closing[d].astype(BF16)
+    for d in range(2):
+        pay_ref[d, STATE_ROWS:, :] = packed(decays[d])
+
+
+def narrow_kernel(
+    nf_hbm, nh_hbm, ex_hbm, v_hbm, nq_hbm, w_hbm, after_ref, out_ref, qr_ref, w_ref,
+    nf_ref, nh_ref, ex_ref, v_ref, nq_ref, sems,
+):
+    del after_ref
+    copies = copied(
+        (nf_hbm, nh_hbm, ex_hbm, v_hbm, nq_hbm, w_hbm), (nf_ref, nh_ref, ex_ref, v_ref, nq_ref, w_ref), sems
+    )
+    for copy in copies[:-1]:
+        copy.wait()
+    own_outputs(0, nf_ref, nh_ref, ex_ref, v_ref, nq_ref, out_ref, qr_ref)
+    copies[-1].wait()
+
+
+def wide_kernel(
+    wf_hbm, wh_hbm, ex_hbm, v_hbm, wq_hbm, after_ref, out_ref, qr_ref, token_ref,
+    wf_ref, wh_ref, ex_ref, v_ref, wq_ref, sems,
+):
+    del after_ref
+    for copy in copied(
+        (wf_hbm, wh_hbm, ex_hbm, v_hbm, wq_hbm), (wf_ref, wh_ref, ex_ref, v_ref, wq_ref), sems
+    ):
+        copy.wait()
+    own_outputs(1, wf_ref, wh_ref, ex_ref, v_ref, wq_ref, out_ref, qr_ref)
+    token_ref[...] = jnp.zeros(token_ref.shape, F32)
+
+
+def own_outputs(group, f_ref, h_ref, ex_ref, v_ref, q_ref, out_ref, qr_ref):
+    tiles = Tiles(ex_ref)
+    low, low2 = tiles.low, tiles.low2
+
+    def prepare(tile):
+        cols, v_cols = place_of(tile)
+        q = silu(q_ref[:, cols].astype(F32)).reshape(NB, BLK, LANES)
+        qi, ki, ke, qr, ends = [], [], [], [], []
+        for d in range(2):
+            opening, inside, end, start, _, k = tiles.decayed(
+                tile, d, f_ref[d, :, cols], h_ref[d : d + 1, cols]
+            )
+            qi.append((q * jnp.exp(inside)).reshape(TOK, LANES))
+            qr.append((q * jnp.exp(inside + start)).reshape(TOK, LANES).astype(BF16))
+            ki.append((opening * jnp.exp(-inside)).reshape(TOK, LANES))
+            ke.append(k)
+            ends.append(end)
+        qr_ref[tile - 2 * group] = jnp.concatenate(qr, axis=1)
+        v = v_ref[:, group, v_cols]
+        states, _ = tiles.swept(tiles.block_values(tile, v, jnp.concatenate(ke, axis=1)), ends)
+        return qi, ki, states, v
 
     def scores(qi, ki):
-        total = jnp.where(tri[0], dot_t(qi[0].astype(BF16), ki[0].astype(BF16)), 0.0)
-        total = total + jnp.where(tri[1], dot_t(qi[1].astype(BF16), ki[1].astype(BF16)), 0.0)
+        total = jnp.where(tiles.tri[0], dot_t(qi[0].astype(BF16), ki[0].astype(BF16)), 0.0)
+        total = total + jnp.where(tiles.tri[1], dot_t(qi[1].astype(BF16), ki[1].astype(BF16)), 0.0)
         return total.astype(BF16)
 
-    for p in range(2):
-        cols = slice(p * LANES, (p + 1) * LANES)
-        v = v_ref[:, 0, cols]
-        extra = jnp.where(low, ex[:, 2 * p : 2 * p + 1], ex[:, 2 * p + 1 : 2 * p + 2])
-        qi, ki, ke, ends = prepare(
-            p, nq_ref[:, cols], (nf_ref[0, :, cols], nf_ref[1, :, cols]),
-            (nh_ref[0:1, cols], nh_ref[1:2, cols]), extra,
-        )
-        vt = transposed(v)
-        kv = jnp.where(low2, dot(spread(vt[:64]), ke), dot(spread(vt[64:]), ke))
-        states = block_states(p, kv, ends)
-        q_cat = jnp.concatenate([x.astype(BF16) for x in qi], axis=1)
+    def joined(qi):
+        return jnp.concatenate([x.astype(BF16) for x in qi], axis=1)
+
+    for p in range(2) if group == 0 else ():
+        qi, ki, states, v = prepare(p)
+        q_cat = joined(qi)
         parts = []
         for b in range(NB):
             s = jnp.concatenate(
@@ -132,20 +214,12 @@
         second = dot(scores(qi, [jnp.where(low, 0.0, k) for k in ki]), v)
         out_ref[p] = jnp.where(low, first, second) + jnp.concatenate(parts, axis=0)
 
-    for p in range(2):
-        v = v_ref[:, 1, p * LANES : (p + 1) * LANES]
-        vt = transposed(v)
+    for p in range(2) if group == 1 else ():
         inner, q_cats, head_states = [], [], []
-        for i in range(2):
-            h = 2 * p + i
-            cols = slice(h * LANES, (h + 1) * LANES)
-            qi, ki, ke, ends = prepare(
-                2 + h, wq_ref[:, cols], (wf_ref[0, :, cols], wf_ref[1, :, cols]),
-                (wh_ref[0:1, cols], wh_ref[1:2, cols]), ex[:, 4 + h : 5 + h],
-            )
-            kv = dot(spread(vt[i * 64 : i * 64 + 64]), ke)
-            head_states.append(block_states(2 + h, kv, ends))
-            q_cats.append(jnp.concatenate([x.astype(BF16) for x in qi], axis=1))
+        for tile in (2 + 2 * p, 3 + 2 * p):
+            qi, ki, states, v = prepare(tile)
+            head_states.append(states)
+            q_cats.append(joined(qi))
             inner.append(dot(scores(qi, ki), v))
         parts = []
         for b in range(NB):
@@ -154,11 +228,7 @@
             parts.append(
                 jnp.where(low, dot_t(q_cats[0][rows], s), dot_t(q_cats[1][rows], s))
             )
-        out_ref[2 + p] = jnp.where(low, inner[0], inner[1]) + jnp.concatenate(parts, axis=0)
-
-    for d in range(2):
-        pay_ref[d, STATE_ROWS:, :] = packed(decays[d * TILES : (d + 1) * TILES])
-    copies[-1].wait()
+        out_ref[p] = jnp.where(low, inner[0], inner[1]) + jnp.concatenate(parts, axis=0)
 
 
 def packed(rows):
@@ -185,6 +255,8 @@
 
 
 def level_kernel(count, axis, last, *refs):
+    if not last:
+        refs = refs[1:]
     pieces, refs = refs[:count], refs[count:]
     backward = lax.axis_index("sp_2") == 1
     here = lax.axis_index(axis)
@@ -254,24 +326,7 @@
     )(*arrays)
 
 
-def entering_states(payload):
-    states = jax.ShapeDtypeStruct((STATE_ROWS, LANES), F32)
-    decays = jax.ShapeDtypeStruct((8, LANES), F32)
-    half = jax.ShapeDtypeStruct((PAY_ROWS, LANES), BF16)
-    pieces = lax.all_gather(payload, "sp_2")
-    chip = small_call(pair_kernel, "pair", half, pieces)
-    s, d, row = small_call(
-        partial(level_kernel, lax.axis_size("sp_1"), "sp_1", False), "level_1", (states, decays, half),
-        chip, *from_each(chip, "sp_1"),
-    )
-    entering = small_call(
-        partial(level_kernel, lax.axis_size("sp_0"), "sp_0", True), "level_0",
-        jax.ShapeDtypeStruct((STATE_ROWS, LANES), BF16), row, *from_each(row, "sp_0"), s, d,
-    )
-    return lax.all_gather(entering, "sp_2"), pieces
-
-
-def mix_kernel(out_ref, qr_ref, in_ref, pieces_ref, gate_ref, gain_ref, *refs):
+def mix_kernel(n_out_ref, n_qr_ref, w_out_ref, w_qr_ref, in_ref, pieces_ref, gate_ref, gain_ref, *refs):
     *tile_refs, mixed_ref = refs
     low = lax.broadcasted_iota(jnp.int32, (1, LANES), 1) < 64
     low2 = (lax.broadcasted_iota(jnp.int32, (1, 2 * LANES), 1) % LANES) < 64
@@ -294,12 +349,11 @@
         if u < 2:
             s = entering(u)
             s = jnp.concatenate([jnp.where(low2, s, 0.0), jnp.where(low2, 0.0, s)], axis=0)
-            o = dot_t(qr_ref[u], s.astype(BF16))
+            o = dot_t(n_qr_ref[u], s.astype(BF16)) + n_out_ref[u]
         else:
             t = 2 + 2 * (u - 2)
-            o = dot_t(qr_ref[t], jnp.concatenate([entering(t), zero], axis=0).astype(BF16))
-            o = o + dot_t(qr_ref[t + 1], jnp.concatenate([zero, entering(t + 1)], axis=0).astype(BF16))
-        o = o + out_ref[u]
+            o = w_out_ref[u - 2] + dot_t(w_qr_ref[t - 2], jnp.concatenate([entering(t), zero], axis=0).astype(BF16))
+            o = o + dot_t(w_qr_ref[t - 1], jnp.concatenate([zero, entering(t + 1)], axis=0).astype(BF16))
         square = o * o
         first = jnp.sum(jnp.where(low, square, 0.0), axis=-1, keepdims=True)
         second = jnp.sum(jnp.where(low, 0.0, square), axis=-1, keepdims=True)
@@ -400,32 +454,66 @@
     routes,
     router_scores_chosen,
 ):
-    local_inputs = (
-        narrow_forget_logits, narrow_forget_headroom, extra_log_decay.transpose(1, 2, 0),
-        narrow_query_weight, value_rows_heads, wide_forget_logits, wide_forget_headroom,
-        wide_query_weight,
-    )
-    payload, inner, q_run, mixer_weight = pl.pallas_call(
-        local_kernel,
-        out_shape=(
-            jax.ShapeDtypeStruct((2, PAY_ROWS, LANES), BF16),
-            jax.ShapeDtypeStruct((4, TOK, LANES), F32),
-            jax.ShapeDtypeStruct((TILES, TOK, 2 * LANES), BF16),
-            pltpu.VMEM(mixer_output_weight.shape, BF16),
-        ),
-        in_specs=[HBM] * 9,
-        out_specs=(VMEM,) * 4,
-        scratch_shapes=[pltpu.VMEM(x.shape, x.dtype) for x in local_inputs]
-        + [pltpu.SemaphoreType.DMA((9,))],
-        compiler_params=pltpu.CompilerParams(vmem_limit_bytes=16 * 2**20),
-        name="local_mixer",
-    )(*map(in_hbm, local_inputs), in_hbm(mixer_output_weight))
-    entering, pieces = entering_states(payload)
+    nf, wf = in_hbm(narrow_forget_logits), in_hbm(wide_forget_logits)
+    nh, wh = in_hbm(narrow_forget_headroom), in_hbm(wide_forget_headroom)
+    nq, wq = in_hbm(narrow_query_weight), in_hbm(wide_query_weight)
+    extra, values = in_hbm(extra_log_decay.transpose(1, 2, 0)), in_hbm(value_rows_heads)
+
+    def from_hbm(kernel, name, inputs, shapes, vmem, after=(), kept=0, flops=0):
+        buffered = inputs[: len(inputs) - kept]
+        return pl.pallas_call(
+            kernel,
+            out_shape=shapes,
+            in_specs=[HBM] * len(inputs) + [VMEM] * len(after),
+            out_specs=jax.tree.map(lambda _: VMEM, shapes),
+            scratch_shapes=[pltpu.VMEM(x.shape, x.dtype) for x in buffered]
+            + [pltpu.SemaphoreType.DMA((len(inputs),))],
+            compiler_params=pltpu.CompilerParams(vmem_limit_bytes=vmem * 2**20),
+            cost_estimate=pl.CostEstimate(
+                flops=flops, bytes_accessed=3 * 2**20, transcendentals=2 * 10**6
+            ),
+            name=name,
+        )(*inputs, *after)
+
+    payload = from_hbm(
+        states_kernel, "local_states", (nf, nh, extra, values, wf, wh),
+        jax.ShapeDtypeStruct((2, PAY_ROWS, LANES), BF16), 12, flops=10**9,
+    )
+    states = jax.ShapeDtypeStruct((STATE_ROWS, LANES), F32)
+    decays = jax.ShapeDtypeStruct((8, LANES), F32)
+    half = jax.ShapeDtypeStruct((PAY_ROWS, LANES), BF16)
+    own = jax.ShapeDtypeStruct((2, TOK, LANES), F32)
+
+    def queries(count):
+        return jax.ShapeDtypeStruct((count, TOK, 2 * LANES), BF16)
+
+    pieces = lax.all_gather(payload, "sp_2")
+    chip = small_call(pair_kernel, "pair", half, pieces)
+    chips = [chip, *from_each(chip, "sp_1")]
+    wide, wide_q, token = from_hbm(
+        wide_kernel, "wide_outputs", (wf, wh, extra, values, wq), (own, queries(4), decays), 20,
+        after=(chip,), flops=3 * 10**9,
+    )
+    s, d, row = small_call(
+        partial(level_kernel, lax.axis_size("sp_1"), "sp_1", False), "level_1", (states, decays, half),
+        token, *chips,
+    )
+    rows_ = [row, *from_each(row, "sp_0")]
+    narrow, narrow_q, mixer_weight = from_hbm(
+        narrow_kernel, "narrow_outputs", (nf, nh, extra, values, nq, in_hbm(mixer_output_weight)),
+        (own, queries(2), pltpu.VMEM(mixer_output_weight.shape, BF16)), 20, after=(d,), kept=1,
+        flops=3 * 10**9,
+    )
+    entering = small_call(
+        partial(level_kernel, lax.axis_size("sp_0"), "sp_0", True), "level_0",
+        jax.ShapeDtypeStruct((STATE_ROWS, LANES), BF16), *rows_, s, d,
+    )
+    entering = lax.all_gather(entering, "sp_2")
     tp = lax.axis_size("tp")
     rows = TOK // tp
     tiles = small_call(
-        mix_kernel, "mix", (jax.ShapeDtypeStruct((rows, 4 * LANES), BF16),) * tp, inner, q_run,
-        entering, pieces, output_gate_logits, per_head_norm_gain.reshape(1, 64),
+        mix_kernel, "mix", (jax.ShapeDtypeStruct((rows, 4 * LANES), BF16),) * tp, narrow, narrow_q,
+        wide, wide_q, entering, pieces, output_gate_logits, per_head_norm_gain.reshape(1, 64),
         scratch=[pltpu.VMEM((TOK, 4 * LANES), BF16)],
     )
     width = stream.shape[1]
@@ -455,16 +543,10 @@
     hidden = (jax.nn.silu(gate) * up).astype(BF16)
     part = jnp.dot(hidden, expert_down_matrix[0], preferred_element_type=F32).astype(BF16)
     back = lax.all_to_all(part, SP_TP, 0, 0, tiled=True)
-    col = width // 4
     return pl.pallas_call(
         final_kernel,
-        grid=(4,),
-        in_specs=[
-            pl.BlockSpec((2 * rows, slots), lambda i: (0, 0)),
-            pl.BlockSpec((slots, col), lambda i: (0, i)),
-            pl.BlockSpec((rows, col), lambda i: (0, i)),
-        ],
-        out_specs=pl.BlockSpec((rows, col), lambda i: (0, i)),
+        in_specs=[VMEM] * 3,
+        out_specs=VMEM,
         out_shape=jax.ShapeDtypeStruct((rows, width), BF16),
         compiler_params=pltpu.CompilerParams(vmem_limit_bytes=12 * 2**20),
         name="combine",

time: 181 us -> 177 us (0.978)
  waiting for transfers between devices: 16.9 us -> 7.45 us
  Pallas kernels: 15.1 us -> 20.3 us
    ppermute x9, waiting for transfers between devices: 16.9 us -> 7.45 us  [from_each(): lax.ppermute(x if tiles is None else tiles[j], axis, [(i, (i + j) % count...]
    pallas_call x2 -> x4, Pallas kernels: 9.85 us -> 15.1 us  [the longest x3 13.7 us: from_hbm(): pl.pallas_call(kernel, out_shape=shapes, in_specs=[HBM] * len(inputs) + [...]
  transfers between devices with their start and end apart: 9 -> 9, of which waited for: 8 -> 5; matrix products, arithmetic and copies ran while one was open for 0% -> 0% of each run, Pallas kernels for 0% -> 5%
where the time goes in v3:
time: 177 us
  blocking collectives  121 us (68%)
  Pallas kernels  20.3 us (11%)
  matrix products  14.4 us (8%)
  starting transfers between devices  13.4 us (8%)
  waiting for transfers between devices  7.45 us (4%)
    all_to_all x1, blocking collectives, local(): tokens = lax.all_to_all(buffers, SP_TP, 0, 0, tiled=True)  58.8 us
    all_to_all x1, blocking collectives, local(): back = lax.all_to_all(part, SP_TP, 0, 0, tiled=True)  56.8 us
    pallas_call x3, Pallas kernels, from_hbm(): pl.pallas_call(kernel, out_shape=shapes, in_specs=[HBM] * len(inputs) + [...  13.7 us
    ppermute x9, starting transfers between devices, from_each(): lax.ppermute(x if tiles is None else tiles[j], axis, [(i, (i + j) % count...  13.4 us
    ppermute x9, waiting for transfers between devices, from_each(): lax.ppermute(x if tiles is None else tiles[j], axis, [(i, (i + j) % count...  7.45 us
    dot_general x1, matrix products, local(): up = jnp.dot(tokens, expert_up_matrix[0], preferred_element_type=F32)  5.14 us
    dot_general x1, matrix products, local(): jnp.dot(hidden, expert_down_matrix[0], preferred_element_type=F32)  4.75 us
    dot_general x1, matrix products, local(): gate = jnp.dot(tokens, expert_gate_matrix[0], preferred_element_type=F32)  4.54 us
  transfers between devices with their start and end apart: 9, of which 5 were waited for; matrix products, arithmetic and copies ran while one was open for 0% of the time, Pallas kernels for 5%

profile of v3, /device:TPU:1, one launch (start us, length us, event | category | flops | bytes accessed | tf_op | source)
XLA Modules:
  0.0 176.8 jit_solution(16445162727295211466)
XLA Ops:
  0.0 4.4 %local_states.1 = bf16[2,400,128]{2,1,0:T(8,128)(2,1)S(1)} custom-call(bf16[2,256,256]{2,1,0:T(8,128)(2,1)} %nf_hbm.3, f32[2,256]{1,0:T(2,128)} %nh_hbm.3, f32[2,4,256]{2,1,0:T(4,128)} %bitcast.41, bf16[256,2,256]{2,1,0:T(2,128)(2,1)} %v_hbm.5, bf16[2,256,512]{2,1,0:T(8,128)(2,1)} %wf_hbm.3, f32[2,512]{1,0:T(2,128)} %wh_hbm.3), custom_call_target="tpu_custom_call" | custom-call | flops 1000000000 | bytes 3145728 | tf_op jit(solution)/shard_map/local_states/pallas_call | solution.py:464
  4.4 3.1 %all-gather = bf16[4,400,128]{2,1,0:T(8,128)(2,1)S(1)} all-gather(bf16[2,400,128]{2,1,0:T(8,128)(2,1)S(1)} %local_states.1), channel_id=2, replica_groups=mesh['sp_0'=4,'sp_1'=4,'sp_2'=2,'tp'=4] {'sp_2'}, dimensions={0}, use_global_device_ids=true | all-gather | bytes 614400 | tf_op jit(solution)/shard_map/all_gather | solution.py:490
  7.5 2.9 %collective-permute-start.2 = (bf16[400,128]{1,0:T(8,128)(2,1)S(1)}, bf16[400,128]{1,0:T(8,128)(2,1)S(1)}, u32[]{:S(2)}, u32[]{:S(2)}) collective-permute-start(bf16[400,128]{1,0:T(8,128)(2,1)S(1)} %pair.1.after_ref.refs_1_), channel_id=1, source_target_pairs={{0,24},{8,0},{16,8},{24,16},{1,25},{9,1},{17,9},{25,17},{2,26},{10... | collective-permute-start | bytes 307208 | tf_op jit(solution)/shard_map/ppermute | solution.py:304
  10.8 0.7 collective-permute-start
  11.5 5.4 %wide_outputs.1 = (f32[2,256,128]{2,1,0:T(8,128)S(1)}, bf16[4,256,256]{2,1,0:T(8,128)(2,1)S(1)}, f32[8,128]{1,0:T(8,128)S(1)}) custom-call(bf16[2,256,512]{2,1,0:T(8,128)(2,1)} %wf_hbm.3, f32[2,512]{1,0:T(2,128)} %wh_hbm.3, f32[2,4,256]{2,1,0:T(4,128)} %bitcast.42, bf16[256,2,256]{2,1,0:T(2,128)(2,1)} %v_hbm.5, bf16[256,512]{1,0:T(8,128)(2,1)} %wq_hbm.1, ...), custom_call_target="tpu_custom_call" | custom-call | flops 3000000000 | bytes 3145728 | tf_op jit(solution)/shard_map/wide_outputs/pallas_call | solution.py:464
  16.9 2.0 %collective-permute-done.refs_2_ = bf16[400,128]{1,0:T(8,128)(2,1)S(1)} collective-permute-done((bf16[400,128]{1,0:T(8,128)(2,1)S(1)}, bf16[400,128]{1,0:T(8,128)(2,1)S(1)}, u32[]{:S(2)}, u32[]{:S(2)}) %collective-permute-start) | collective-permute-done | bytes 102432 | tf_op jit(solution)/shard_map/ppermute | solution.py:304
  19.1 3.8 %collective-permute-start.5 = (bf16[400,128]{1,0:T(8,128)(2,1)S(1)}, bf16[400,128]{1,0:T(8,128)(2,1)S(1)}, u32[]{:S(2)}, u32[]{:S(2)}) collective-permute-start(bf16[400,128]{1,0:T(8,128)(2,1)S(1)} %get-tuple-element.27.refs_0_), channel_id=1, source_target_pairs={{0,96},{32,0},{64,32},{96,64},{1,97},{33,1},{65,33},{97,65},{2,98}... | collective-permute-start | bytes 307208 | tf_op jit(solution)/shard_map/ppermute | solution.py:304
  22.9 0.7 collective-permute-start.3
  23.6 3.9 %narrow_outputs.1 = (f32[2,256,128]{2,1,0:T(8,128)S(1)}, bf16[2,256,256]{2,1,0:T(8,128)(2,1)S(1)}, bf16[2,1024,2048]{2,1,0:T(8,128)(2,1)S(1)}) custom-call(bf16[2,256,256]{2,1,0:T(8,128)(2,1)} %nf_hbm.3, f32[2,256]{1,0:T(2,128)} %nh_hbm.3, f32[2,4,256]{2,1,0:T(4,128)} %bitcast.43, bf16[256,2,256]{2,1,0:T(2,128)(2,1)} %v_hbm.5, bf16[256,256]{1,0:T(8,128)(2,1)} %nq_hbm.1, ...), custom_call_target="tpu_custom_call" | custom-call | flops 3000000000 | bytes 3145728 | tf_op jit(solution)/shard_map/narrow_outputs/pallas_call | solution.py:464
  28.0 2.8 %collective-permute-done.3.refs_1_ = bf16[400,128]{1,0:T(8,128)(2,1)S(1)} collective-permute-done((bf16[400,128]{1,0:T(8,128)(2,1)S(1)}, bf16[400,128]{1,0:T(8,128)(2,1)S(1)}, u32[]{:S(2)}, u32[]{:S(2)}) %collective-permute-start.3) | collective-permute-done | bytes 102432 | tf_op jit(solution)/shard_map/ppermute | solution.py:304
  30.9 2.4 %all-gather.1 = bf16[768,128]{1,0:T(8,128)(2,1)S(1)} all-gather(bf16[384,128]{1,0:T(8,128)(2,1)S(1)} %level_0.1), channel_id=3, replica_groups=mesh['sp_0'=4,'sp_1'=4,'sp_2'=2,'tp'=4] {'sp_2'}, dimensions={0}, use_global_device_ids=true | all-gather | bytes 294912 | tf_op jit(solution)/shard_map/all_gather | solution.py:511
  33.3 1.9 %mix.1 = (bf16[64,512]{1,0:T(8,128)(2,1)S(1)}, bf16[64,512]{1,0:T(8,128)(2,1)S(1)}, bf16[64,512]{1,0:T(8,128)(2,1)S(1)}, bf16[64,512]{1,0:T(8,128)(2,1)S(1)}) custom-call(f32[2,256,128]{2,1,0:T(8,128)S(1)} %get-tuple-element.23.n_out_ref, bf16[2,256,256]{2,1,0:T(8,128)(2,1)S(1)} %get-tuple-element.24.n_qr_ref, ...), custom_call_target="tpu_custom_call" | custom-call | tf_op jit(solution)/shard_map/mix/pallas_call | solution.py:318
  35.2 1.3 collective-permute-start.6
  36.5 2.4 %collective-permute-start.7 = (bf16[64,512]{1,0:T(8,128)(2,1)S(1)}, bf16[64,512]{1,0:T(8,128)(2,1)S(1)}, u32[]{:S(2)}, u32[]{:S(2)}) collective-permute-start(bf16[64,512]{1,0:T(8,128)(2,1)S(1)} %get-tuple-element.31), channel_id=1, source_target_pairs={{0,2},{1,3},{2,0},{3,1},{4,6},{5,7},{6,4},{7,5},{8,10},{9,11},{10,... | collective-permute-start | bytes 196616 | tf_op jit(solution)/shard_map/ppermute | solution.py:304
  38.9 1.2 collective-permute-start.8
  40.1 1.8 %collective-permute-done.7.x2_ref = bf16[64,512]{1,0:T(8,128)(2,1)S(1)} collective-permute-done((bf16[64,512]{1,0:T(8,128)(2,1)S(1)}, bf16[64,512]{1,0:T(8,128)(2,1)S(1)}, u32[]{:S(2)}, u32[]{:S(2)}) %collective-permute-start.7) | collective-permute-done | bytes 65568 | tf_op jit(solution)/shard_map/ppermute | solution.py:304
  41.9 0.5 collective-permute-done.8.x3_ref
  42.4 2.9 %project_and_route.1 = (f32[64,2048]{1,0:T(8,128)S(1)}, bf16[1024,2048]{1,0:T(8,128)(2,1)S(1)}, bf16[128,1024]{1,0:T(8,128)(2,1)S(1)}) custom-call(bf16[64,512]{1,0:T(8,128)(2,1)S(1)} %get-tuple-element.29.x0_ref, bf16[64,512]{1,0:T(8,128)(2,1)S(1)} %collective-permute-done.6.x1_ref, bf16[64,512]{1,0:T(8,128)(2,1)S(1)} %collective-permute-done.7.x2_ref, ...), custom_call_target="tpu_custom_call" | custom-call | tf_op jit(solution)/shard_map/project_and_route/pallas_call | solution.py:524
  45.3 58.8 %all_to_all.23 = bf16[128,8,2048]{2,1,0:T(8,128)(2,1)S(1)} all-to-all(bf16[128,8,2048]{2,1,0:T(8,128)(2,1)S(1)} %bitcast.33), channel_id=1, replica_groups=mesh['sp_0'=4,'sp_1'=4,'sp_2'=2,'tp'=4] {'sp_0','sp_1','sp_2','tp'}, dimensions={0} | all-to-all | bytes 8388608 | tf_op jit(solution)/shard_map/all_to_all | solution.py:540
  104.1 4.5 %fusion.4 = f32[1024,1024]{1,0:T(8,128)S(1)} fusion(bf16[1,2048,1024]{2,1,0:T(8,128)(2,1)S(1)} %copy-done.6, bf16[128,8,2048]{2,1,0:T(8,128)(2,1)S(1)} %all_to_all.23), kind=kOutput, calls=%fused_computation.4 | convolution fusion | flops 4294967296 | bytes 12582912 | tf_op jit(solution)/shard_map/dot_general | solution.py:541
  108.7 5.1 %multiply_convert_fusion = bf16[1024,1024]{1,0:T(8,128)(2,1)S(1)} fusion(f32[1024,1024]{1,0:T(8,128)S(1)} %fusion.4, bf16[1,2048,1024]{2,1,0:T(8,128)(2,1)S(1)} %copy-done.7, bf16[128,8,2048]{2,1,0:T(8,128)(2,1)S(1)} %all_to_all.23), kind=kOutput, calls=%fused_computation.9 | convolution fusion | flops 4301258752 | bytes 14680064 | tf_op jit(solution)/shard_map/dot_general | solution.py:542
  113.9 4.8 %convert_bitcast_fusion = bf16[128,8,2048]{2,1,0:T(8,128)(2,1)S(1)} fusion(bf16[1024,1024]{1,0:T(8,128)(2,1)S(1)} %multiply_convert_fusion, bf16[1,1024,2048]{2,1,0:T(8,128)(2,1)S(1)} %copy-done.8), kind=kOutput, calls=%fused_computation.8 | convolution fusion | flops 4297064448 | bytes 10485760 | tf_op jit(solution)/shard_map/dot_general | solution.py:544
  118.6 56.8 %all_to_all.24 = bf16[128,8,2048]{2,1,0:T(8,128)(2,1)S(1)} all-to-all(bf16[128,8,2048]{2,1,0:T(8,128)(2,1)S(1)} %convert_bitcast_fusion), channel_id=1, replica_groups=mesh['sp_0'=4,'sp_1'=4,'sp_2'=2,'tp'=4] {'sp_0','sp_1','sp_2','tp'}, dimensions={0} | all-to-all | bytes 8388608 | tf_op jit(solution)/shard_map/all_to_all | solution.py:545
  175.4 1.4 combine.1
  (28 shorter events, 1.2 us)
Async XLA Ops:
  7.5 9.3 %collective-permute-start.2 = (bf16[400,128]{1,0:T(8,128)(2,1)S(1)}, bf16[400,128]{1,0:T(8,128)(2,1)S(1)}, u32[]{:S(2)}, u32[]{:S(2)}) collective-permute-start(bf16[400,128]{1,0:T(8,128)(2,1)S(1)} %pair.1.after_ref.refs_1_), channel_id=1, source_target_pairs={{0,24},{8,0},{16,8},{24,16},{1,25},{9,1},{17,9},{25,17},{2,26},{10... | collective-permute-start | bytes 307208 | tf_op jit(solution)/shard_map/ppermute | solution.py:304
  10.5 6.4 %collective-permute-start.1 = (bf16[400,128]{1,0:T(8,128)(2,1)S(1)}, bf16[400,128]{1,0:T(8,128)(2,1)S(1)}, u32[]{:S(2)}, u32[]{:S(2)}) collective-permute-start(bf16[400,128]{1,0:T(8,128)(2,1)S(1)} %pair.1.after_ref.refs_1_), channel_id=1, source_target_pairs={{0,16},{8,24},{16,0},{24,8},{1,17},{9,25},{17,1},{25,9},{2,18},{10... | collective-permute-start | bytes 307208 | tf_op jit(solution)/shard_map/ppermute | solution.py:304
  10.8 8.1 %collective-permute-start = (bf16[400,128]{1,0:T(8,128)(2,1)S(1)}, bf16[400,128]{1,0:T(8,128)(2,1)S(1)}, u32[]{:S(2)}, u32[]{:S(2)}) collective-permute-start(bf16[400,128]{1,0:T(8,128)(2,1)S(1)} %pair.1.after_ref.refs_1_), channel_id=1, source_target_pairs={{0,8},{8,16},{16,24},{24,0},{1,9},{9,17},{17,25},{25,1},{2,10},{10... | collective-permute-start | bytes 307208 | tf_op jit(solution)/shard_map/ppermute | solution.py:304
  19.1 8.5 %collective-permute-start.5 = (bf16[400,128]{1,0:T(8,128)(2,1)S(1)}, bf16[400,128]{1,0:T(8,128)(2,1)S(1)}, u32[]{:S(2)}, u32[]{:S(2)}) collective-permute-start(bf16[400,128]{1,0:T(8,128)(2,1)S(1)} %get-tuple-element.27.refs_0_), channel_id=1, source_target_pairs={{0,96},{32,0},{64,32},{96,64},{1,97},{33,1},{65,33},{97,65},{2,98}... | collective-permute-start | bytes 307208 | tf_op jit(solution)/shard_map/ppermute | solution.py:304
  22.9 5.1 %collective-permute-start.4 = (bf16[400,128]{1,0:T(8,128)(2,1)S(1)}, bf16[400,128]{1,0:T(8,128)(2,1)S(1)}, u32[]{:S(2)}, u32[]{:S(2)}) collective-permute-start(bf16[400,128]{1,0:T(8,128)(2,1)S(1)} %get-tuple-element.27.refs_0_), channel_id=1, source_target_pairs={{0,64},{32,96},{64,0},{96,32},{1,65},{33,97},{65,1},{97,33},{2,66}... | collective-permute-start | bytes 307208 | tf_op jit(solution)/shard_map/ppermute | solution.py:304
  22.9 7.9 %collective-permute-start.3 = (bf16[400,128]{1,0:T(8,128)(2,1)S(1)}, bf16[400,128]{1,0:T(8,128)(2,1)S(1)}, u32[]{:S(2)}, u32[]{:S(2)}) collective-permute-start(bf16[400,128]{1,0:T(8,128)(2,1)S(1)} %get-tuple-element.27.refs_0_), channel_id=1, source_target_pairs={{0,32},{32,64},{64,96},{96,0},{1,33},{33,65},{65,97},{97,1},{2,34}... | collective-permute-start | bytes 307208 | tf_op jit(solution)/shard_map/ppermute | solution.py:304
  23.6 9.7 %copy-start.1 = (bf16[256,2,256]{2,1,0:T(2,128)(2,1)S(1)}, bf16[256,2,256]{2,1,0:T(2,128)(2,1)}, u32[]{:S(2)}) copy-start(bf16[256,2,256]{2,1,0:T(2,128)(2,1)} %gate_ref.1) | copy-start | bytes 786436
  23.6 9.7 %copy-start.5 = (f32[64]{0:T(128)S(1)}, f32[64]{0:T(128)}, u32[]{:S(2)}) copy-start(f32[64]{0:T(128)} %param.28) | copy-start | bytes 772
  23.6 18.7 %copy-start = (bf16[256,2048]{1,0:T(8,128)(2,1)S(1)}, bf16[256,2048]{1,0:T(8,128)(2,1)}, u32[]{:S(2)}) copy-start(bf16[256,2048]{1,0:T(8,128)(2,1)} %stream_ref.1) | copy-start | bytes 3145732
  23.6 18.7 %copy-start.2 = (f32[2048]{0:T(1024)S(1)}, f32[2048]{0:T(1024)}, u32[]{:S(2)}) copy-start(f32[2048]{0:T(1024)} %param.30) | copy-start | bytes 24580
  23.6 18.7 %copy-start.3 = (s32[256,2]{0,1:T(2,128)S(1)}, s32[256,2]{0,1:T(2,128)}, u32[]{:S(2)}) copy-start(s32[256,2]{0,1:T(2,128)} %param.34) | copy-start | bytes 6148
  23.6 18.7 %copy-start.4 = (f32[256,2]{0,1:T(2,128)S(1)}, f32[256,2]{0,1:T(2,128)}, u32[]{:S(2)}) copy-start(f32[256,2]{0,1:T(2,128)} %param.35) | copy-start | bytes 6148
  35.2 4.9 %collective-permute-start.6 = (bf16[64,512]{1,0:T(8,128)(2,1)S(1)}, bf16[64,512]{1,0:T(8,128)(2,1)S(1)}, u32[]{:S(2)}, u32[]{:S(2)}) collective-permute-start(bf16[64,512]{1,0:T(8,128)(2,1)S(1)} %get-tuple-element.30), channel_id=1, source_target_pairs={{0,1},{1,2},{2,3},{3,0},{4,5},{5,6},{6,7},{7,4},{8,9},{9,10},{10,1... | collective-permute-start | bytes 196616 | tf_op jit(solution)/shard_map/ppermute | solution.py:304
  36.5 5.4 %collective-permute-start.7 = (bf16[64,512]{1,0:T(8,128)(2,1)S(1)}, bf16[64,512]{1,0:T(8,128)(2,1)S(1)}, u32[]{:S(2)}, u32[]{:S(2)}) collective-permute-start(bf16[64,512]{1,0:T(8,128)(2,1)S(1)} %get-tuple-element.31), channel_id=1, source_target_pairs={{0,2},{1,3},{2,0},{3,1},{4,6},{5,7},{6,4},{7,5},{8,10},{9,11},{10,... | collective-permute-start | bytes 196616 | tf_op jit(solution)/shard_map/ppermute | solution.py:304
  38.9 3.4 %collective-permute-start.8 = (bf16[64,512]{1,0:T(8,128)(2,1)S(1)}, bf16[64,512]{1,0:T(8,128)(2,1)S(1)}, u32[]{:S(2)}, u32[]{:S(2)}) collective-permute-start(bf16[64,512]{1,0:T(8,128)(2,1)S(1)} %get-tuple-element.32), channel_id=1, source_target_pairs={{0,3},{1,0},{2,1},{3,2},{4,7},{5,4},{6,5},{7,6},{8,11},{9,8},{10,9... | collective-permute-start | bytes 196616 | tf_op jit(solution)/shard_map/ppermute | solution.py:304
  45.3 58.8 %copy-start.6 = (bf16[1,2048,1024]{2,1,0:T(8,128)(2,1)S(1)}, bf16[1,2048,1024]{2,1,0:T(8,128)(2,1)}, u32[]{:S(2)}) copy-start(bf16[1,2048,1024]{2,1,0:T(8,128)(2,1)} %param.31) | copy-start | bytes 12582916
  104.1 4.6 %copy-start.7 = (bf16[1,2048,1024]{2,1,0:T(8,128)(2,1)S(1)}, bf16[1,2048,1024]{2,1,0:T(8,128)(2,1)}, u32[]{:S(2)}) copy-start(bf16[1,2048,1024]{2,1,0:T(8,128)(2,1)} %param.32) | copy-start | bytes 12582916
  108.7 5.2 %copy-start.8 = (bf16[1,1024,2048]{2,1,0:T(8,128)(2,1)S(1)}, bf16[1,1024,2048]{2,1,0:T(8,128)(2,1)}, u32[]{:S(2)}) copy-start(bf16[1,1024,2048]{2,1,0:T(8,128)(2,1)} %param.33) | copy-start | bytes 12582916

commit v4 on v3

--- a/solution.py
+++ b/solution.py
@@ -314,13 +314,14 @@
     return pltpu.with_memory_space_constraint(x, pltpu.HBM)
 
 
-def small_call(kernel, name, shapes, *arrays, scratch=()):
+def small_call(kernel, name, shapes, *arrays, scratch=(), flops=0):
     return pl.pallas_call(
         kernel,
         out_shape=shapes,
         in_specs=[VMEM] * len(arrays),
         out_specs=jax.tree.map(lambda _: VMEM, shapes),
         scratch_shapes=scratch,
+        cost_estimate=pl.CostEstimate(flops=flops, bytes_accessed=2**20, transcendentals=0),
         compiler_params=pltpu.CompilerParams(vmem_limit_bytes=8 * 2**20),
         name=name,
     )(*arrays)
@@ -389,28 +390,14 @@
     return own[0] * capacity + rank0, own[1] * capacity + rank1
 
 
-def route_kernel(
-    experts, capacity, copies, x0_ref, x1_ref, x2_ref, x3_ref, w_ref, stream_ref, gain_ref,
-    routes_ref, score_ref, res_ref, buf_ref, pick_ref, table_ref,
-):
-    rows, width = res_ref.shape
-    here = lax.axis_index("tp")
-    own = pl.ds(here * rows, rows)
-    residual = stream_ref[own, :].astype(F32)
-    span = 2 * LANES
-    for j, x_ref in enumerate((x0_ref, x1_ref, x2_ref, x3_ref)):
-        source = lax.rem(here + copies - j, copies)
-        for g in range(2):
-            part = x_ref[:, g * span : (g + 1) * span]
-            residual = residual + dot(part, w_ref[g, pl.ds(source * span, span), :])
-    res_ref[...] = residual
-    mean = jnp.mean(residual * residual, axis=-1, keepdims=True)
-    norm = (residual * lax.rsqrt(mean + EPS) * gain_ref[...]).astype(BF16)
+def picks_kernel(experts, capacity, copies, routes_ref, score_ref, after_ref, pick_ref, chosen_ref, table_ref):
+    del after_ref
+    rows = chosen_ref.shape[1]
     table = jnp.concatenate(
         [routes_ref[...].astype(F32), score_ref[...], jnp.zeros((4, routes_ref.shape[1]), F32)], axis=0
     )
     table_ref[...] = jnp.transpose(table)
-    table = table_ref[own, :]
+    table = table_ref[pl.ds(lax.axis_index("tp") * rows, rows), :]
     table_t = jnp.transpose(table)
     col = [table[:, k : k + 1].astype(jnp.int32) for k in range(2)]
     row = [table_t[k : k + 1, :].astype(jnp.int32) for k in range(2)]
@@ -424,8 +411,30 @@
     high = pick.astype(BF16)
     pick_ref[:rows, :] = high
     pick_ref[rows:, :] = (pick - high.astype(F32)).astype(BF16)
-    chosen = jnp.transpose(jnp.where(hits[0] | hits[1], 1.0, 0.0)).astype(BF16)
-    buf_ref[...] = dot(chosen, norm).astype(BF16)
+    j = lax.broadcasted_iota(jnp.int32, (rows, experts * capacity), 1)
+    chosen = jnp.where((j == slots[0]) | (j == slots[1]), 1.0, 0.0)
+    chosen_ref[...] = jnp.transpose(chosen).astype(BF16)
+
+
+def route_kernel(
+    x0_ref, x1_ref, x2_ref, x3_ref, w_ref, stream_ref, gain_ref, chosen_ref, res_ref, buf_ref
+):
+    rows, width = res_ref.shape
+    experts, copies, capacity, _ = buf_ref.shape
+    here = lax.axis_index("tp")
+    residual = stream_ref[pl.ds(here * rows, rows), :].astype(F32)
+    span = 2 * LANES
+    for j, x_ref in enumerate((x0_ref, x1_ref, x2_ref, x3_ref)):
+        source = lax.rem(here + copies - j, copies)
+        for g in range(2):
+            part = x_ref[:, g * span : (g + 1) * span]
+            residual = residual + dot(part, w_ref[g, pl.ds(source * span, span), :])
+    res_ref[...] = residual
+    mean = jnp.mean(residual * residual, axis=-1, keepdims=True)
+    norm = (residual * lax.rsqrt(mean + EPS) * gain_ref[...]).astype(BF16)
+    sent = dot(chosen_ref[...], norm).astype(BF16).reshape(experts, capacity, width)
+    for t in range(copies):
+        buf_ref[:, t] = sent
 
 
 def final_kernel(pick_ref, back_ref, res_ref, o_ref):
@@ -520,23 +529,30 @@
     experts = lax.axis_size(SP)
     capacity = max(2, 2 * routes.shape[1] * rows // experts)
     slots = experts * tp * capacity
+    pick, chosen = small_call(
+        partial(picks_kernel, experts, capacity, tp), "picks",
+        (
+            jax.ShapeDtypeStruct((2 * rows, slots), BF16),
+            jax.ShapeDtypeStruct((experts * capacity, rows), BF16),
+        ),
+        routes.T, router_scores_chosen.T, d, scratch=[pltpu.VMEM((TOK, 8), F32)],
+        flops=10**9,
+    )
     arrived = [tiles[0]] + from_each(None, "tp", tiles)
-    residual, buffers, pick = pl.pallas_call(
-        partial(route_kernel, experts, capacity, tp),
+    residual, buffers = pl.pallas_call(
+        route_kernel,
         out_shape=(
             jax.ShapeDtypeStruct((rows, width), F32),
-            jax.ShapeDtypeStruct((slots, width), BF16),
-            jax.ShapeDtypeStruct((2 * rows, slots), BF16),
+            jax.ShapeDtypeStruct((experts, tp, capacity, width), BF16),
         ),
-        in_specs=[VMEM] * 9,
-        out_specs=(VMEM,) * 3,
-        scratch_shapes=[pltpu.VMEM((TOK, 8), F32)],
-        compiler_params=pltpu.CompilerParams(vmem_limit_bytes=24 * 2**20),
+        in_specs=[VMEM] * 8,
+        out_specs=(VMEM,) * 2,
+        compiler_params=pltpu.CompilerParams(vmem_limit_bytes=20 * 2**20),
         name="project_and_route",
     )(
-        *arrived, mixer_weight, stream, feedforward_norm_gain.reshape(1, width),
-        routes.T, router_scores_chosen.T,
-    )
+        *arrived, mixer_weight, stream, feedforward_norm_gain.reshape(1, width), chosen,
+    )
+    buffers = buffers.reshape(slots, width)
     tokens = lax.all_to_all(buffers, SP_TP, 0, 0, tiled=True)
     gate = jnp.dot(tokens, expert_gate_matrix[0], preferred_element_type=F32)
     up = jnp.dot(tokens, expert_up_matrix[0], preferred_element_type=F32)

time: 177 us -> 176 us (level)
  transfers between devices with their start and end apart: 9 -> 9, of which waited for: 5 -> 5; matrix products, arithmetic and copies ran while one was open for 0% -> 0% of each run, Pallas kernels for 5% -> 6%
where the time goes in v4:
time: 176 us
  blocking collectives  121 us (69%)
  Pallas kernels  20 us (11%)
  matrix products  14.4 us (8%)
  starting transfers between devices  13.4 us (8%)
  waiting for transfers between devices  6.92 us (4%)
    all_to_all x1, blocking collectives, local(): tokens = lax.all_to_all(buffers, SP_TP, 0, 0, tiled=True)  58.8 us
    all_to_all x1, blocking collectives, local(): back = lax.all_to_all(part, SP_TP, 0, 0, tiled=True)  56.8 us
    pallas_call x3, Pallas kernels, from_hbm(): pl.pallas_call(kernel, out_shape=shapes, in_specs=[HBM] * len(inputs) + [...  13.7 us
    ppermute x9, starting transfers between devices, from_each(): lax.ppermute(x if tiles is None else tiles[j], axis, [(i, (i + j) % count...  13.4 us
    ppermute x9, waiting for transfers between devices, from_each(): lax.ppermute(x if tiles is None else tiles[j], axis, [(i, (i + j) % count...  6.92 us
    dot_general x1, matrix products, local(): up = jnp.dot(tokens, expert_up_matrix[0], preferred_element_type=F32)  5.2 us
    dot_general x1, matrix products, local(): jnp.dot(hidden, expert_down_matrix[0], preferred_element_type=F32)  4.73 us
    dot_general x1, matrix products, local(): gate = jnp.dot(tokens, expert_gate_matrix[0], preferred_element_type=F32)  4.49 us
  transfers between devices with their start and end apart: 9, of which 5 were waited for; matrix products, arithmetic and copies ran while one was open for 0% of the time, Pallas kernels for 6%

profile of v4, /device:TPU:1, one launch (start us, length us, event | category | flops | bytes accessed | tf_op | source)
XLA Modules:
  0.0 176.0 jit_solution(12739216871792508568)
XLA Ops:
  0.0 4.4 %local_states.1 = bf16[2,400,128]{2,1,0:T(8,128)(2,1)S(1)} custom-call(bf16[2,256,256]{2,1,0:T(8,128)(2,1)} %nf_hbm.3, f32[2,256]{1,0:T(2,128)} %nh_hbm.3, f32[2,4,256]{2,1,0:T(4,128)} %bitcast.41, bf16[256,2,256]{2,1,0:T(2,128)(2,1)} %v_hbm.5, bf16[2,256,512]{2,1,0:T(8,128)(2,1)} %wf_hbm.3, f32[2,512]{1,0:T(2,128)} %wh_hbm.3), custom_call_target="tpu_custom_call" | custom-call | flops 1000000000 | bytes 3145728 | tf_op jit(solution)/shard_map/local_states/pallas_call | solution.py:473
  4.4 3.1 %all-gather = bf16[4,400,128]{2,1,0:T(8,128)(2,1)S(1)} all-gather(bf16[2,400,128]{2,1,0:T(8,128)(2,1)S(1)} %local_states.1), channel_id=2, replica_groups=mesh['sp_0'=4,'sp_1'=4,'sp_2'=2,'tp'=4] {'sp_2'}, dimensions={0}, use_global_device_ids=true | all-gather | bytes 614400 | tf_op jit(solution)/shard_map/all_gather | solution.py:499
  7.5 2.9 %collective-permute-start.2 = (bf16[400,128]{1,0:T(8,128)(2,1)S(1)}, bf16[400,128]{1,0:T(8,128)(2,1)S(1)}, u32[]{:S(2)}, u32[]{:S(2)}) collective-permute-start(bf16[400,128]{1,0:T(8,128)(2,1)S(1)} %pair.1.after_ref.refs_1_), channel_id=1, source_target_pairs={{0,24},{8,0},{16,8},{24,16},{1,25},{9,1},{17,9},{25,17},{2,26},{10... | collective-permute-start | bytes 307208 | tf_op jit(solution)/shard_map/ppermute | solution.py:304
  10.8 0.7 collective-permute-start
  11.5 5.4 %wide_outputs.1 = (f32[2,256,128]{2,1,0:T(8,128)S(1)}, bf16[4,256,256]{2,1,0:T(8,128)(2,1)S(1)}, f32[8,128]{1,0:T(8,128)S(1)}) custom-call(bf16[2,256,512]{2,1,0:T(8,128)(2,1)} %wf_hbm.3, f32[2,512]{1,0:T(2,128)} %wh_hbm.3, f32[2,4,256]{2,1,0:T(4,128)} %bitcast.42, bf16[256,2,256]{2,1,0:T(2,128)(2,1)} %v_hbm.5, bf16[256,512]{1,0:T(8,128)(2,1)} %wq_hbm.1, ...), custom_call_target="tpu_custom_call" | custom-call | flops 3000000000 | bytes 3145728 | tf_op jit(solution)/shard_map/wide_outputs/pallas_call | solution.py:473
  16.9 2.0 %collective-permute-done.refs_2_ = bf16[400,128]{1,0:T(8,128)(2,1)S(1)} collective-permute-done((bf16[400,128]{1,0:T(8,128)(2,1)S(1)}, bf16[400,128]{1,0:T(8,128)(2,1)S(1)}, u32[]{:S(2)}, u32[]{:S(2)}) %collective-permute-start) | collective-permute-done | bytes 102432 | tf_op jit(solution)/shard_map/ppermute | solution.py:304
  19.1 3.8 %collective-permute-start.5 = (bf16[400,128]{1,0:T(8,128)(2,1)S(1)}, bf16[400,128]{1,0:T(8,128)(2,1)S(1)}, u32[]{:S(2)}, u32[]{:S(2)}) collective-permute-start(bf16[400,128]{1,0:T(8,128)(2,1)S(1)} %get-tuple-element.29.refs_0_), channel_id=1, source_target_pairs={{0,96},{32,0},{64,32},{96,64},{1,97},{33,1},{65,33},{97,65},{2,98}... | collective-permute-start | bytes 307208 | tf_op jit(solution)/shard_map/ppermute | solution.py:304
  22.9 0.7 collective-permute-start.3
  23.6 3.9 %narrow_outputs.1 = (f32[2,256,128]{2,1,0:T(8,128)S(1)}, bf16[2,256,256]{2,1,0:T(8,128)(2,1)S(1)}, bf16[2,1024,2048]{2,1,0:T(8,128)(2,1)S(1)}) custom-call(bf16[2,256,256]{2,1,0:T(8,128)(2,1)} %nf_hbm.3, f32[2,256]{1,0:T(2,128)} %nh_hbm.3, f32[2,4,256]{2,1,0:T(4,128)} %bitcast.43, bf16[256,2,256]{2,1,0:T(2,128)(2,1)} %v_hbm.5, bf16[256,256]{1,0:T(8,128)(2,1)} %nq_hbm.1, ...), custom_call_target="tpu_custom_call" | custom-call | flops 3000000000 | bytes 3145728 | tf_op jit(solution)/shard_map/narrow_outputs/pallas_call | solution.py:473
  28.0 2.8 %collective-permute-done.3.refs_1_ = bf16[400,128]{1,0:T(8,128)(2,1)S(1)} collective-permute-done((bf16[400,128]{1,0:T(8,128)(2,1)S(1)}, bf16[400,128]{1,0:T(8,128)(2,1)S(1)}, u32[]{:S(2)}, u32[]{:S(2)}) %collective-permute-start.3) | collective-permute-done | bytes 102432 | tf_op jit(solution)/shard_map/ppermute | solution.py:304
  30.9 2.4 %all-gather.1 = bf16[768,128]{1,0:T(8,128)(2,1)S(1)} all-gather(bf16[384,128]{1,0:T(8,128)(2,1)S(1)} %level_0.1), channel_id=3, replica_groups=mesh['sp_0'=4,'sp_1'=4,'sp_2'=2,'tp'=4] {'sp_2'}, dimensions={0}, use_global_device_ids=true | all-gather | bytes 294912 | tf_op jit(solution)/shard_map/all_gather | solution.py:520
  33.3 1.9 %mix.1 = (bf16[64,512]{1,0:T(8,128)(2,1)S(1)}, bf16[64,512]{1,0:T(8,128)(2,1)S(1)}, bf16[64,512]{1,0:T(8,128)(2,1)S(1)}, bf16[64,512]{1,0:T(8,128)(2,1)S(1)}) custom-call(f32[2,256,128]{2,1,0:T(8,128)S(1)} %get-tuple-element.25.n_out_ref, bf16[2,256,256]{2,1,0:T(8,128)(2,1)S(1)} %get-tuple-element.26.n_qr_ref, ...), custom_call_target="tpu_custom_call" | custom-call | bytes 1048576 | tf_op jit(solution)/shard_map/mix/pallas_call | solution.py:318
  35.2 1.3 collective-permute-start.6
  36.5 2.4 %collective-permute-start.7 = (bf16[64,512]{1,0:T(8,128)(2,1)S(1)}, bf16[64,512]{1,0:T(8,128)(2,1)S(1)}, u32[]{:S(2)}, u32[]{:S(2)}) collective-permute-start(bf16[64,512]{1,0:T(8,128)(2,1)S(1)} %get-tuple-element.33), channel_id=1, source_target_pairs={{0,2},{1,3},{2,0},{3,1},{4,6},{5,7},{6,4},{7,5},{8,10},{9,11},{10,... | collective-permute-start | bytes 196616 | tf_op jit(solution)/shard_map/ppermute | solution.py:304
  38.9 1.2 collective-permute-start.8
  40.1 0.6 picks.1
  40.7 1.2 collective-permute-done.7.x2_ref
  42.3 2.1 %project_and_route.1 = (f32[64,2048]{1,0:T(8,128)S(1)}, bf16[32,4,8,2048]{3,2,1,0:T(8,128)(2,1)S(1)}) custom-call(bf16[64,512]{1,0:T(8,128)(2,1)S(1)} %get-tuple-element.31.x0_ref, bf16[64,512]{1,0:T(8,128)(2,1)S(1)} %collective-permute-done.6.x1_ref, bf16[64,512]{1,0:T(8,128)(2,1)S(1)} %collective-permute-done.7.x2_ref, ...), custom_call_target="tpu_custom_call" | custom-call | tf_op jit(solution)/shard_map/project_and_route/pallas_call | solution.py:542
  44.5 58.8 %all_to_all.23 = bf16[128,8,2048]{2,1,0:T(8,128)(2,1)S(1)} all-to-all(bf16[128,8,2048]{2,1,0:T(8,128)(2,1)S(1)} %bitcast.33), channel_id=1, replica_groups=mesh['sp_0'=4,'sp_1'=4,'sp_2'=2,'tp'=4] {'sp_0','sp_1','sp_2','tp'}, dimensions={0} | all-to-all | bytes 8388608 | tf_op jit(solution)/shard_map/all_to_all | solution.py:556
  103.3 4.5 %fusion.4 = f32[1024,1024]{1,0:T(8,128)S(1)} fusion(bf16[1,2048,1024]{2,1,0:T(8,128)(2,1)S(1)} %copy-done.6, bf16[128,8,2048]{2,1,0:T(8,128)(2,1)S(1)} %all_to_all.23), kind=kOutput, calls=%fused_computation.4 | convolution fusion | flops 4294967296 | bytes 12582912 | tf_op jit(solution)/shard_map/dot_general | solution.py:557
  107.8 5.2 %multiply_convert_fusion = bf16[1024,1024]{1,0:T(8,128)(2,1)S(1)} fusion(f32[1024,1024]{1,0:T(8,128)S(1)} %fusion.4, bf16[1,2048,1024]{2,1,0:T(8,128)(2,1)S(1)} %copy-done.7, bf16[128,8,2048]{2,1,0:T(8,128)(2,1)S(1)} %all_to_all.23), kind=kOutput, calls=%fused_computation.9 | convolution fusion | flops 4301258752 | bytes 14680064 | tf_op jit(solution)/shard_map/dot_general | solution.py:558
  113.0 4.7 %convert_bitcast_fusion = bf16[128,8,2048]{2,1,0:T(8,128)(2,1)S(1)} fusion(bf16[1024,1024]{1,0:T(8,128)(2,1)S(1)} %multiply_convert_fusion, bf16[1,1024,2048]{2,1,0:T(8,128)(2,1)S(1)} %copy-done.8), kind=kOutput, calls=%fused_computation.8 | convolution fusion | flops 4297064448 | bytes 10485760 | tf_op jit(solution)/shard_map/dot_general | solution.py:560
  117.8 56.8 %all_to_all.24 = bf16[128,8,2048]{2,1,0:T(8,128)(2,1)S(1)} all-to-all(bf16[128,8,2048]{2,1,0:T(8,128)(2,1)S(1)} %convert_bitcast_fusion), channel_id=1, replica_groups=mesh['sp_0'=4,'sp_1'=4,'sp_2'=2,'tp'=4] {'sp_0','sp_1','sp_2','tp'}, dimensions={0} | all-to-all | bytes 8388608 | tf_op jit(solution)/shard_map/all_to_all | solution.py:561
  174.6 1.4 combine.1
  (29 shorter events, 1.7 us)
Async XLA Ops:
  7.5 9.3 %collective-permute-start.2 = (bf16[400,128]{1,0:T(8,128)(2,1)S(1)}, bf16[400,128]{1,0:T(8,128)(2,1)S(1)}, u32[]{:S(2)}, u32[]{:S(2)}) collective-permute-start(bf16[400,128]{1,0:T(8,128)(2,1)S(1)} %pair.1.after_ref.refs_1_), channel_id=1, source_target_pairs={{0,24},{8,0},{16,8},{24,16},{1,25},{9,1},{17,9},{25,17},{2,26},{10... | collective-permute-start | bytes 307208 | tf_op jit(solution)/shard_map/ppermute | solution.py:304
  10.5 6.4 %collective-permute-start.1 = (bf16[400,128]{1,0:T(8,128)(2,1)S(1)}, bf16[400,128]{1,0:T(8,128)(2,1)S(1)}, u32[]{:S(2)}, u32[]{:S(2)}) collective-permute-start(bf16[400,128]{1,0:T(8,128)(2,1)S(1)} %pair.1.after_ref.refs_1_), channel_id=1, source_target_pairs={{0,16},{8,24},{16,0},{24,8},{1,17},{9,25},{17,1},{25,9},{2,18},{10... | collective-permute-start | bytes 307208 | tf_op jit(solution)/shard_map/ppermute | solution.py:304
  10.8 8.1 %collective-permute-start = (bf16[400,128]{1,0:T(8,128)(2,1)S(1)}, bf16[400,128]{1,0:T(8,128)(2,1)S(1)}, u32[]{:S(2)}, u32[]{:S(2)}) collective-permute-start(bf16[400,128]{1,0:T(8,128)(2,1)S(1)} %pair.1.after_ref.refs_1_), channel_id=1, source_target_pairs={{0,8},{8,16},{16,24},{24,0},{1,9},{9,17},{17,25},{25,1},{2,10},{10... | collective-permute-start | bytes 307208 | tf_op jit(solution)/shard_map/ppermute | solution.py:304
  19.1 8.5 %collective-permute-start.5 = (bf16[400,128]{1,0:T(8,128)(2,1)S(1)}, bf16[400,128]{1,0:T(8,128)(2,1)S(1)}, u32[]{:S(2)}, u32[]{:S(2)}) collective-permute-start(bf16[400,128]{1,0:T(8,128)(2,1)S(1)} %get-tuple-element.29.refs_0_), channel_id=1, source_target_pairs={{0,96},{32,0},{64,32},{96,64},{1,97},{33,1},{65,33},{97,65},{2,98}... | collective-permute-start | bytes 307208 | tf_op jit(solution)/shard_map/ppermute | solution.py:304
  22.9 5.1 %collective-permute-start.4 = (bf16[400,128]{1,0:T(8,128)(2,1)S(1)}, bf16[400,128]{1,0:T(8,128)(2,1)S(1)}, u32[]{:S(2)}, u32[]{:S(2)}) collective-permute-start(bf16[400,128]{1,0:T(8,128)(2,1)S(1)} %get-tuple-element.29.refs_0_), channel_id=1, source_target_pairs={{0,64},{32,96},{64,0},{96,32},{1,65},{33,97},{65,1},{97,33},{2,66}... | collective-permute-start | bytes 307208 | tf_op jit(solution)/shard_map/ppermute | solution.py:304
  22.9 7.9 %collective-permute-start.3 = (bf16[400,128]{1,0:T(8,128)(2,1)S(1)}, bf16[400,128]{1,0:T(8,128)(2,1)S(1)}, u32[]{:S(2)}, u32[]{:S(2)}) collective-permute-start(bf16[400,128]{1,0:T(8,128)(2,1)S(1)} %get-tuple-element.29.refs_0_), channel_id=1, source_target_pairs={{0,32},{32,64},{64,96},{96,0},{1,33},{33,65},{65,97},{97,1},{2,34}... | collective-permute-start | bytes 307208 | tf_op jit(solution)/shard_map/ppermute | solution.py:304
  23.6 9.7 %copy-start.1 = (bf16[256,2,256]{2,1,0:T(2,128)(2,1)S(1)}, bf16[256,2,256]{2,1,0:T(2,128)(2,1)}, u32[]{:S(2)}) copy-start(bf16[256,2,256]{2,1,0:T(2,128)(2,1)} %gate_ref.1) | copy-start | bytes 786436
  23.6 9.7 %copy-start.3 = (f32[64]{0:T(128)S(1)}, f32[64]{0:T(128)}, u32[]{:S(2)}) copy-start(f32[64]{0:T(128)} %param.28) | copy-start | bytes 772
  23.6 16.5 %copy-start.4 = (s32[256,2]{0,1:T(2,128)S(1)}, s32[256,2]{0,1:T(2,128)}, u32[]{:S(2)}) copy-start(s32[256,2]{0,1:T(2,128)} %param.34) | copy-start | bytes 6148
  23.6 16.5 %copy-start.5 = (f32[256,2]{0,1:T(2,128)S(1)}, f32[256,2]{0,1:T(2,128)}, u32[]{:S(2)}) copy-start(f32[256,2]{0,1:T(2,128)} %param.35) | copy-start | bytes 6148
  27.5 14.8 %copy-start = (bf16[256,2048]{1,0:T(8,128)(2,1)S(1)}, bf16[256,2048]{1,0:T(8,128)(2,1)}, u32[]{:S(2)}) copy-start(bf16[256,2048]{1,0:T(8,128)(2,1)} %stream_ref.1) | copy-start | bytes 3145732
  27.5 14.8 %copy-start.2 = (f32[2048]{0:T(1024)S(1)}, f32[2048]{0:T(1024)}, u32[]{:S(2)}) copy-start(f32[2048]{0:T(1024)} %param.30) | copy-start | bytes 24580
  35.2 5.5 %collective-permute-start.6 = (bf16[64,512]{1,0:T(8,128)(2,1)S(1)}, bf16[64,512]{1,0:T(8,128)(2,1)S(1)}, u32[]{:S(2)}, u32[]{:S(2)}) collective-permute-start(bf16[64,512]{1,0:T(8,128)(2,1)S(1)} %get-tuple-element.32), channel_id=1, source_target_pairs={{0,1},{1,2},{2,3},{3,0},{4,5},{5,6},{6,7},{7,4},{8,9},{9,10},{10,1... | collective-permute-start | bytes 196616 | tf_op jit(solution)/shard_map/ppermute | solution.py:304
  36.5 5.4 %collective-permute-start.7 = (bf16[64,512]{1,0:T(8,128)(2,1)S(1)}, bf16[64,512]{1,0:T(8,128)(2,1)S(1)}, u32[]{:S(2)}, u32[]{:S(2)}) collective-permute-start(bf16[64,512]{1,0:T(8,128)(2,1)S(1)} %get-tuple-element.33), channel_id=1, source_target_pairs={{0,2},{1,3},{2,0},{3,1},{4,6},{5,7},{6,4},{7,5},{8,10},{9,11},{10,... | collective-permute-start | bytes 196616 | tf_op jit(solution)/shard_map/ppermute | solution.py:304
  38.9 3.4 %collective-permute-start.8 = (bf16[64,512]{1,0:T(8,128)(2,1)S(1)}, bf16[64,512]{1,0:T(8,128)(2,1)S(1)}, u32[]{:S(2)}, u32[]{:S(2)}) collective-permute-start(bf16[64,512]{1,0:T(8,128)(2,1)S(1)} %get-tuple-element.34), channel_id=1, source_target_pairs={{0,3},{1,0},{2,1},{3,2},{4,7},{5,4},{6,5},{7,6},{8,11},{9,8},{10,9... | collective-permute-start | bytes 196616 | tf_op jit(solution)/shard_map/ppermute | solution.py:304
  44.5 58.8 %copy-start.6 = (bf16[1,2048,1024]{2,1,0:T(8,128)(2,1)S(1)}, bf16[1,2048,1024]{2,1,0:T(8,128)(2,1)}, u32[]{:S(2)}) copy-start(bf16[1,2048,1024]{2,1,0:T(8,128)(2,1)} %param.31) | copy-start | bytes 12582916
  103.3 4.5 %copy-start.7 = (bf16[1,2048,1024]{2,1,0:T(8,128)(2,1)S(1)}, bf16[1,2048,1024]{2,1,0:T(8,128)(2,1)}, u32[]{:S(2)}) copy-start(bf16[1,2048,1024]{2,1,0:T(8,128)(2,1)} %param.32) | copy-start | bytes 12582916
  107.8 5.2 %copy-start.8 = (bf16[1,1024,2048]{2,1,0:T(8,128)(2,1)S(1)}, bf16[1,1024,2048]{2,1,0:T(8,128)(2,1)}, u32[]{:S(2)}) copy-start(bf16[1,1024,2048]{2,1,0:T(8,128)(2,1)} %param.33) | copy-start | bytes 12582916

commit v5 on v4

--- a/solution.py
+++ b/solution.py
@@ -51,7 +51,8 @@
         ci = lax.broadcasted_iota(jnp.int32, (TOK, TOK), 1)
         self.same = (ri // BLK) == (ci // BLK)
         self.tri = (self.same & (ci <= ri), self.same & (ci >= ri))
-        self.ones = tuple(jnp.where(t, 1.0, 0.0).astype(BF16) for t in self.tri)
+        ones = [jnp.where(t, 1.0, 0.0).astype(BF16) for t in self.tri]
+        self.ones = [jnp.concatenate([t, t], axis=1) for t in ones]
         self.low = lax.broadcasted_iota(jnp.int32, (1, LANES), 1) < 64
         self.low2 = (lax.broadcasted_iota(jnp.int32, (1, 2 * LANES), 1) % LANES) < 64
         self.ex = jnp.transpose(jnp.concatenate([ex_ref[0], ex_ref[1]], axis=0))
@@ -68,8 +69,7 @@
         ld = jnp.log(1.0 - opening) + self.extra(tile)
         hi = ld.astype(BF16)
         lo = (ld - hi.astype(F32)).astype(BF16)
-        both = dot(self.ones[d], jnp.concatenate([hi, lo], axis=1))
-        inside = (both[:, :LANES] + both[:, LANES:]).reshape(NB, BLK, LANES)
+        inside = dot(self.ones[d], jnp.concatenate([hi, lo], axis=0)).reshape(NB, BLK, LANES)
         edge = BLK - 1 if d == 0 else 0
         end = [inside[b, edge : edge + 1, :] for b in range(NB)]
         start = [None] * NB
@@ -145,16 +145,21 @@
 
 
 def narrow_kernel(
-    nf_hbm, nh_hbm, ex_hbm, v_hbm, nq_hbm, w_hbm, after_ref, out_ref, qr_ref, w_ref,
-    nf_ref, nh_ref, ex_ref, v_ref, nq_ref, sems,
+    nf_hbm, nh_hbm, ex_hbm, v_hbm, nq_hbm, gate_hbm, w_hbm, gain_ref, after_ref, out_ref, qr_ref,
+    gates_ref, w_ref, nf_ref, nh_ref, ex_ref, v_ref, nq_ref, gate_ref, sems,
 ):
     del after_ref
     copies = copied(
-        (nf_hbm, nh_hbm, ex_hbm, v_hbm, nq_hbm, w_hbm), (nf_ref, nh_ref, ex_ref, v_ref, nq_ref, w_ref), sems
+        (nf_hbm, nh_hbm, ex_hbm, v_hbm, nq_hbm, gate_hbm, w_hbm),
+        (nf_ref, nh_ref, ex_ref, v_ref, nq_ref, gate_ref, w_ref), sems,
     )
     for copy in copies[:-1]:
         copy.wait()
     own_outputs(0, nf_ref, nh_ref, ex_ref, v_ref, nq_ref, out_ref, qr_ref)
+    gain = jnp.concatenate([gain_ref[...], gain_ref[...]], axis=1)
+    for u in range(4):
+        c = (u % 2) * LANES
+        gates_ref[u] = silu(gate_ref[:, u // 2, c : c + LANES].astype(F32)) * gain
     copies[-1].wait()
 
 
@@ -327,13 +332,12 @@
     )(*arrays)
 
 
-def mix_kernel(n_out_ref, n_qr_ref, w_out_ref, w_qr_ref, in_ref, pieces_ref, gate_ref, gain_ref, *refs):
+def mix_kernel(n_out_ref, n_qr_ref, w_out_ref, w_qr_ref, in_ref, pieces_ref, gates_ref, *refs):
     *tile_refs, mixed_ref = refs
     low = lax.broadcasted_iota(jnp.int32, (1, LANES), 1) < 64
     low2 = (lax.broadcasted_iota(jnp.int32, (1, 2 * LANES), 1) % LANES) < 64
 
     core = lax.axis_index("sp_2")
-    gain = jnp.concatenate([gain_ref[...], gain_ref[...]], axis=1)
     dec = [unpacked(pieces_ref[d, d, STATE_ROWS:, :]) for d in range(2)]
 
     def entering(tile):
@@ -359,9 +363,7 @@
         first = jnp.sum(jnp.where(low, square, 0.0), axis=-1, keepdims=True)
         second = jnp.sum(jnp.where(low, 0.0, square), axis=-1, keepdims=True)
         scale = lax.rsqrt(jnp.where(low, first, second) * (1.0 / 64) + EPS)
-        c = (u % 2) * LANES
-        gate = silu(gate_ref[:, u // 2, c : c + LANES].astype(F32))
-        mixed = o * scale * gain * gate
+        mixed = o * scale * gates_ref[u]
         mixed_ref[:, u * LANES : (u + 1) * LANES] = mixed.astype(BF16)
     count, rows = len(tile_refs), tile_refs[0].shape[0]
     for j, tile_ref in enumerate(tile_refs):
@@ -508,9 +510,14 @@
         token, *chips,
     )
     rows_ = [row, *from_each(row, "sp_0")]
-    narrow, narrow_q, mixer_weight = from_hbm(
-        narrow_kernel, "narrow_outputs", (nf, nh, extra, values, nq, in_hbm(mixer_output_weight)),
-        (own, queries(2), pltpu.VMEM(mixer_output_weight.shape, BF16)), 20, after=(d,), kept=1,
+    narrow, narrow_q, gates, mixer_weight = from_hbm(
+        narrow_kernel, "narrow_outputs",
+        (nf, nh, extra, values, nq, in_hbm(output_gate_logits), in_hbm(mixer_output_weight)),
+        (
+            own, queries(2), jax.ShapeDtypeStruct((4, TOK, LANES), F32),
+            pltpu.VMEM(mixer_output_weight.shape, BF16),
+        ),
+        20, after=(per_head_norm_gain.reshape(1, 64), d), kept=1,
         flops=3 * 10**9,
     )
     entering = small_call(
@@ -522,7 +529,7 @@
     rows = TOK // tp
     tiles = small_call(
         mix_kernel, "mix", (jax.ShapeDtypeStruct((rows, 4 * LANES), BF16),) * tp, narrow, narrow_q,
-        wide, wide_q, entering, pieces, output_gate_logits, per_head_norm_gain.reshape(1, 64),
+        wide, wide_q, entering, pieces, gates,
         scratch=[pltpu.VMEM((TOK, 4 * LANES), BF16)],
     )
     width = stream.shape[1]

time: 176 us -> 177 us (level)
  waiting for transfers between devices: 6.92 us -> 4.18 us
  Pallas kernels: 20 us -> 22 us
  blocking collectives: 121 us -> 123 us
    pallas_call x3, Pallas kernels: 13.7 us -> 16.9 us  [from_hbm(): pl.pallas_call(kernel, out_shape=shapes, in_specs=[HBM] * len(inputs) + [...]
    ppermute x9, waiting for transfers between devices: 6.92 us -> 4.18 us  [from_each(): lax.ppermute(x if tiles is None else tiles[j], axis, [(i, (i + j) % count...]
    all_to_all x1, blocking collectives: 58.8 us -> 60.8 us  [local(): tokens = lax.all_to_all(buffers, SP_TP, 0, 0, tiled=True)]
  transfers between devices with their start and end apart: 9 -> 9, of which waited for: 5 -> 4; matrix products, arithmetic and copies ran while one was open for 0% -> 0% of each run, Pallas kernels for 6% -> 7%
where the time goes in v5:
time: 177 us
  blocking collectives  123 us (69%)
  Pallas kernels  22 us (12%)
  matrix products  14.4 us (8%)
  starting transfers between devices  13.3 us (8%)
  waiting for transfers between devices  4.18 us (2%)
    all_to_all x1, blocking collectives, local(): tokens = lax.all_to_all(buffers, SP_TP, 0, 0, tiled=True)  60.8 us
    all_to_all x1, blocking collectives, local(): back = lax.all_to_all(part, SP_TP, 0, 0, tiled=True)  56.8 us
    pallas_call x3, Pallas kernels, from_hbm(): pl.pallas_call(kernel, out_shape=shapes, in_specs=[HBM] * len(inputs) + [...  16.9 us
    ppermute x9, starting transfers between devices, from_each(): lax.ppermute(x if tiles is None else tiles[j], axis, [(i, (i + j) % count...  13.3 us
    dot_general x1, matrix products, local(): up = jnp.dot(tokens, expert_up_matrix[0], preferred_element_type=F32)  5.2 us
    dot_general x1, matrix products, local(): jnp.dot(hidden, expert_down_matrix[0], preferred_element_type=F32)  4.73 us
    dot_general x1, matrix products, local(): gate = jnp.dot(tokens, expert_gate_matrix[0], preferred_element_type=F32)  4.49 us
    ppermute x9, waiting for transfers between devices, from_each(): lax.ppermute(x if tiles is None else tiles[j], axis, [(i, (i + j) % count...  4.18 us
  transfers between devices with their start and end apart: 9, of which 4 were waited for; matrix products, arithmetic and copies ran while one was open for 0% of the time, Pallas kernels for 7%

profile of v5, /device:TPU:1, one launch (start us, length us, event | category | flops | bytes accessed | tf_op | source)
XLA Modules:
  0.0 177.3 jit_solution(15131908440683390751)
XLA Ops:
  0.0 4.9 %local_states.1 = bf16[2,400,128]{2,1,0:T(8,128)(2,1)S(1)} custom-call(bf16[2,256,256]{2,1,0:T(8,128)(2,1)} %nf_hbm.3, f32[2,256]{1,0:T(2,128)} %nh_hbm.3, f32[2,4,256]{2,1,0:T(4,128)} %bitcast.41, bf16[256,2,256]{2,1,0:T(2,128)(2,1)} %v_hbm.5, bf16[2,256,512]{2,1,0:T(8,128)(2,1)} %wf_hbm.3, f32[2,512]{1,0:T(2,128)} %wh_hbm.3), custom_call_target="tpu_custom_call" | custom-call | flops 1000000000 | bytes 3145728 | tf_op jit(solution)/shard_map/local_states/pallas_call | solution.py:475
  4.9 3.1 %all-gather = bf16[4,400,128]{2,1,0:T(8,128)(2,1)S(1)} all-gather(bf16[2,400,128]{2,1,0:T(8,128)(2,1)S(1)} %local_states.1), channel_id=2, replica_groups=mesh['sp_0'=4,'sp_1'=4,'sp_2'=2,'tp'=4] {'sp_2'}, dimensions={0}, use_global_device_ids=true | all-gather | bytes 614400 | tf_op jit(solution)/shard_map/all_gather | solution.py:501
  8.1 2.9 %collective-permute-start.2 = (bf16[400,128]{1,0:T(8,128)(2,1)S(1)}, bf16[400,128]{1,0:T(8,128)(2,1)S(1)}, u32[]{:S(2)}, u32[]{:S(2)}) collective-permute-start(bf16[400,128]{1,0:T(8,128)(2,1)S(1)} %pair.1.after_ref.refs_1_), channel_id=1, source_target_pairs={{0,24},{8,0},{16,8},{24,16},{1,25},{9,1},{17,9},{25,17},{2,26},{10... | collective-permute-start | bytes 307208 | tf_op jit(solution)/shard_map/ppermute | solution.py:309
  11.3 0.7 collective-permute-start
  12.0 5.8 %wide_outputs.1 = (f32[2,256,128]{2,1,0:T(8,128)S(1)}, bf16[4,256,256]{2,1,0:T(8,128)(2,1)S(1)}, f32[8,128]{1,0:T(8,128)S(1)}) custom-call(bf16[2,256,512]{2,1,0:T(8,128)(2,1)} %wf_hbm.3, f32[2,512]{1,0:T(2,128)} %wh_hbm.3, f32[2,4,256]{2,1,0:T(4,128)} %bitcast.42, bf16[256,2,256]{2,1,0:T(2,128)(2,1)} %v_hbm.5, bf16[256,512]{1,0:T(8,128)(2,1)} %wq_hbm.1, ...), custom_call_target="tpu_custom_call" | custom-call | flops 3000000000 | bytes 3145728 | tf_op jit(solution)/shard_map/wide_outputs/pallas_call | solution.py:475
  17.9 1.5 collective-permute-done.refs_2_
  19.6 3.8 %collective-permute-start.5 = (bf16[400,128]{1,0:T(8,128)(2,1)S(1)}, bf16[400,128]{1,0:T(8,128)(2,1)S(1)}, u32[]{:S(2)}, u32[]{:S(2)}) collective-permute-start(bf16[400,128]{1,0:T(8,128)(2,1)S(1)} %get-tuple-element.30.refs_0_), channel_id=1, source_target_pairs={{0,96},{32,0},{64,32},{96,64},{1,97},{33,1},{65,33},{97,65},{2,98}... | collective-permute-start | bytes 307208 | tf_op jit(solution)/shard_map/ppermute | solution.py:309
  23.4 0.7 collective-permute-start.3
  24.1 6.2 %narrow_outputs.1 = (f32[2,256,128]{2,1,0:T(8,128)S(1)}, bf16[2,256,256]{2,1,0:T(8,128)(2,1)S(1)}, f32[4,256,128]{2,1,0:T(8,128)S(1)}, bf16[2,1024,2048]{2,1,0:T(8,128)(2,1)S(1)}) custom-call(bf16[2,256,256]{2,1,0:T(8,128)(2,1)} %nf_hbm.3, f32[2,256]{1,0:T(2,128)} %nh_hbm.3, f32[2,4,256]{2,1,0:T(4,128)} %bitcast.43, bf16[256,2,256]{2,1,0:T(2,128)(2,1)} %v_hbm.5, ...), custom_call_target="tpu_custom_call" | custom-call | flops 3000000000 | bytes 3145728 | tf_op jit(solution)/shard_map/narrow_outputs/pallas_call | solution.py:475
  30.4 1.0 collective-permute-done.3.refs_1_
  31.5 2.4 %all-gather.1 = bf16[768,128]{1,0:T(8,128)(2,1)S(1)} all-gather(bf16[384,128]{1,0:T(8,128)(2,1)S(1)} %level_0.1), channel_id=3, replica_groups=mesh['sp_0'=4,'sp_1'=4,'sp_2'=2,'tp'=4] {'sp_2'}, dimensions={0}, use_global_device_ids=true | all-gather | bytes 294912 | tf_op jit(solution)/shard_map/all_gather | solution.py:527
  33.8 0.6 mix.1
  34.4 1.3 collective-permute-start.6
  35.7 2.5 %collective-permute-start.7 = (bf16[64,512]{1,0:T(8,128)(2,1)S(1)}, bf16[64,512]{1,0:T(8,128)(2,1)S(1)}, u32[]{:S(2)}, u32[]{:S(2)}) collective-permute-start(bf16[64,512]{1,0:T(8,128)(2,1)S(1)} %get-tuple-element.35), channel_id=1, source_target_pairs={{0,2},{1,3},{2,0},{3,1},{4,6},{5,7},{6,4},{7,5},{8,10},{9,11},{10,... | collective-permute-start | bytes 196616 | tf_op jit(solution)/shard_map/ppermute | solution.py:309
  38.1 1.1 collective-permute-start.8
  39.3 0.6 picks.1
  39.9 1.2 collective-permute-done.7.x2_ref
  41.6 2.1 %project_and_route.1 = (f32[64,2048]{1,0:T(8,128)S(1)}, bf16[32,4,8,2048]{3,2,1,0:T(8,128)(2,1)S(1)}) custom-call(bf16[64,512]{1,0:T(8,128)(2,1)S(1)} %get-tuple-element.33.x0_ref, bf16[64,512]{1,0:T(8,128)(2,1)S(1)} %collective-permute-done.6.x1_ref, bf16[64,512]{1,0:T(8,128)(2,1)S(1)} %collective-permute-done.7.x2_ref, ...), custom_call_target="tpu_custom_call" | custom-call | tf_op jit(solution)/shard_map/project_and_route/pallas_call | solution.py:549
  43.7 60.8 %all_to_all.23 = bf16[128,8,2048]{2,1,0:T(8,128)(2,1)S(1)} all-to-all(bf16[128,8,2048]{2,1,0:T(8,128)(2,1)S(1)} %bitcast.33), channel_id=1, replica_groups=mesh['sp_0'=4,'sp_1'=4,'sp_2'=2,'tp'=4] {'sp_0','sp_1','sp_2','tp'}, dimensions={0} | all-to-all | bytes 8388608 | tf_op jit(solution)/shard_map/all_to_all | solution.py:563
  104.5 4.5 %fusion.4 = f32[1024,1024]{1,0:T(8,128)S(1)} fusion(bf16[1,2048,1024]{2,1,0:T(8,128)(2,1)S(1)} %copy-done.5, bf16[128,8,2048]{2,1,0:T(8,128)(2,1)S(1)} %all_to_all.23), kind=kOutput, calls=%fused_computation.4 | convolution fusion | flops 4294967296 | bytes 12582912 | tf_op jit(solution)/shard_map/dot_general | solution.py:564
  109.1 5.2 %multiply_convert_fusion = bf16[1024,1024]{1,0:T(8,128)(2,1)S(1)} fusion(f32[1024,1024]{1,0:T(8,128)S(1)} %fusion.4, bf16[1,2048,1024]{2,1,0:T(8,128)(2,1)S(1)} %copy-done.6, bf16[128,8,2048]{2,1,0:T(8,128)(2,1)S(1)} %all_to_all.23), kind=kOutput, calls=%fused_computation.9 | convolution fusion | flops 4301258752 | bytes 14680064 | tf_op jit(solution)/shard_map/dot_general | solution.py:565
  114.3 4.7 %convert_bitcast_fusion = bf16[128,8,2048]{2,1,0:T(8,128)(2,1)S(1)} fusion(bf16[1024,1024]{1,0:T(8,128)(2,1)S(1)} %multiply_convert_fusion, bf16[1,1024,2048]{2,1,0:T(8,128)(2,1)S(1)} %copy-done.7), kind=kOutput, calls=%fused_computation.8 | convolution fusion | flops 4297064448 | bytes 10485760 | tf_op jit(solution)/shard_map/dot_general | solution.py:567
  119.0 56.8 %all_to_all.24 = bf16[128,8,2048]{2,1,0:T(8,128)(2,1)S(1)} all-to-all(bf16[128,8,2048]{2,1,0:T(8,128)(2,1)S(1)} %convert_bitcast_fusion), channel_id=1, replica_groups=mesh['sp_0'=4,'sp_1'=4,'sp_2'=2,'tp'=4] {'sp_0','sp_1','sp_2','tp'}, dimensions={0} | all-to-all | bytes 8388608 | tf_op jit(solution)/shard_map/all_to_all | solution.py:568
  175.8 1.4 combine.1
  (27 shorter events, 1.2 us)
Async XLA Ops:
  8.0 16.1 %copy-start.4 = (f32[64]{0:T(128)S(1)}, f32[64]{0:T(128)}, u32[]{:S(2)}) copy-start(f32[64]{0:T(128)} %param.28) | copy-start | bytes 772
  8.1 9.8 %collective-permute-start.2 = (bf16[400,128]{1,0:T(8,128)(2,1)S(1)}, bf16[400,128]{1,0:T(8,128)(2,1)S(1)}, u32[]{:S(2)}, u32[]{:S(2)}) collective-permute-start(bf16[400,128]{1,0:T(8,128)(2,1)S(1)} %pair.1.after_ref.refs_1_), channel_id=1, source_target_pairs={{0,24},{8,0},{16,8},{24,16},{1,25},{9,1},{17,9},{25,17},{2,26},{10... | collective-permute-start | bytes 307208 | tf_op jit(solution)/shard_map/ppermute | solution.py:309
  11.0 6.9 %collective-permute-start.1 = (bf16[400,128]{1,0:T(8,128)(2,1)S(1)}, bf16[400,128]{1,0:T(8,128)(2,1)S(1)}, u32[]{:S(2)}, u32[]{:S(2)}) collective-permute-start(bf16[400,128]{1,0:T(8,128)(2,1)S(1)} %pair.1.after_ref.refs_1_), channel_id=1, source_target_pairs={{0,16},{8,24},{16,0},{24,8},{1,17},{9,25},{17,1},{25,9},{2,18},{10... | collective-permute-start | bytes 307208 | tf_op jit(solution)/shard_map/ppermute | solution.py:309
  11.3 8.1 %collective-permute-start = (bf16[400,128]{1,0:T(8,128)(2,1)S(1)}, bf16[400,128]{1,0:T(8,128)(2,1)S(1)}, u32[]{:S(2)}, u32[]{:S(2)}) collective-permute-start(bf16[400,128]{1,0:T(8,128)(2,1)S(1)} %pair.1.after_ref.refs_1_), channel_id=1, source_target_pairs={{0,8},{8,16},{16,24},{24,0},{1,9},{9,17},{17,25},{25,1},{2,10},{10... | collective-permute-start | bytes 307208 | tf_op jit(solution)/shard_map/ppermute | solution.py:309
  19.6 10.8 %collective-permute-start.5 = (bf16[400,128]{1,0:T(8,128)(2,1)S(1)}, bf16[400,128]{1,0:T(8,128)(2,1)S(1)}, u32[]{:S(2)}, u32[]{:S(2)}) collective-permute-start(bf16[400,128]{1,0:T(8,128)(2,1)S(1)} %get-tuple-element.30.refs_0_), channel_id=1, source_target_pairs={{0,96},{32,0},{64,32},{96,64},{1,97},{33,1},{65,33},{97,65},{2,98}... | collective-permute-start | bytes 307208 | tf_op jit(solution)/shard_map/ppermute | solution.py:309
  23.4 7.0 %collective-permute-start.4 = (bf16[400,128]{1,0:T(8,128)(2,1)S(1)}, bf16[400,128]{1,0:T(8,128)(2,1)S(1)}, u32[]{:S(2)}, u32[]{:S(2)}) collective-permute-start(bf16[400,128]{1,0:T(8,128)(2,1)S(1)} %get-tuple-element.30.refs_0_), channel_id=1, source_target_pairs={{0,64},{32,96},{64,0},{96,32},{1,65},{33,97},{65,1},{97,33},{2,66}... | collective-permute-start | bytes 307208 | tf_op jit(solution)/shard_map/ppermute | solution.py:309
  23.4 7.9 %collective-permute-start.3 = (bf16[400,128]{1,0:T(8,128)(2,1)S(1)}, bf16[400,128]{1,0:T(8,128)(2,1)S(1)}, u32[]{:S(2)}, u32[]{:S(2)}) collective-permute-start(bf16[400,128]{1,0:T(8,128)(2,1)S(1)} %get-tuple-element.30.refs_0_), channel_id=1, source_target_pairs={{0,32},{32,64},{64,96},{96,0},{1,33},{33,65},{65,97},{97,1},{2,34}... | collective-permute-start | bytes 307208 | tf_op jit(solution)/shard_map/ppermute | solution.py:309
  24.1 15.2 %copy-start.2 = (s32[256,2]{0,1:T(2,128)S(1)}, s32[256,2]{0,1:T(2,128)}, u32[]{:S(2)}) copy-start(s32[256,2]{0,1:T(2,128)} %param.34) | copy-start | bytes 6148
  24.1 15.2 %copy-start.3 = (f32[256,2]{0,1:T(2,128)S(1)}, f32[256,2]{0,1:T(2,128)}, u32[]{:S(2)}) copy-start(f32[256,2]{0,1:T(2,128)} %param.35) | copy-start | bytes 6148
  30.3 11.2 %copy-start = (bf16[256,2048]{1,0:T(8,128)(2,1)S(1)}, bf16[256,2048]{1,0:T(8,128)(2,1)}, u32[]{:S(2)}) copy-start(bf16[256,2048]{1,0:T(8,128)(2,1)} %stream_ref.1) | copy-start | bytes 3145732
  30.3 11.2 %copy-start.1 = (f32[2048]{0:T(1024)S(1)}, f32[2048]{0:T(1024)}, u32[]{:S(2)}) copy-start(f32[2048]{0:T(1024)} %param.30) | copy-start | bytes 24580
  34.4 5.4 %collective-permute-start.6 = (bf16[64,512]{1,0:T(8,128)(2,1)S(1)}, bf16[64,512]{1,0:T(8,128)(2,1)S(1)}, u32[]{:S(2)}, u32[]{:S(2)}) collective-permute-start(bf16[64,512]{1,0:T(8,128)(2,1)S(1)} %get-tuple-element.34), channel_id=1, source_target_pairs={{0,1},{1,2},{2,3},{3,0},{4,5},{5,6},{6,7},{7,4},{8,9},{9,10},{10,1... | collective-permute-start | bytes 196616 | tf_op jit(solution)/shard_map/ppermute | solution.py:309
  35.7 5.4 %collective-permute-start.7 = (bf16[64,512]{1,0:T(8,128)(2,1)S(1)}, bf16[64,512]{1,0:T(8,128)(2,1)S(1)}, u32[]{:S(2)}, u32[]{:S(2)}) collective-permute-start(bf16[64,512]{1,0:T(8,128)(2,1)S(1)} %get-tuple-element.35), channel_id=1, source_target_pairs={{0,2},{1,3},{2,0},{3,1},{4,6},{5,7},{6,4},{7,5},{8,10},{9,11},{10,... | collective-permute-start | bytes 196616 | tf_op jit(solution)/shard_map/ppermute | solution.py:309
  38.1 3.4 %collective-permute-start.8 = (bf16[64,512]{1,0:T(8,128)(2,1)S(1)}, bf16[64,512]{1,0:T(8,128)(2,1)S(1)}, u32[]{:S(2)}, u32[]{:S(2)}) collective-permute-start(bf16[64,512]{1,0:T(8,128)(2,1)S(1)} %get-tuple-element.36), channel_id=1, source_target_pairs={{0,3},{1,0},{2,1},{3,2},{4,7},{5,4},{6,5},{7,6},{8,11},{9,8},{10,9... | collective-permute-start | bytes 196616 | tf_op jit(solution)/shard_map/ppermute | solution.py:309
  43.7 60.9 %copy-start.5 = (bf16[1,2048,1024]{2,1,0:T(8,128)(2,1)S(1)}, bf16[1,2048,1024]{2,1,0:T(8,128)(2,1)}, u32[]{:S(2)}) copy-start(bf16[1,2048,1024]{2,1,0:T(8,128)(2,1)} %param.31) | copy-start | bytes 12582916
  104.5 4.5 %copy-start.6 = (bf16[1,2048,1024]{2,1,0:T(8,128)(2,1)S(1)}, bf16[1,2048,1024]{2,1,0:T(8,128)(2,1)}, u32[]{:S(2)}) copy-start(bf16[1,2048,1024]{2,1,0:T(8,128)(2,1)} %param.32) | copy-start | bytes 12582916
  109.0 5.2 %copy-start.7 = (bf16[1,1024,2048]{2,1,0:T(8,128)(2,1)S(1)}, bf16[1,1024,2048]{2,1,0:T(8,128)(2,1)}, u32[]{:S(2)}) copy-start(bf16[1,1024,2048]{2,1,0:T(8,128)(2,1)} %param.33) | copy-start | bytes 12582916

commit v6 on v5

--- a/solution.py
+++ b/solution.py
@@ -51,8 +51,7 @@
         ci = lax.broadcasted_iota(jnp.int32, (TOK, TOK), 1)
         self.same = (ri // BLK) == (ci // BLK)
         self.tri = (self.same & (ci <= ri), self.same & (ci >= ri))
-        ones = [jnp.where(t, 1.0, 0.0).astype(BF16) for t in self.tri]
-        self.ones = [jnp.concatenate([t, t], axis=1) for t in ones]
+        self.ones = tuple(jnp.where(t, 1.0, 0.0).astype(BF16) for t in self.tri)
         self.low = lax.broadcasted_iota(jnp.int32, (1, LANES), 1) < 64
         self.low2 = (lax.broadcasted_iota(jnp.int32, (1, 2 * LANES), 1) % LANES) < 64
         self.ex = jnp.transpose(jnp.concatenate([ex_ref[0], ex_ref[1]], axis=0))
@@ -69,7 +68,8 @@
         ld = jnp.log(1.0 - opening) + self.extra(tile)
         hi = ld.astype(BF16)
         lo = (ld - hi.astype(F32)).astype(BF16)
-        inside = dot(self.ones[d], jnp.concatenate([hi, lo], axis=0)).reshape(NB, BLK, LANES)
+        both = dot(self.ones[d], jnp.concatenate([hi, lo], axis=1))
+        inside = (both[:, :LANES] + both[:, LANES:]).reshape(NB, BLK, LANES)
         edge = BLK - 1 if d == 0 else 0
         end = [inside[b, edge : edge + 1, :] for b in range(NB)]
         start = [None] * NB

time: 177 us -> 176 us (level)
  no operation moved by 1% of the time
where the time goes in v6:
time: 176 us
  blocking collectives  123 us (70%)
  Pallas kernels  20.9 us (12%)
  matrix products  14.4 us (8%)
  starting transfers between devices  13.4 us (8%)
  waiting for transfers between devices  4.7 us (3%)
    all_to_all x1, blocking collectives, local(): tokens = lax.all_to_all(buffers, SP_TP, 0, 0, tiled=True)  60.3 us
    all_to_all x1, blocking collectives, local(): back = lax.all_to_all(part, SP_TP, 0, 0, tiled=True)  56.8 us
    pallas_call x3, Pallas kernels, from_hbm(): pl.pallas_call(kernel, out_shape=shapes, in_specs=[HBM] * len(inputs) + [...  15.9 us
    ppermute x9, starting transfers between devices, from_each(): lax.ppermute(x if tiles is None else tiles[j], axis, [(i, (i + j) % count...  13.4 us
    dot_general x1, matrix products, local(): up = jnp.dot(tokens, expert_up_matrix[0], preferred_element_type=F32)  5.2 us
    dot_general x1, matrix products, local(): jnp.dot(hidden, expert_down_matrix[0], preferred_element_type=F32)  4.73 us
    ppermute x9, waiting for transfers between devices, from_each(): lax.ppermute(x if tiles is None else tiles[j], axis, [(i, (i + j) % count...  4.7 us
    dot_general x1, matrix products, local(): gate = jnp.dot(tokens, expert_gate_matrix[0], preferred_element_type=F32)  4.49 us
  transfers between devices with their start and end apart: 9, of which 4 were waited for; matrix products, arithmetic and copies ran while one was open for 0% of the time, Pallas kernels for 7%

profile of v6, /device:TPU:1, one launch (start us, length us, event | category | flops | bytes accessed | tf_op | source)
XLA Modules:
  0.0 176.2 jit_solution(2792737169373541194)
XLA Ops:
  0.0 4.4 %local_states.1 = bf16[2,400,128]{2,1,0:T(8,128)(2,1)S(1)} custom-call(bf16[2,256,256]{2,1,0:T(8,128)(2,1)} %nf_hbm.3, f32[2,256]{1,0:T(2,128)} %nh_hbm.3, f32[2,4,256]{2,1,0:T(4,128)} %bitcast.41, bf16[256,2,256]{2,1,0:T(2,128)(2,1)} %v_hbm.5, bf16[2,256,512]{2,1,0:T(8,128)(2,1)} %wf_hbm.3, f32[2,512]{1,0:T(2,128)} %wh_hbm.3), custom_call_target="tpu_custom_call" | custom-call | flops 1000000000 | bytes 3145728 | tf_op jit(solution)/shard_map/local_states/pallas_call | solution.py:475
  4.4 3.1 %all-gather = bf16[4,400,128]{2,1,0:T(8,128)(2,1)S(1)} all-gather(bf16[2,400,128]{2,1,0:T(8,128)(2,1)S(1)} %local_states.1), channel_id=2, replica_groups=mesh['sp_0'=4,'sp_1'=4,'sp_2'=2,'tp'=4] {'sp_2'}, dimensions={0}, use_global_device_ids=true | all-gather | bytes 614400 | tf_op jit(solution)/shard_map/all_gather | solution.py:501
  7.6 2.9 %collective-permute-start.2 = (bf16[400,128]{1,0:T(8,128)(2,1)S(1)}, bf16[400,128]{1,0:T(8,128)(2,1)S(1)}, u32[]{:S(2)}, u32[]{:S(2)}) collective-permute-start(bf16[400,128]{1,0:T(8,128)(2,1)S(1)} %pair.1.after_ref.refs_1_), channel_id=1, source_target_pairs={{0,24},{8,0},{16,8},{24,16},{1,25},{9,1},{17,9},{25,17},{2,26},{10... | collective-permute-start | bytes 307208 | tf_op jit(solution)/shard_map/ppermute | solution.py:309
  10.8 0.7 collective-permute-start
  11.5 5.4 %wide_outputs.1 = (f32[2,256,128]{2,1,0:T(8,128)S(1)}, bf16[4,256,256]{2,1,0:T(8,128)(2,1)S(1)}, f32[8,128]{1,0:T(8,128)S(1)}) custom-call(bf16[2,256,512]{2,1,0:T(8,128)(2,1)} %wf_hbm.3, f32[2,512]{1,0:T(2,128)} %wh_hbm.3, f32[2,4,256]{2,1,0:T(4,128)} %bitcast.42, bf16[256,2,256]{2,1,0:T(2,128)(2,1)} %v_hbm.5, bf16[256,512]{1,0:T(8,128)(2,1)} %wq_hbm.1, ...), custom_call_target="tpu_custom_call" | custom-call | flops 3000000000 | bytes 3145728 | tf_op jit(solution)/shard_map/wide_outputs/pallas_call | solution.py:475
  16.9 2.0 %collective-permute-done.refs_2_ = bf16[400,128]{1,0:T(8,128)(2,1)S(1)} collective-permute-done((bf16[400,128]{1,0:T(8,128)(2,1)S(1)}, bf16[400,128]{1,0:T(8,128)(2,1)S(1)}, u32[]{:S(2)}, u32[]{:S(2)}) %collective-permute-start) | collective-permute-done | bytes 102432 | tf_op jit(solution)/shard_map/ppermute | solution.py:309
  19.1 3.8 %collective-permute-start.5 = (bf16[400,128]{1,0:T(8,128)(2,1)S(1)}, bf16[400,128]{1,0:T(8,128)(2,1)S(1)}, u32[]{:S(2)}, u32[]{:S(2)}) collective-permute-start(bf16[400,128]{1,0:T(8,128)(2,1)S(1)} %get-tuple-element.30.refs_0_), channel_id=1, source_target_pairs={{0,96},{32,0},{64,32},{96,64},{1,97},{33,1},{65,33},{97,65},{2,98}... | collective-permute-start | bytes 307208 | tf_op jit(solution)/shard_map/ppermute | solution.py:309
  22.9 0.7 collective-permute-start.3
  23.6 6.1 %narrow_outputs.1 = (f32[2,256,128]{2,1,0:T(8,128)S(1)}, bf16[2,256,256]{2,1,0:T(8,128)(2,1)S(1)}, f32[4,256,128]{2,1,0:T(8,128)S(1)}, bf16[2,1024,2048]{2,1,0:T(8,128)(2,1)S(1)}) custom-call(bf16[2,256,256]{2,1,0:T(8,128)(2,1)} %nf_hbm.3, f32[2,256]{1,0:T(2,128)} %nh_hbm.3, f32[2,4,256]{2,1,0:T(4,128)} %bitcast.43, bf16[256,2,256]{2,1,0:T(2,128)(2,1)} %v_hbm.5, ...), custom_call_target="tpu_custom_call" | custom-call | flops 3000000000 | bytes 3145728 | tf_op jit(solution)/shard_map/narrow_outputs/pallas_call | solution.py:475
  29.8 1.1 collective-permute-done.3.refs_1_
  31.0 2.4 %all-gather.1 = bf16[768,128]{1,0:T(8,128)(2,1)S(1)} all-gather(bf16[384,128]{1,0:T(8,128)(2,1)S(1)} %level_0.1), channel_id=3, replica_groups=mesh['sp_0'=4,'sp_1'=4,'sp_2'=2,'tp'=4] {'sp_2'}, dimensions={0}, use_global_device_ids=true | all-gather | bytes 294912 | tf_op jit(solution)/shard_map/all_gather | solution.py:527
  33.3 0.6 mix.1
  33.9 1.3 collective-permute-start.6
  35.2 2.4 %collective-permute-start.7 = (bf16[64,512]{1,0:T(8,128)(2,1)S(1)}, bf16[64,512]{1,0:T(8,128)(2,1)S(1)}, u32[]{:S(2)}, u32[]{:S(2)}) collective-permute-start(bf16[64,512]{1,0:T(8,128)(2,1)S(1)} %get-tuple-element.35), channel_id=1, source_target_pairs={{0,2},{1,3},{2,0},{3,1},{4,6},{5,7},{6,4},{7,5},{8,10},{9,11},{10,... | collective-permute-start | bytes 196616 | tf_op jit(solution)/shard_map/ppermute | solution.py:309
  37.6 1.2 collective-permute-start.8
  38.8 0.6 picks.1
  39.4 1.2 collective-permute-done.7.x2_ref
  41.1 2.1 %project_and_route.1 = (f32[64,2048]{1,0:T(8,128)S(1)}, bf16[32,4,8,2048]{3,2,1,0:T(8,128)(2,1)S(1)}) custom-call(bf16[64,512]{1,0:T(8,128)(2,1)S(1)} %get-tuple-element.33.x0_ref, bf16[64,512]{1,0:T(8,128)(2,1)S(1)} %collective-permute-done.6.x1_ref, bf16[64,512]{1,0:T(8,128)(2,1)S(1)} %collective-permute-done.7.x2_ref, ...), custom_call_target="tpu_custom_call" | custom-call | tf_op jit(solution)/shard_map/project_and_route/pallas_call | solution.py:549
  43.2 60.3 %all_to_all.23 = bf16[128,8,2048]{2,1,0:T(8,128)(2,1)S(1)} all-to-all(bf16[128,8,2048]{2,1,0:T(8,128)(2,1)S(1)} %bitcast.33), channel_id=1, replica_groups=mesh['sp_0'=4,'sp_1'=4,'sp_2'=2,'tp'=4] {'sp_0','sp_1','sp_2','tp'}, dimensions={0} | all-to-all | bytes 8388608 | tf_op jit(solution)/shard_map/all_to_all | solution.py:563
  103.5 4.5 %fusion.4 = f32[1024,1024]{1,0:T(8,128)S(1)} fusion(bf16[1,2048,1024]{2,1,0:T(8,128)(2,1)S(1)} %copy-done.5, bf16[128,8,2048]{2,1,0:T(8,128)(2,1)S(1)} %all_to_all.23), kind=kOutput, calls=%fused_computation.4 | convolution fusion | flops 4294967296 | bytes 12582912 | tf_op jit(solution)/shard_map/dot_general | solution.py:564
  108.0 5.2 %multiply_convert_fusion = bf16[1024,1024]{1,0:T(8,128)(2,1)S(1)} fusion(f32[1024,1024]{1,0:T(8,128)S(1)} %fusion.4, bf16[1,2048,1024]{2,1,0:T(8,128)(2,1)S(1)} %copy-done.6, bf16[128,8,2048]{2,1,0:T(8,128)(2,1)S(1)} %all_to_all.23), kind=kOutput, calls=%fused_computation.9 | convolution fusion | flops 4301258752 | bytes 14680064 | tf_op jit(solution)/shard_map/dot_general | solution.py:565
  113.2 4.7 %convert_bitcast_fusion = bf16[128,8,2048]{2,1,0:T(8,128)(2,1)S(1)} fusion(bf16[1024,1024]{1,0:T(8,128)(2,1)S(1)} %multiply_convert_fusion, bf16[1,1024,2048]{2,1,0:T(8,128)(2,1)S(1)} %copy-done.7), kind=kOutput, calls=%fused_computation.8 | convolution fusion | flops 4297064448 | bytes 10485760 | tf_op jit(solution)/shard_map/dot_general | solution.py:567
  117.9 56.8 %all_to_all.24 = bf16[128,8,2048]{2,1,0:T(8,128)(2,1)S(1)} all-to-all(bf16[128,8,2048]{2,1,0:T(8,128)(2,1)S(1)} %convert_bitcast_fusion), channel_id=1, replica_groups=mesh['sp_0'=4,'sp_1'=4,'sp_2'=2,'tp'=4] {'sp_0','sp_1','sp_2','tp'}, dimensions={0} | all-to-all | bytes 8388608 | tf_op jit(solution)/shard_map/all_to_all | solution.py:568
  174.7 1.4 combine.1
  (27 shorter events, 1.2 us)
Async XLA Ops:
  7.5 16.1 %copy-start.4 = (f32[64]{0:T(128)S(1)}, f32[64]{0:T(128)}, u32[]{:S(2)}) copy-start(f32[64]{0:T(128)} %param.28) | copy-start | bytes 772
  7.6 9.4 %collective-permute-start.2 = (bf16[400,128]{1,0:T(8,128)(2,1)S(1)}, bf16[400,128]{1,0:T(8,128)(2,1)S(1)}, u32[]{:S(2)}, u32[]{:S(2)}) collective-permute-start(bf16[400,128]{1,0:T(8,128)(2,1)S(1)} %pair.1.after_ref.refs_1_), channel_id=1, source_target_pairs={{0,24},{8,0},{16,8},{24,16},{1,25},{9,1},{17,9},{25,17},{2,26},{10... | collective-permute-start | bytes 307208 | tf_op jit(solution)/shard_map/ppermute | solution.py:309
  10.5 6.4 %collective-permute-start.1 = (bf16[400,128]{1,0:T(8,128)(2,1)S(1)}, bf16[400,128]{1,0:T(8,128)(2,1)S(1)}, u32[]{:S(2)}, u32[]{:S(2)}) collective-permute-start(bf16[400,128]{1,0:T(8,128)(2,1)S(1)} %pair.1.after_ref.refs_1_), channel_id=1, source_target_pairs={{0,16},{8,24},{16,0},{24,8},{1,17},{9,25},{17,1},{25,9},{2,18},{10... | collective-permute-start | bytes 307208 | tf_op jit(solution)/shard_map/ppermute | solution.py:309
  10.8 8.1 %collective-permute-start = (bf16[400,128]{1,0:T(8,128)(2,1)S(1)}, bf16[400,128]{1,0:T(8,128)(2,1)S(1)}, u32[]{:S(2)}, u32[]{:S(2)}) collective-permute-start(bf16[400,128]{1,0:T(8,128)(2,1)S(1)} %pair.1.after_ref.refs_1_), channel_id=1, source_target_pairs={{0,8},{8,16},{16,24},{24,0},{1,9},{9,17},{17,25},{25,1},{2,10},{10... | collective-permute-start | bytes 307208 | tf_op jit(solution)/shard_map/ppermute | solution.py:309
  19.1 10.7 %collective-permute-start.5 = (bf16[400,128]{1,0:T(8,128)(2,1)S(1)}, bf16[400,128]{1,0:T(8,128)(2,1)S(1)}, u32[]{:S(2)}, u32[]{:S(2)}) collective-permute-start(bf16[400,128]{1,0:T(8,128)(2,1)S(1)} %get-tuple-element.30.refs_0_), channel_id=1, source_target_pairs={{0,96},{32,0},{64,32},{96,64},{1,97},{33,1},{65,33},{97,65},{2,98}... | collective-permute-start | bytes 307208 | tf_op jit(solution)/shard_map/ppermute | solution.py:309
  22.9 6.9 %collective-permute-start.4 = (bf16[400,128]{1,0:T(8,128)(2,1)S(1)}, bf16[400,128]{1,0:T(8,128)(2,1)S(1)}, u32[]{:S(2)}, u32[]{:S(2)}) collective-permute-start(bf16[400,128]{1,0:T(8,128)(2,1)S(1)} %get-tuple-element.30.refs_0_), channel_id=1, source_target_pairs={{0,64},{32,96},{64,0},{96,32},{1,65},{33,97},{65,1},{97,33},{2,66}... | collective-permute-start | bytes 307208 | tf_op jit(solution)/shard_map/ppermute | solution.py:309
  22.9 7.9 %collective-permute-start.3 = (bf16[400,128]{1,0:T(8,128)(2,1)S(1)}, bf16[400,128]{1,0:T(8,128)(2,1)S(1)}, u32[]{:S(2)}, u32[]{:S(2)}) collective-permute-start(bf16[400,128]{1,0:T(8,128)(2,1)S(1)} %get-tuple-element.30.refs_0_), channel_id=1, source_target_pairs={{0,32},{32,64},{64,96},{96,0},{1,33},{33,65},{65,97},{97,1},{2,34}... | collective-permute-start | bytes 307208 | tf_op jit(solution)/shard_map/ppermute | solution.py:309
  23.6 15.2 %copy-start.2 = (s32[256,2]{0,1:T(2,128)S(1)}, s32[256,2]{0,1:T(2,128)}, u32[]{:S(2)}) copy-start(s32[256,2]{0,1:T(2,128)} %param.34) | copy-start | bytes 6148
  23.6 15.2 %copy-start.3 = (f32[256,2]{0,1:T(2,128)S(1)}, f32[256,2]{0,1:T(2,128)}, u32[]{:S(2)}) copy-start(f32[256,2]{0,1:T(2,128)} %param.35) | copy-start | bytes 6148
  29.7 11.3 %copy-start = (bf16[256,2048]{1,0:T(8,128)(2,1)S(1)}, bf16[256,2048]{1,0:T(8,128)(2,1)}, u32[]{:S(2)}) copy-start(bf16[256,2048]{1,0:T(8,128)(2,1)} %stream_ref.1) | copy-start | bytes 3145732
  29.7 11.3 %copy-start.1 = (f32[2048]{0:T(1024)S(1)}, f32[2048]{0:T(1024)}, u32[]{:S(2)}) copy-start(f32[2048]{0:T(1024)} %param.30) | copy-start | bytes 24580
  33.9 5.5 %collective-permute-start.6 = (bf16[64,512]{1,0:T(8,128)(2,1)S(1)}, bf16[64,512]{1,0:T(8,128)(2,1)S(1)}, u32[]{:S(2)}, u32[]{:S(2)}) collective-permute-start(bf16[64,512]{1,0:T(8,128)(2,1)S(1)} %get-tuple-element.34), channel_id=1, source_target_pairs={{0,1},{1,2},{2,3},{3,0},{4,5},{5,6},{6,7},{7,4},{8,9},{9,10},{10,1... | collective-permute-start | bytes 196616 | tf_op jit(solution)/shard_map/ppermute | solution.py:309
  35.2 5.4 %collective-permute-start.7 = (bf16[64,512]{1,0:T(8,128)(2,1)S(1)}, bf16[64,512]{1,0:T(8,128)(2,1)S(1)}, u32[]{:S(2)}, u32[]{:S(2)}) collective-permute-start(bf16[64,512]{1,0:T(8,128)(2,1)S(1)} %get-tuple-element.35), channel_id=1, source_target_pairs={{0,2},{1,3},{2,0},{3,1},{4,6},{5,7},{6,4},{7,5},{8,10},{9,11},{10,... | collective-permute-start | bytes 196616 | tf_op jit(solution)/shard_map/ppermute | solution.py:309
  37.6 3.4 %collective-permute-start.8 = (bf16[64,512]{1,0:T(8,128)(2,1)S(1)}, bf16[64,512]{1,0:T(8,128)(2,1)S(1)}, u32[]{:S(2)}, u32[]{:S(2)}) collective-permute-start(bf16[64,512]{1,0:T(8,128)(2,1)S(1)} %get-tuple-element.36), channel_id=1, source_target_pairs={{0,3},{1,0},{2,1},{3,2},{4,7},{5,4},{6,5},{7,6},{8,11},{9,8},{10,9... | collective-permute-start | bytes 196616 | tf_op jit(solution)/shard_map/ppermute | solution.py:309
  43.2 60.3 %copy-start.5 = (bf16[1,2048,1024]{2,1,0:T(8,128)(2,1)S(1)}, bf16[1,2048,1024]{2,1,0:T(8,128)(2,1)}, u32[]{:S(2)}) copy-start(bf16[1,2048,1024]{2,1,0:T(8,128)(2,1)} %param.31) | copy-start | bytes 12582916
  103.5 4.5 %copy-start.6 = (bf16[1,2048,1024]{2,1,0:T(8,128)(2,1)S(1)}, bf16[1,2048,1024]{2,1,0:T(8,128)(2,1)}, u32[]{:S(2)}) copy-start(bf16[1,2048,1024]{2,1,0:T(8,128)(2,1)} %param.32) | copy-start | bytes 12582916
  108.0 5.2 %copy-start.7 = (bf16[1,1024,2048]{2,1,0:T(8,128)(2,1)S(1)}, bf16[1,1024,2048]{2,1,0:T(8,128)(2,1)}, u32[]{:S(2)}) copy-start(bf16[1,1024,2048]{2,1,0:T(8,128)(2,1)} %param.33) | copy-start | bytes 12582916
